TPU v7x, 128 devices: a whole 4x4x4 slice. The times are simulated.
128 devices in a mesh: sp: 32 (over z, y, core), tp: 4 (over x).
Axes of the slice: x: 4, y: 4, z: 4, core: 2. Of those that a mesh axis runs over, the one named last changes fastest.
Arguments:
- residual: bfloat16 [16384, 2048], P(('sp', 'tp')), may hold values from -6 to 6
- query_proj: bfloat16 [16384, 2048], P('sp', 'tp'), may hold values from -12 to 12
- key_proj: bfloat16 [16384, 512], P('sp', 'tp'), may hold values from -12 to 12
- value_proj: bfloat16 [16384, 512], P('sp', 'tp'), may hold values from -6 to 6
- query_gain: float32 [128], replicated, may hold values from 0.4 to 4.5
- key_gain: float32 [128], replicated, may hold values from 0.4 to 4.5
- document_ids: int32 [16384], P('sp'), may hold values from 0 to 15, never falling along the last dimension, each value on 1 to 1537 neighbouring positions
- output_weight: bfloat16 [2048, 2048], replicated, may hold values from -0.125 to 0.125
- norm_gain: float32 [2048], replicated, may hold values from 0.1 to 1.9
- expert_ids: int32 [16384, 2], P(('sp', 'tp')), may hold values from 0 to 127, all different within a row; in each aligned block of 128 rows (0 to 127, 128 to 255, ...) at most 4 rows name the same one
- route_weights: float32 [16384, 2], P(('sp', 'tp')), may hold values from 0.2 to 1
- gate_weight: bfloat16 [128, 2048, 512], P(('sp', 'tp')), may hold values from -0.125 to 0.125
- up_weight: bfloat16 [128, 2048, 512], P(('sp', 'tp')), may hold values from -0.125 to 0.125
- down_weight: bfloat16 [128, 512, 2048], P(('sp', 'tp')), may hold values from -0.25 to 0.25
Outputs:
- updated: bfloat16 [16384, 2048], P(('sp', 'tp'))
Inputs may be any that keep to these rules, and one draw needn't show every extreme that they name: `document_ids`: document numbers never fall along the positions; each document has at most 1537 positions, and one has exactly 1537. `expert_ids`: each row names 2 different experts; within the rows of one device no expert is named more than 4 times, and in some device's rows an expert is named exactly 4 times.
All inputs are finite; a program needn't handle non-finite values.
Results may differ from a plain program's by a relative error of at most 0.017.
Values may be sent and summed in bfloat16 or wider, within the bound.
No kernel may reach another device: no remote copies, remote signals or barrier semaphores. Data moves between devices by JAX's collectives and lax.ppermute only.
A program may use at most 128 MiB of HBM per device.

v0:
```python
import jax
import jax.numpy as jnp
from jax import lax
from jax.sharding import PartitionSpec as P

HEAD = 128
GRID_W = 64
REACH = 3


norm_eps = 1e-06
rope_base = 10000.0
masked_low = -1e30


def from_behind(block, axis, distance):
    devices = range(lax.axis_size(axis))
    route = [(i - distance, i) for i in devices if i - distance in devices]
    return lax.ppermute(block, axis, route)


def rotary_tables(first_row, length):
    freq_count = HEAD // 4
    inverse = 1.0 / rope_base ** (jnp.arange(freq_count, dtype=jnp.float32) / freq_count)
    position = first_row + jnp.arange(length, dtype=jnp.int32)
    grid_row = (position // GRID_W).astype(jnp.float32)
    grid_col = (position % GRID_W).astype(jnp.float32)
    angles = jnp.concatenate(
        [grid_row[:, None] * inverse[None, :], grid_col[:, None] * inverse[None, :]], axis=1
    )
    return (jnp.cos(angles), jnp.sin(angles))


def norm_rotate(projected, gains, cosine, sine_table):
    length = projected.shape[0]
    values_wide = projected.astype(jnp.float32).reshape(length, -1, HEAD)
    scaled = (
        values_wide
        * lax.rsqrt(jnp.mean(values_wide * values_wide, axis=-1, keepdims=True) + norm_eps)
        * gains
    )
    half_size = HEAD // 2
    first_half = scaled[..., :half_size]
    second_half = scaled[..., half_size:]
    cosine_rows = cosine[:, None, :]
    sine_rows = sine_table[:, None, :]
    turned = jnp.concatenate(
        [
            first_half * cosine_rows - second_half * sine_rows,
            first_half * sine_rows + second_half * cosine_rows,
        ],
        axis=-1,
    )
    return turned.reshape(length, -1).astype(jnp.bfloat16)


def on_device(
    residual,
    query_proj,
    key_proj,
    value_proj,
    query_gain,
    key_gain,
    document_ids,
    output_weight,
    norm_gain,
    expert_ids,
    route_weights,
    gate_weight,
    up_weight,
    down_weight,
):
    rows_here = query_proj.shape[0]
    cosine, sine_table = rotary_tables(lax.axis_index("sp") * rows_here, rows_here)
    query_norm = norm_rotate(query_proj, query_gain, cosine, sine_table)
    key_norm = norm_rotate(key_proj, key_gain, cosine, sine_table)
    key_heads = key_proj.shape[1] // HEAD
    groups = query_proj.shape[1] // key_proj.shape[1]
    query_grid = query_norm.reshape(rows_here, key_heads, groups, HEAD)
    local_doc = document_ids + 1
    start_carry = (
        jnp.full((key_heads, groups, rows_here), masked_low, jnp.float32),
        jnp.zeros((key_heads, groups, rows_here), jnp.float32),
        jnp.zeros((key_heads, groups, rows_here, HEAD), jnp.float32),
    )
    key_list = [key_norm]
    value_list = [value_proj]
    doc_list = [local_doc]
    for distance in range(1, REACH + 1):
        for direction in (1, -1):
            moved = from_behind((key_norm, value_proj, local_doc), "sp", direction * distance)
            key_list.append(moved[0])
            value_list.append(moved[1])
            doc_list.append(moved[2])
    key_part = jnp.concatenate(key_list, axis=0)
    value_part = jnp.concatenate(value_list, axis=0)
    doc_part = jnp.concatenate(doc_list, axis=0)
    part_rows = key_part.shape[0]

    def one_block(turn_index, inner):
        running_max, denominator, weighted = inner
        first_row = turn_index * rows_here
        key_block = lax.dynamic_slice_in_dim(key_part, first_row, rows_here, 0).reshape(
            rows_here, key_heads, HEAD
        )
        value_block = lax.dynamic_slice_in_dim(value_part, first_row, rows_here, 0).reshape(
            rows_here, key_heads, HEAD
        )
        doc_block = lax.dynamic_slice_in_dim(doc_part, first_row, rows_here, 0)
        scores = jnp.einsum(
            "qhgd,khd->hgqk", query_grid, key_block, preferred_element_type=jnp.float32
        ) * HEAD ** (-0.5)
        same_doc = (local_doc[:, None] == doc_block[None, :])[None, None]
        scores = jnp.where(same_doc, scores, masked_low)
        new_max = jnp.maximum(running_max, jnp.max(scores, axis=-1))
        weights = jnp.where(same_doc, jnp.exp(scores - new_max[..., None]), 0.0)
        rescale = jnp.exp(running_max - new_max)
        denominator = denominator * rescale + jnp.sum(weights, axis=-1)
        weighted = weighted * rescale[..., None] + jnp.einsum(
            "hgqk,khd->hgqd",
            weights.astype(jnp.bfloat16),
            value_block,
            preferred_element_type=jnp.float32,
        )
        return (new_max, denominator, weighted)

    final_carry = lax.fori_loop(0, part_rows // rows_here, one_block, start_carry)
    attn = jnp.transpose(final_carry[2] / final_carry[1][..., None], (2, 0, 1, 3))
    attn = attn.reshape(rows_here, key_heads * groups * HEAD).astype(jnp.bfloat16)
    token_rows = residual.shape[0]
    all_heads = lax.all_to_all(attn, "tp", split_axis=0, concat_axis=1, tiled=True)
    projected = jnp.dot(all_heads, output_weight, preferred_element_type=jnp.float32)
    hidden = (residual.astype(jnp.float32) + projected).astype(jnp.bfloat16)
    hidden_wide = hidden.astype(jnp.float32)
    normed = (
        hidden_wide
        * lax.rsqrt(jnp.mean(hidden_wide * hidden_wide, axis=-1, keepdims=True) + norm_eps)
        * norm_gain
    ).astype(jnp.bfloat16)
    top_count = expert_ids.shape[1]
    experts_all = lax.axis_size("sp") * lax.axis_size("tp")
    capacity = max(2, 2 * token_rows * top_count // experts_all)
    flat_ids = expert_ids.reshape(-1)
    onehot = (flat_ids[:, None] == jnp.arange(experts_all, dtype=jnp.int32)[None, :]).astype(
        jnp.int32
    )
    arrival = jnp.sum(jnp.cumsum(onehot, axis=0) * onehot, axis=1) - 1
    slot_index = flat_ids * capacity + arrival
    slot_grid = slot_index.reshape(token_rows, top_count)
    placing = jnp.sum(
        (
            jnp.arange(experts_all * capacity, dtype=jnp.int32)[:, None, None] == slot_grid[None]
        ).astype(jnp.float32),
        axis=2,
    ).astype(jnp.bfloat16)
    outgoing = jnp.dot(placing, normed, preferred_element_type=jnp.float32).astype(jnp.bfloat16)
    outgoing = outgoing.reshape(experts_all, capacity, normed.shape[1])
    arrived = lax.all_to_all(outgoing, ("sp", "tp"), split_axis=0, concat_axis=0, tiled=True)
    sources, slots, width = arrived.shape
    flat_rows = arrived.reshape(sources * slots, width)
    gate_part = jnp.dot(flat_rows, gate_weight[0], preferred_element_type=jnp.float32)
    up_part = jnp.dot(flat_rows, up_weight[0], preferred_element_type=jnp.float32)
    activity = (jax.nn.silu(gate_part) * up_part).astype(jnp.bfloat16)
    expert_out = jnp.dot(activity, down_weight[0], preferred_element_type=jnp.float32).astype(
        jnp.bfloat16
    )
    returned = lax.all_to_all(
        expert_out.reshape(sources, slots, width),
        ("sp", "tp"),
        split_axis=0,
        concat_axis=0,
        tiled=True,
    )
    fetched = returned.reshape(experts_all * capacity, -1)[slot_index]
    fetched = fetched.reshape(token_rows, top_count, -1).astype(jnp.float32)
    combined = jnp.sum(fetched * route_weights[..., None], axis=1)
    return (hidden_wide + combined).astype(jnp.bfloat16)


def solution(mesh):
    in_specs = (
        P(("sp", "tp"), None),
        P("sp", "tp"),
        P("sp", "tp"),
        P("sp", "tp"),
        P(),
        P(),
        P("sp"),
        P(),
        P(),
        P(("sp", "tp"), None),
        P(("sp", "tp"), None),
        P(("sp", "tp"), None, None),
        P(("sp", "tp"), None, None),
        P(("sp", "tp"), None, None),
    )
    out_specs = P(("sp", "tp"), None)
    return jax.shard_map(
        on_device, mesh=mesh, in_specs=in_specs, out_specs=out_specs, check_vma=False
    )
```

profile of v0, /device:TPU:1, one launch (start us, length us, event | category | flops | bytes accessed | tf_op | source)
XLA Modules:
  0.0 311.9 jit_solution(11646445521298524354)
XLA Ops:
  0.1 1.2 copy.46
  2.6 4.6 %collective-permute-start.6 = (bf16[512,128]{0,1:T(8,128)(2,1)S(1)}, bf16[512,128]{0,1:T(8,128)(2,1)}, u32[]{:S(2)}, u32[]{:S(2)}) collective-permute-start(bf16[512,128]{0,1:T(8,128)(2,1)S(1)} %maximum_bitcast_fusion), channel_id=1, source_target_pairs={{0,4},{4,8},{8,12},{12,16},{16,20},{20,24},{24,28},{28,32},{32,36}... | collective-permute-start | bytes 393224 | tf_op jit(solution)/shard_map/ppermute | solution.py:19
  7.2 1.9 collective-permute-start.7
  9.2 3.9 %collective-permute-start.8 = (bf16[512,128]{0,1:T(8,128)(2,1)S(1)}, bf16[512,128]{0,1:T(8,128)(2,1)}, u32[]{:S(2)}, u32[]{:S(2)}) collective-permute-start(bf16[512,128]{0,1:T(8,128)(2,1)S(1)} %maximum_bitcast_fusion), channel_id=1, source_target_pairs={{0,8},{4,12},{8,16},{12,20},{16,24},{20,28},{24,32},{28,36},{32,40... | collective-permute-start | bytes 393224 | tf_op jit(solution)/shard_map/ppermute | solution.py:19
  13.0 1.3 collective-permute-start.9
  15.0 5.0 %collective-permute-start = (s32[512]{0:T(512)S(1)}, s32[512]{0:T(512)S(1)}, u32[]{:S(2)}, u32[]{:S(2)}) collective-permute-start(s32[512]{0:T(512)S(1)} %get-tuple-element.328), channel_id=1, source_target_pairs={{0,4},{4,8},{8,12},{12,16},{16,20},{20,24},{24,28},{28,32},{32,36}... | collective-permute-start | bytes 6152 | tf_op jit(solution)/shard_map/ppermute | solution.py:19
  24.2 1.9 collective-permute-start.1
  26.1 3.0 collective-permute-done.1
  29.1 2.6 collective-permute-start.2
  32.4 1.3 collective-permute-start.3
  33.7 4.4 %collective-permute-done.3 = s32[512]{0:T(512)S(1)} collective-permute-done((s32[512]{0:T(512)S(1)}, s32[512]{0:T(512)S(1)}, u32[]{:S(2)}, u32[]{:S(2)}) %collective-permute-start.3) | collective-permute-done | bytes 2080 | tf_op jit(solution)/shard_map/ppermute | solution.py:19
  38.1 9.8 %collective-permute-start.4 = (s32[512]{0:T(512)S(1)}, s32[512]{0:T(512)S(1)}, u32[]{:S(2)}, u32[]{:S(2)}) collective-permute-start(s32[512]{0:T(512)S(1)} %get-tuple-element.328), channel_id=1, source_target_pairs={{0,12},{4,16},{8,20},{12,24},{16,28},{20,32},{24,36},{28,40},{32,4... | collective-permute-start | bytes 6152 | tf_op jit(solution)/shard_map/ppermute | solution.py:19
  48.6 1.3 collective-permute-start.5
  49.9 6.2 %collective-permute-done.5 = s32[512]{0:T(512)S(1)} collective-permute-done((s32[512]{0:T(512)S(1)}, s32[512]{0:T(512)S(1)}, u32[]{:S(2)}, u32[]{:S(2)}) %collective-permute-start.5) | collective-permute-done | bytes 2080 | tf_op jit(solution)/shard_map/ppermute | solution.py:19
  56.1 3.6 %collective-permute-start.10 = (bf16[512,128]{0,1:T(8,128)(2,1)S(1)}, bf16[512,128]{0,1:T(8,128)(2,1)S(1)}, u32[]{:S(2)}, u32[]{:S(2)}) collective-permute-start(bf16[512,128]{0,1:T(8,128)(2,1)S(1)} %maximum_bitcast_fusion), channel_id=1, source_target_pairs={{0,12},{4,16},{8,20},{12,24},{16,28},{20,32},{24,36},{28,40},{32,4... | collective-permute-start | bytes 393224 | tf_op jit(solution)/shard_map/ppermute | solution.py:19
  59.8 1.3 collective-permute-start.11
  61.1 1.6 constant_dynamic-update-slice_fusion.6
  62.6 5.4 %collective-permute-start.12 = (bf16[512,128]{1,0:T(8,128)(2,1)S(1)}, bf16[512,128]{1,0:T(8,128)(2,1)S(1)}, u32[]{:S(2)}, u32[]{:S(2)}) collective-permute-start(bf16[512,128]{1,0:T(8,128)(2,1)S(1)} %copy-done.3), channel_id=1, source_target_pairs={{0,4},{4,8},{8,12},{12,16},{16,20},{20,24},{24,28},{28,32},{32,36}... | collective-permute-start | bytes 393224 | tf_op jit(solution)/shard_map/ppermute | solution.py:19
  68.0 1.6 constant_dynamic-update-slice_fusion.5
  69.6 1.9 collective-permute-start.13
  71.5 1.6 constant_dynamic-update-slice_fusion.4
  73.1 4.6 %collective-permute-start.14 = (bf16[512,128]{1,0:T(8,128)(2,1)S(1)}, bf16[512,128]{1,0:T(8,128)(2,1)S(1)}, u32[]{:S(2)}, u32[]{:S(2)}) collective-permute-start(bf16[512,128]{1,0:T(8,128)(2,1)S(1)} %copy-done.3), channel_id=1, source_target_pairs={{0,8},{4,12},{8,16},{12,20},{16,24},{20,28},{24,32},{28,36},{32,40... | collective-permute-start | bytes 393224 | tf_op jit(solution)/shard_map/ppermute | solution.py:19
  77.7 1.6 constant_dynamic-update-slice_fusion.3
  79.3 1.3 collective-permute-start.15
  81.3 7.9 %collective-permute-start.16 = (bf16[512,128]{1,0:T(8,128)(2,1)S(1)}, bf16[512,128]{1,0:T(8,128)(2,1)S(1)}, u32[]{:S(2)}, u32[]{:S(2)}) collective-permute-start(bf16[512,128]{1,0:T(8,128)(2,1)S(1)} %copy-done.3), channel_id=1, source_target_pairs={{0,12},{4,16},{8,20},{12,24},{16,28},{20,32},{24,36},{28,40},{32,4... | collective-permute-start | bytes 393224 | tf_op jit(solution)/shard_map/ppermute | solution.py:19
  89.9 1.3 collective-permute-start.17
  94.5 4.2 %collective-permute-done.17 = bf16[512,128]{1,0:T(8,128)(2,1)S(1)} collective-permute-done((bf16[512,128]{1,0:T(8,128)(2,1)S(1)}, bf16[512,128]{1,0:T(8,128)(2,1)S(1)}, u32[]{:S(2)}, u32[]{:S(2)}) %collective-permute-start.17) | collective-permute-done | bytes 131104 | tf_op jit(solution)/shard_map/ppermute | solution.py:19
  99.4 71.8 %while.18 = (s32[]{:T(128)}, f32[1,4,512]{2,1,0:T(4,128)S(1)}, f32[1,4,512]{2,1,0:T(4,128)S(1)}, f32[1,4,512,128]{3,2,1,0:T(8,128)}, s32[512]{0:T(512)S(1)}, /*i...) while((s32[]{:T(128)}, f32[1,4,512]{2,1,0:T(4,128)S(1)}, ...), condition=%wide.region_5.6_spmd.clone, body=%wide.region_2.5_spmd.clone.sunk | while | flops 551563264 | bytes 33431772 | solution.py:127
  99.7 3.8 %fusion.82 = (f32[4,512]{1,0:T(4,128)S(1)}, f32[512,512,4]{1,0,2:T(8,128)}) fusion(pred[512,512]{0,1:T(8,128)(4,1)S(1)} %broadcast_compare_fusion.2, bf16[512,1,4,128]{3,0,2,1:T(8,128)(2,1)S(1)} %get-tuple-element.357, bf16[3584,128]{0,1:T(8,128)(2,1)} %get-tuple-element.356, s32[]{:T(128)S(6)} %select_n.106), kind=kOutput, calls=%fused_computation.3.clone.1 | convolution fusion | flops 271579136 | bytes 5120004 | tf_op jit(solution)/shard_map/while/body/eval_jaxpr/qhgd,khd->hgqk/dot_general | solution.py:110
  103.5 4.8 %fusion.85 = f32[1,4,512,128]{3,2,1,0:T(8,128)} fusion(f32[512,512,4]{1,0,2:T(8,128)} %get-tuple-element.322, f32[4,512]{1,0:T(4,128)S(1)} %bitcast.133, pred[512,512]{0,1:T(8,128)(4,1)S(1)} %broadcast_compare_fusion.2, f32[1,4,512,128]{3,2,1,0:T(8,128)} %get-tuple-element.340, f32[4,512]{1,0:T(4,128)S(1)} %get-tuple-element.323, pred[]{:T(512)S(6)} %compare.14, ...), kind=kOutput, calls=%fused_computation.10.clone.1 | convolution fusion | flops 274464768 | bytes 6701061 | tf_op jit(solution)/shard_map/while/body/eval_jaxpr/hgqk,khd->hgqd/dot_general | solution.py:119
  108.3 1.0 fusion.84
  109.7 3.8 %fusion.82 = (f32[4,512]{1,0:T(4,128)S(1)}, f32[512,512,4]{1,0,2:T(8,128)}) fusion(pred[512,512]{0,1:T(8,128)(4,1)S(1)} %broadcast_compare_fusion.2, bf16[512,1,4,128]{3,0,2,1:T(8,128)(2,1)S(1)} %get-tuple-element.357, bf16[3584,128]{0,1:T(8,128)(2,1)} %get-tuple-element.356, s32[]{:T(128)S(6)} %select_n.106), kind=kOutput, calls=%fused_computation.3.clone.1 | convolution fusion | flops 271579136 | bytes 5120004 | tf_op jit(solution)/shard_map/while/body/eval_jaxpr/qhgd,khd->hgqk/dot_general | solution.py:110
  113.5 5.1 %fusion.85 = f32[1,4,512,128]{3,2,1,0:T(8,128)} fusion(f32[512,512,4]{1,0,2:T(8,128)} %get-tuple-element.322, f32[4,512]{1,0:T(4,128)S(1)} %bitcast.133, pred[512,512]{0,1:T(8,128)(4,1)S(1)} %broadcast_compare_fusion.2, f32[1,4,512,128]{3,2,1,0:T(8,128)} %get-tuple-element.340, f32[4,512]{1,0:T(4,128)S(1)} %get-tuple-element.323, pred[]{:T(512)S(6)} %compare.14, ...), kind=kOutput, calls=%fused_computation.10.clone.1 | convolution fusion | flops 274464768 | bytes 6701061 | tf_op jit(solution)/shard_map/while/body/eval_jaxpr/hgqk,khd->hgqd/dot_general | solution.py:119
  118.6 1.0 fusion.84
  120.0 3.8 %fusion.82 = (f32[4,512]{1,0:T(4,128)S(1)}, f32[512,512,4]{1,0,2:T(8,128)}) fusion(pred[512,512]{0,1:T(8,128)(4,1)S(1)} %broadcast_compare_fusion.2, bf16[512,1,4,128]{3,0,2,1:T(8,128)(2,1)S(1)} %get-tuple-element.357, bf16[3584,128]{0,1:T(8,128)(2,1)} %get-tuple-element.356, s32[]{:T(128)S(6)} %select_n.106), kind=kOutput, calls=%fused_computation.3.clone.1 | convolution fusion | flops 271579136 | bytes 5120004 | tf_op jit(solution)/shard_map/while/body/eval_jaxpr/qhgd,khd->hgqk/dot_general | solution.py:110
  123.8 5.1 %fusion.85 = f32[1,4,512,128]{3,2,1,0:T(8,128)} fusion(f32[512,512,4]{1,0,2:T(8,128)} %get-tuple-element.322, f32[4,512]{1,0:T(4,128)S(1)} %bitcast.133, pred[512,512]{0,1:T(8,128)(4,1)S(1)} %broadcast_compare_fusion.2, f32[1,4,512,128]{3,2,1,0:T(8,128)} %get-tuple-element.340, f32[4,512]{1,0:T(4,128)S(1)} %get-tuple-element.323, pred[]{:T(512)S(6)} %compare.14, ...), kind=kOutput, calls=%fused_computation.10.clone.1 | convolution fusion | flops 274464768 | bytes 6701061 | tf_op jit(solution)/shard_map/while/body/eval_jaxpr/hgqk,khd->hgqd/dot_general | solution.py:119
  128.9 1.0 fusion.84
  130.3 3.8 %fusion.82 = (f32[4,512]{1,0:T(4,128)S(1)}, f32[512,512,4]{1,0,2:T(8,128)}) fusion(pred[512,512]{0,1:T(8,128)(4,1)S(1)} %broadcast_compare_fusion.2, bf16[512,1,4,128]{3,0,2,1:T(8,128)(2,1)S(1)} %get-tuple-element.357, bf16[3584,128]{0,1:T(8,128)(2,1)} %get-tuple-element.356, s32[]{:T(128)S(6)} %select_n.106), kind=kOutput, calls=%fused_computation.3.clone.1 | convolution fusion | flops 271579136 | bytes 5120004 | tf_op jit(solution)/shard_map/while/body/eval_jaxpr/qhgd,khd->hgqk/dot_general | solution.py:110
  134.1 5.1 %fusion.85 = f32[1,4,512,128]{3,2,1,0:T(8,128)} fusion(f32[512,512,4]{1,0,2:T(8,128)} %get-tuple-element.322, f32[4,512]{1,0:T(4,128)S(1)} %bitcast.133, pred[512,512]{0,1:T(8,128)(4,1)S(1)} %broadcast_compare_fusion.2, f32[1,4,512,128]{3,2,1,0:T(8,128)} %get-tuple-element.340, f32[4,512]{1,0:T(4,128)S(1)} %get-tuple-element.323, pred[]{:T(512)S(6)} %compare.14, ...), kind=kOutput, calls=%fused_computation.10.clone.1 | convolution fusion | flops 274464768 | bytes 6701061 | tf_op jit(solution)/shard_map/while/body/eval_jaxpr/hgqk,khd->hgqd/dot_general | solution.py:119
  139.2 1.0 fusion.84
  140.6 3.8 %fusion.82 = (f32[4,512]{1,0:T(4,128)S(1)}, f32[512,512,4]{1,0,2:T(8,128)}) fusion(pred[512,512]{0,1:T(8,128)(4,1)S(1)} %broadcast_compare_fusion.2, bf16[512,1,4,128]{3,0,2,1:T(8,128)(2,1)S(1)} %get-tuple-element.357, bf16[3584,128]{0,1:T(8,128)(2,1)} %get-tuple-element.356, s32[]{:T(128)S(6)} %select_n.106), kind=kOutput, calls=%fused_computation.3.clone.1 | convolution fusion | flops 271579136 | bytes 5120004 | tf_op jit(solution)/shard_map/while/body/eval_jaxpr/qhgd,khd->hgqk/dot_general | solution.py:110
  144.4 5.1 %fusion.85 = f32[1,4,512,128]{3,2,1,0:T(8,128)} fusion(f32[512,512,4]{1,0,2:T(8,128)} %get-tuple-element.322, f32[4,512]{1,0:T(4,128)S(1)} %bitcast.133, pred[512,512]{0,1:T(8,128)(4,1)S(1)} %broadcast_compare_fusion.2, f32[1,4,512,128]{3,2,1,0:T(8,128)} %get-tuple-element.340, f32[4,512]{1,0:T(4,128)S(1)} %get-tuple-element.323, pred[]{:T(512)S(6)} %compare.14, ...), kind=kOutput, calls=%fused_computation.10.clone.1 | convolution fusion | flops 274464768 | bytes 6701061 | tf_op jit(solution)/shard_map/while/body/eval_jaxpr/hgqk,khd->hgqd/dot_general | solution.py:119
  149.5 1.0 fusion.84
  150.9 3.8 %fusion.82 = (f32[4,512]{1,0:T(4,128)S(1)}, f32[512,512,4]{1,0,2:T(8,128)}) fusion(pred[512,512]{0,1:T(8,128)(4,1)S(1)} %broadcast_compare_fusion.2, bf16[512,1,4,128]{3,0,2,1:T(8,128)(2,1)S(1)} %get-tuple-element.357, bf16[3584,128]{0,1:T(8,128)(2,1)} %get-tuple-element.356, s32[]{:T(128)S(6)} %select_n.106), kind=kOutput, calls=%fused_computation.3.clone.1 | convolution fusion | flops 271579136 | bytes 5120004 | tf_op jit(solution)/shard_map/while/body/eval_jaxpr/qhgd,khd->hgqk/dot_general | solution.py:110
  154.7 5.1 %fusion.85 = f32[1,4,512,128]{3,2,1,0:T(8,128)} fusion(f32[512,512,4]{1,0,2:T(8,128)} %get-tuple-element.322, f32[4,512]{1,0:T(4,128)S(1)} %bitcast.133, pred[512,512]{0,1:T(8,128)(4,1)S(1)} %broadcast_compare_fusion.2, f32[1,4,512,128]{3,2,1,0:T(8,128)} %get-tuple-element.340, f32[4,512]{1,0:T(4,128)S(1)} %get-tuple-element.323, pred[]{:T(512)S(6)} %compare.14, ...), kind=kOutput, calls=%fused_computation.10.clone.1 | convolution fusion | flops 274464768 | bytes 6701061 | tf_op jit(solution)/shard_map/while/body/eval_jaxpr/hgqk,khd->hgqd/dot_general | solution.py:119
  161.2 3.8 %fusion.82 = (f32[4,512]{1,0:T(4,128)S(1)}, f32[512,512,4]{1,0,2:T(8,128)}) fusion(pred[512,512]{0,1:T(8,128)(4,1)S(1)} %broadcast_compare_fusion.2, bf16[512,1,4,128]{3,0,2,1:T(8,128)(2,1)S(1)} %get-tuple-element.357, bf16[3584,128]{0,1:T(8,128)(2,1)} %get-tuple-element.356, s32[]{:T(128)S(6)} %select_n.106), kind=kOutput, calls=%fused_computation.3.clone.1 | convolution fusion | flops 271579136 | bytes 5120004 | tf_op jit(solution)/shard_map/while/body/eval_jaxpr/qhgd,khd->hgqk/dot_general | solution.py:110
  165.0 5.1 %fusion.85 = f32[1,4,512,128]{3,2,1,0:T(8,128)} fusion(f32[512,512,4]{1,0,2:T(8,128)} %get-tuple-element.322, f32[4,512]{1,0:T(4,128)S(1)} %bitcast.133, pred[512,512]{0,1:T(8,128)(4,1)S(1)} %broadcast_compare_fusion.2, f32[1,4,512,128]{3,2,1,0:T(8,128)} %get-tuple-element.340, f32[4,512]{1,0:T(4,128)S(1)} %get-tuple-element.323, pred[]{:T(512)S(6)} %compare.14, ...), kind=kOutput, calls=%fused_computation.10.clone.1 | convolution fusion | flops 274464768 | bytes 6701061 | tf_op jit(solution)/shard_map/while/body/eval_jaxpr/hgqk,khd->hgqd/dot_general | solution.py:119
  171.2 1.6 fusion.45
  174.2 4.0 %all-to-all-start = ((bf16[4,128,512]{2,1,0:T(8,128)(2,1)}), bf16[4,128,512]{2,1,0:T(8,128)(2,1)S(1)}, u32[]{:S(2)}, u32[]{:S(2)}) async-start(bf16[4,128,512]{2,1,0:T(8,128)(2,1)} %convert_element_type.95), calls=%async_computation | async-start | bytes 1048576 | tf_op jit(solution)/shard_map/all_to_all | solution.py:131
  178.5 9.2 %all-to-all-done = bf16[4,128,512]{2,1,0:T(8,128)(2,1)S(1)} async-done(((bf16[4,128,512]{2,1,0:T(8,128)(2,1)}), bf16[4,128,512]{2,1,0:T(8,128)(2,1)S(1)}, u32[]{:S(2)}, u32[]{:S(2)}) %all-to-all-start) | async-done | bytes 524320 | tf_op jit(solution)/shard_map/all_to_all | solution.py:131
  188.8 4.9 %multiply_reduce_fusion.1 = (f32[128]{0:T(128)S(1)}, f32[128,2048]{1,0:T(8,128)S(1)}) fusion(bf16[128,2048]{0,1:T(8,128)(2,1)} %bitcast.132, bf16[2048,2048]{1,0:T(8,128)(2,1)} %param.23, bf16[128,2048]{1,0:T(8,128)(2,1)} %param.16), kind=kOutput, calls=%fused_computation.48 | convolution fusion | flops 1075314560 | bytes 10486272 | tf_op jit(solution)/shard_map/dot_general | solution.py:132
  193.7 2.1 convolution_convert_fusion
  195.8 4.1 %reshape.413 = bf16[128,4,2048]{2,1,0:T(4,128)(2,1)} reshape(bf16[512,2048]{1,0:T(8,128)(2,1)} %convolution_convert_fusion) | data formatting | bytes 4194304 | tf_op jit(solution)/shard_map/reshape | solution.py:157
  199.9 39.5 %all_to_all.26 = bf16[128,4,2048]{2,1,0:T(4,128)(2,1)} all-to-all(bf16[128,4,2048]{2,1,0:T(4,128)(2,1)} %reshape.413), channel_id=1, replica_groups=mesh['sp'=32,'tp'=4] {'sp','tp'}, dimensions={0} | all-to-all | bytes 4194304 | tf_op jit(solution)/shard_map/all_to_all | solution.py:158
  239.4 3.9 %reshape.414 = bf16[512,2048]{1,0:T(8,128)(2,1)} reshape(bf16[128,4,2048]{2,1,0:T(4,128)(2,1)} %all_to_all.26) | data formatting | bytes 4194304 | tf_op jit(solution)/shard_map/reshape | solution.py:160
  243.3 4.4 %fusion.30 = f32[512,512]{1,0:T(8,128)} fusion(bf16[512,2048]{1,0:T(8,128)(2,1)} %reshape.414, bf16[1,2048,512]{2,1,0:T(8,128)(2,1)} %param.27), kind=kOutput, calls=%fused_computation.37 | convolution fusion | flops 1073741824 | bytes 5242880 | tf_op jit(solution)/shard_map/dot_general | solution.py:161
  247.8 6.2 %convolution_convert_fusion.1 = bf16[512,2048]{1,0:T(8,128)(2,1)} fusion(bf16[1,512,2048]{2,1,0:T(8,128)(2,1)S(1)} %copy-done, bf16[512,2048]{1,0:T(8,128)(2,1)} %reshape.414, bf16[1,2048,512]{2,1,0:T(8,128)(2,1)} %param.28, f32[512,512]{1,0:T(8,128)} %fusion.30), kind=kOutput, calls=%fused_computation.30 | convolution fusion | flops 2150105088 | bytes 9437184 | tf_op jit(solution)/shard_map/dot_general | solution.py:164
  254.0 4.1 %reshape.415 = bf16[128,4,2048]{2,1,0:T(4,128)(2,1)} reshape(bf16[512,2048]{1,0:T(8,128)(2,1)} %convolution_convert_fusion.1) | data formatting | bytes 4194304 | tf_op jit(solution)/shard_map/reshape | solution.py:168
  258.1 5.0 %all-to-all-start.2 = ((bf16[128,4,2048]{2,1,0:T(4,128)(2,1)}), bf16[128,4,2048]{2,1,0:T(4,128)(2,1)}, u32[]{:S(2)}, u32[]{:S(2)}) async-start(bf16[128,4,2048]{2,1,0:T(4,128)(2,1)} %reshape.415), calls=%async_computation.2 | async-start | bytes 4194304 | tf_op jit(solution)/shard_map/all_to_all | solution.py:167
  263.4 30.3 %all-to-all-done.2 = bf16[128,4,2048]{2,1,0:T(4,128)(2,1)} async-done(((bf16[128,4,2048]{2,1,0:T(4,128)(2,1)}), bf16[128,4,2048]{2,1,0:T(4,128)(2,1)}, u32[]{:S(2)}, u32[]{:S(2)}) %all-to-all-start.2) | async-done | bytes 2097184 | tf_op jit(solution)/shard_map/all_to_all | solution.py:167
  293.6 3.9 %reshape.416 = bf16[512,2048]{1,0:T(8,128)(2,1)} reshape(bf16[128,4,2048]{2,1,0:T(4,128)(2,1)} %all-to-all-done.2) | data formatting | bytes 4194304 | tf_op jit(solution)/shard_map/reshape | solution.py:174
  297.6 5.2 %gather_fusion = bf16[256,2048]{1,0:T(8,128)(2,1)} fusion(bf16[512,2048]{1,0:T(8,128)(2,1)} %reshape.416, s32[1024]{0:T(1024)S(1)} %pad_clamp_fusion), kind=kCustom, calls=%fused_computation | custom fusion | bytes 2098176 | tf_op jit(solution)/shard_map/gather | solution.py:174
  302.8 3.4 %reshape.419 = f32[128,2,2048]{2,1,0:T(2,128)} reshape(bf16[256,2048]{1,0:T(8,128)(2,1)} %gather_fusion) | data formatting | bytes 3145728 | tf_op jit(solution)/shard_map/convert_element_type | solution.py:175
  306.1 4.8 %multiply_reduce_fusion = f32[128,2048]{1,0:T(8,128)S(1)} fusion(f32[128,2,2048]{2,1,0:T(2,128)} %reshape.419, f32[128,2]{1,0:T(8,128)S(1)} %copy.58), kind=kLoop, calls=%fused_computation.39 | loop fusion | flops 786432 | bytes 3146752 | tf_op jit(solution)/shard_map/reduce_sum | solution.py:176
  (142 shorter events, 21.4 us)
Async XLA Ops:
  0.0 247.8 %copy-start = (bf16[1,512,2048]{2,1,0:T(8,128)(2,1)S(1)}, bf16[1,512,2048]{2,1,0:T(8,128)(2,1)}, u32[]{:S(2)}) copy-start(bf16[1,512,2048]{2,1,0:T(8,128)(2,1)} %param.29) | copy-start | bytes 6291460
  0.0 20.7 %copy-start.5 = (s32[128,2]{0,1:T(2,128)S(1)}, s32[128,2]{0,1:T(2,128)}, u32[]{:S(2)}) copy-start(s32[128,2]{0,1:T(2,128)} %param.25) | copy-start | bytes 3076
  0.0 21.1 %copy-start.2 = (bf16[512,512]{1,0:T(8,128)(2,1)S(1)}, bf16[512,512]{1,0:T(8,128)(2,1)}, u32[]{:S(2)}) copy-start(bf16[512,512]{1,0:T(8,128)(2,1)} %param.17) | copy-start | bytes 1572868
  2.1 20.2 %copy-start.7 = (f32[128]{0:T(128)S(1)}, f32[128]{0:T(128)}, u32[]{:S(2)}) copy-start(f32[128]{0:T(128)} %param.20) | copy-start | bytes 1540
  2.6 57.1 %collective-permute-start.6 = (bf16[512,128]{0,1:T(8,128)(2,1)S(1)}, bf16[512,128]{0,1:T(8,128)(2,1)}, u32[]{:S(2)}, u32[]{:S(2)}) collective-permute-start(bf16[512,128]{0,1:T(8,128)(2,1)S(1)} %maximum_bitcast_fusion), channel_id=1, source_target_pairs={{0,4},{4,8},{8,12},{12,16},{16,20},{20,24},{24,28},{28,32},{32,36}... | collective-permute-start | bytes 393224 | tf_op jit(solution)/shard_map/ppermute | solution.py:19
  7.2 55.4 %collective-permute-start.7 = (bf16[512,128]{0,1:T(8,128)(2,1)S(1)}, bf16[512,128]{0,1:T(8,128)(2,1)}, u32[]{:S(2)}, u32[]{:S(2)}) collective-permute-start(bf16[512,128]{0,1:T(8,128)(2,1)S(1)} %maximum_bitcast_fusion), channel_id=1, source_target_pairs={{4,0},{8,4},{12,8},{16,12},{20,16},{24,20},{28,24},{32,28},{36,32}... | collective-permute-start | bytes 393224 | tf_op jit(solution)/shard_map/ppermute | solution.py:19
  9.2 60.5 %collective-permute-start.8 = (bf16[512,128]{0,1:T(8,128)(2,1)S(1)}, bf16[512,128]{0,1:T(8,128)(2,1)}, u32[]{:S(2)}, u32[]{:S(2)}) collective-permute-start(bf16[512,128]{0,1:T(8,128)(2,1)S(1)} %maximum_bitcast_fusion), channel_id=1, source_target_pairs={{0,8},{4,12},{8,16},{12,20},{16,24},{20,28},{24,32},{28,36},{32,40... | collective-permute-start | bytes 393224 | tf_op jit(solution)/shard_map/ppermute | solution.py:19
  13.0 60.1 %collective-permute-start.9 = (bf16[512,128]{0,1:T(8,128)(2,1)S(1)}, bf16[512,128]{0,1:T(8,128)(2,1)}, u32[]{:S(2)}, u32[]{:S(2)}) collective-permute-start(bf16[512,128]{0,1:T(8,128)(2,1)S(1)} %maximum_bitcast_fusion), channel_id=1, source_target_pairs={{8,0},{12,4},{16,8},{20,12},{24,16},{28,20},{32,24},{36,28},{40,32... | collective-permute-start | bytes 393224 | tf_op jit(solution)/shard_map/ppermute | solution.py:19
  15.0 9.2 %collective-permute-start = (s32[512]{0:T(512)S(1)}, s32[512]{0:T(512)S(1)}, u32[]{:S(2)}, u32[]{:S(2)}) collective-permute-start(s32[512]{0:T(512)S(1)} %get-tuple-element.328), channel_id=1, source_target_pairs={{0,4},{4,8},{8,12},{12,16},{16,20},{20,24},{24,28},{28,32},{32,36}... | collective-permute-start | bytes 6152 | tf_op jit(solution)/shard_map/ppermute | solution.py:19
  22.3 0.9 copy-start.3
  24.2 4.9 %collective-permute-start.1 = (s32[512]{0:T(512)S(1)}, s32[512]{0:T(512)S(1)}, u32[]{:S(2)}, u32[]{:S(2)}) collective-permute-start(s32[512]{0:T(512)S(1)} %get-tuple-element.328), channel_id=1, source_target_pairs={{4,0},{8,4},{12,8},{16,12},{20,16},{24,20},{28,24},{32,28},{36,32}... | collective-permute-start | bytes 6152 | tf_op jit(solution)/shard_map/ppermute | solution.py:19
  29.1 3.3 %collective-permute-start.2 = (s32[512]{0:T(512)S(1)}, s32[512]{0:T(512)S(1)}, u32[]{:S(2)}, u32[]{:S(2)}) collective-permute-start(s32[512]{0:T(512)S(1)} %get-tuple-element.328), channel_id=1, source_target_pairs={{0,8},{4,12},{8,16},{12,20},{16,24},{20,28},{24,32},{28,36},{32,40... | collective-permute-start | bytes 6152 | tf_op jit(solution)/shard_map/ppermute | solution.py:19
  32.4 5.7 %collective-permute-start.3 = (s32[512]{0:T(512)S(1)}, s32[512]{0:T(512)S(1)}, u32[]{:S(2)}, u32[]{:S(2)}) collective-permute-start(s32[512]{0:T(512)S(1)} %get-tuple-element.328), channel_id=1, source_target_pairs={{8,0},{12,4},{16,8},{20,12},{24,16},{28,20},{32,24},{36,28},{40,32... | collective-permute-start | bytes 6152 | tf_op jit(solution)/shard_map/ppermute | solution.py:19
  38.1 10.5 %collective-permute-start.4 = (s32[512]{0:T(512)S(1)}, s32[512]{0:T(512)S(1)}, u32[]{:S(2)}, u32[]{:S(2)}) collective-permute-start(s32[512]{0:T(512)S(1)} %get-tuple-element.328), channel_id=1, source_target_pairs={{0,12},{4,16},{8,20},{12,24},{16,28},{20,32},{24,36},{28,40},{32,4... | collective-permute-start | bytes 6152 | tf_op jit(solution)/shard_map/ppermute | solution.py:19
  48.6 7.5 %collective-permute-start.5 = (s32[512]{0:T(512)S(1)}, s32[512]{0:T(512)S(1)}, u32[]{:S(2)}, u32[]{:S(2)}) collective-permute-start(s32[512]{0:T(512)S(1)} %get-tuple-element.328), channel_id=1, source_target_pairs={{12,0},{16,4},{20,8},{24,12},{28,16},{32,20},{36,24},{40,28},{44,3... | collective-permute-start | bytes 6152 | tf_op jit(solution)/shard_map/ppermute | solution.py:19
  56.1 23.2 %collective-permute-start.10 = (bf16[512,128]{0,1:T(8,128)(2,1)S(1)}, bf16[512,128]{0,1:T(8,128)(2,1)S(1)}, u32[]{:S(2)}, u32[]{:S(2)}) collective-permute-start(bf16[512,128]{0,1:T(8,128)(2,1)S(1)} %maximum_bitcast_fusion), channel_id=1, source_target_pairs={{0,12},{4,16},{8,20},{12,24},{16,28},{20,32},{24,36},{28,40},{32,4... | collective-permute-start | bytes 393224 | tf_op jit(solution)/shard_map/ppermute | solution.py:19
  59.8 21.5 %collective-permute-start.11 = (bf16[512,128]{0,1:T(8,128)(2,1)S(1)}, bf16[512,128]{0,1:T(8,128)(2,1)S(1)}, u32[]{:S(2)}, u32[]{:S(2)}) collective-permute-start(bf16[512,128]{0,1:T(8,128)(2,1)S(1)} %maximum_bitcast_fusion), channel_id=1, source_target_pairs={{12,0},{16,4},{20,8},{24,12},{28,16},{32,20},{36,24},{40,28},{44,3... | collective-permute-start | bytes 393224 | tf_op jit(solution)/shard_map/ppermute | solution.py:19
  62.6 27.2 %collective-permute-start.12 = (bf16[512,128]{1,0:T(8,128)(2,1)S(1)}, bf16[512,128]{1,0:T(8,128)(2,1)S(1)}, u32[]{:S(2)}, u32[]{:S(2)}) collective-permute-start(bf16[512,128]{1,0:T(8,128)(2,1)S(1)} %copy-done.3), channel_id=1, source_target_pairs={{0,4},{4,8},{8,12},{12,16},{16,20},{20,24},{24,28},{28,32},{32,36}... | collective-permute-start | bytes 393224 | tf_op jit(solution)/shard_map/ppermute | solution.py:19
  69.6 22.2 %collective-permute-start.13 = (bf16[512,128]{1,0:T(8,128)(2,1)S(1)}, bf16[512,128]{1,0:T(8,128)(2,1)S(1)}, u32[]{:S(2)}, u32[]{:S(2)}) collective-permute-start(bf16[512,128]{1,0:T(8,128)(2,1)S(1)} %copy-done.3), channel_id=1, source_target_pairs={{4,0},{8,4},{12,8},{16,12},{20,16},{24,20},{28,24},{32,28},{36,32}... | collective-permute-start | bytes 393224 | tf_op jit(solution)/shard_map/ppermute | solution.py:19
  73.1 19.4 %collective-permute-start.14 = (bf16[512,128]{1,0:T(8,128)(2,1)S(1)}, bf16[512,128]{1,0:T(8,128)(2,1)S(1)}, u32[]{:S(2)}, u32[]{:S(2)}) collective-permute-start(bf16[512,128]{1,0:T(8,128)(2,1)S(1)} %copy-done.3), channel_id=1, source_target_pairs={{0,8},{4,12},{8,16},{12,20},{16,24},{20,28},{24,32},{28,36},{32,40... | collective-permute-start | bytes 393224 | tf_op jit(solution)/shard_map/ppermute | solution.py:19
  79.3 13.9 %collective-permute-start.15 = (bf16[512,128]{1,0:T(8,128)(2,1)S(1)}, bf16[512,128]{1,0:T(8,128)(2,1)S(1)}, u32[]{:S(2)}, u32[]{:S(2)}) collective-permute-start(bf16[512,128]{1,0:T(8,128)(2,1)S(1)} %copy-done.3), channel_id=1, source_target_pairs={{8,0},{12,4},{16,8},{20,12},{24,16},{28,20},{32,24},{36,28},{40,32... | collective-permute-start | bytes 393224 | tf_op jit(solution)/shard_map/ppermute | solution.py:19
  81.3 12.5 %collective-permute-start.16 = (bf16[512,128]{1,0:T(8,128)(2,1)S(1)}, bf16[512,128]{1,0:T(8,128)(2,1)S(1)}, u32[]{:S(2)}, u32[]{:S(2)}) collective-permute-start(bf16[512,128]{1,0:T(8,128)(2,1)S(1)} %copy-done.3), channel_id=1, source_target_pairs={{0,12},{4,16},{8,20},{12,24},{16,28},{20,32},{24,36},{28,40},{32,4... | collective-permute-start | bytes 393224 | tf_op jit(solution)/shard_map/ppermute | solution.py:19
  89.9 8.8 %collective-permute-start.17 = (bf16[512,128]{1,0:T(8,128)(2,1)S(1)}, bf16[512,128]{1,0:T(8,128)(2,1)S(1)}, u32[]{:S(2)}, u32[]{:S(2)}) collective-permute-start(bf16[512,128]{1,0:T(8,128)(2,1)S(1)} %copy-done.3), channel_id=1, source_target_pairs={{12,0},{16,4},{20,8},{24,12},{28,16},{32,20},{36,24},{40,28},{44,3... | collective-permute-start | bytes 393224 | tf_op jit(solution)/shard_map/ppermute | solution.py:19
  103.5 4.8 %copy-start.1 = (f32[512,512,4]{1,0,2:T(8,128)S(1)}, f32[512,512,4]{1,0,2:T(8,128)}, u32[]{:S(2)}) copy-start(f32[512,512,4]{1,0,2:T(8,128)} %get-tuple-element.322) | copy-start | bytes 12582916 | tf_op jit(solution)/shard_map/while
  113.4 5.1 %copy-start.1 = (f32[512,512,4]{1,0,2:T(8,128)S(1)}, f32[512,512,4]{1,0,2:T(8,128)}, u32[]{:S(2)}) copy-start(f32[512,512,4]{1,0,2:T(8,128)} %get-tuple-element.322) | copy-start | bytes 12582916 | tf_op jit(solution)/shard_map/while
  123.8 5.1 %copy-start.1 = (f32[512,512,4]{1,0,2:T(8,128)S(1)}, f32[512,512,4]{1,0,2:T(8,128)}, u32[]{:S(2)}) copy-start(f32[512,512,4]{1,0,2:T(8,128)} %get-tuple-element.322) | copy-start | bytes 12582916 | tf_op jit(solution)/shard_map/while
  134.1 5.1 %copy-start.1 = (f32[512,512,4]{1,0,2:T(8,128)S(1)}, f32[512,512,4]{1,0,2:T(8,128)}, u32[]{:S(2)}) copy-start(f32[512,512,4]{1,0,2:T(8,128)} %get-tuple-element.322) | copy-start | bytes 12582916 | tf_op jit(solution)/shard_map/while
  144.4 5.1 %copy-start.1 = (f32[512,512,4]{1,0,2:T(8,128)S(1)}, f32[512,512,4]{1,0,2:T(8,128)}, u32[]{:S(2)}) copy-start(f32[512,512,4]{1,0,2:T(8,128)} %get-tuple-element.322) | copy-start | bytes 12582916 | tf_op jit(solution)/shard_map/while
  154.7 5.1 %copy-start.1 = (f32[512,512,4]{1,0,2:T(8,128)S(1)}, f32[512,512,4]{1,0,2:T(8,128)}, u32[]{:S(2)}) copy-start(f32[512,512,4]{1,0,2:T(8,128)} %get-tuple-element.322) | copy-start | bytes 12582916 | tf_op jit(solution)/shard_map/while
  165.0 5.1 %copy-start.1 = (f32[512,512,4]{1,0,2:T(8,128)S(1)}, f32[512,512,4]{1,0,2:T(8,128)}, u32[]{:S(2)}) copy-start(f32[512,512,4]{1,0,2:T(8,128)} %get-tuple-element.322) | copy-start | bytes 12582916 | tf_op jit(solution)/shard_map/while
  174.2 13.6 %all-to-all-start = ((bf16[4,128,512]{2,1,0:T(8,128)(2,1)}), bf16[4,128,512]{2,1,0:T(8,128)(2,1)S(1)}, u32[]{:S(2)}, u32[]{:S(2)}) async-start(bf16[4,128,512]{2,1,0:T(8,128)(2,1)} %convert_element_type.95), calls=%async_computation | async-start | bytes 1048576 | tf_op jit(solution)/shard_map/all_to_all | solution.py:131
  188.8 5.0 %copy-start.4 = (f32[2048]{0:T(1024)S(1)}, f32[2048]{0:T(1024)}, u32[]{:S(2)}) copy-start(f32[2048]{0:T(1024)} %param.24) | copy-start | bytes 24580
  258.1 5.1 %copy-start.6 = (f32[128,2]{0,1:T(2,128)S(1)}, f32[128,2]{0,1:T(2,128)}, u32[]{:S(2)}) copy-start(f32[128,2]{0,1:T(2,128)} %param.26) | copy-start | bytes 3076
  258.1 35.5 %all-to-all-start.2 = ((bf16[128,4,2048]{2,1,0:T(4,128)(2,1)}), bf16[128,4,2048]{2,1,0:T(4,128)(2,1)}, u32[]{:S(2)}, u32[]{:S(2)}) async-start(bf16[128,4,2048]{2,1,0:T(4,128)(2,1)} %reshape.415), calls=%async_computation.2 | async-start | bytes 4194304 | tf_op jit(solution)/shard_map/all_to_all | solution.py:167
where the time goes:
time: 313 us; the launch traced here: 312 us
  matrix products  79.6 us (25%)
  starting transfers between devices  69.7 us (22%)
  waiting for transfers between devices  58.7 us (19%)
  local copies, waits for them, and re-layouts  43 us (14%)
  blocking collectives  39.5 us (13%)
  other arithmetic  20.7 us (7%)
    ppermute x18, starting transfers between devices, from_behind(): return lax.ppermute(block, axis, route)  60.7 us
    all_to_all x1, blocking collectives, on_device(): lax.all_to_all(outgoing, ('sp', 'tp'), split_axis=0, concat_axis=0, tiled...  39.5 us
    dot_general x7, matrix products, one_block(): jnp.einsum('hgqk,khd->hgqd', weights.astype(jnp.bfloat16), value_block, p...  35.4 us
    all_to_all x1, waiting for transfers between devices, on_device(): lax.all_to_all(expert_out.reshape(sources, slots, width), ('sp', 'tp'), s...  30.3 us
    dot_general x7, matrix products, one_block(): jnp.einsum('qhgd,khd->hgqk', query_grid, key_block, preferred_element_typ...  26.4 us
    ppermute x18, waiting for transfers between devices, from_behind(): return lax.ppermute(block, axis, route)  19.2 us
    unnamed x36, local copies, waits for them, and re-layouts  13.3 us
    all_to_all x1, waiting for transfers between devices, on_device(): lax.all_to_all(attn, 'tp', split_axis=0, concat_axis=1, tiled=True)  9.23 us
  transfers between devices with their start and end apart: 20, of which 8 were waited for; matrix products, arithmetic and copies ran while one was open for 5% of the time, Pallas kernels for 0%

commit v1 on v0

v1 whole, which is shorter than its diff:
```python
import functools

import jax
import jax.numpy as jnp
from jax import lax
from jax.experimental import pallas as pl
from jax.experimental.pallas import tpu as pltpu
from jax.sharding import PartitionSpec as P

HEAD = 128
HALF = HEAD // 2
GRID_W = 64
norm_eps = 1e-06
rope_base = 10000.0
LOW = -1e30
KB = 256
DOC_ROWS = 16
VMEM = pltpu.VMEM


def rotary_tables(first_row, length):
    count = HEAD // 4
    inverse = 1.0 / rope_base ** (jnp.arange(count, dtype=jnp.float32) / count)
    rows = (first_row // GRID_W + jnp.arange(length // GRID_W, dtype=jnp.int32)).astype(jnp.float32)
    cols = jnp.arange(GRID_W, dtype=jnp.int32).astype(jnp.float32)
    row_angle = rows[:, None] * inverse[None, :]
    col_angle = cols[:, None] * inverse[None, :]
    rz = jnp.zeros_like(row_angle)
    cz = jnp.zeros_like(col_angle)
    rc, rs = jnp.cos(row_angle), jnp.sin(row_angle)
    cc, cs = jnp.cos(col_angle), jnp.sin(col_angle)
    row_tab = jnp.stack(
        [jnp.concatenate([rc, rz, rc, rz], 1), jnp.concatenate([-rs, rz, rs, rz], 1)]
    )
    col_tab = jnp.stack(
        [jnp.concatenate([cz, cc, cz, cc], 1), jnp.concatenate([cz, -cs, cz, cs], 1)]
    )
    return row_tab, col_tab


def norm_rotate(x, gain, cos_full, sin_full):
    wide = x.astype(jnp.float32)
    mean = jnp.mean(wide * wide, axis=-1, keepdims=True)
    scaled = wide * lax.rsqrt(mean + norm_eps) * gain
    return (scaled * cos_full + pltpu.roll(scaled, HALF, 1) * sin_full).astype(jnp.bfloat16)


def key_kernel(k_ref, v_ref, doc_ref, gain_ref, row_ref, col_ref, out_ref):
    rows = k_ref.shape[0]
    gain = gain_ref[...]
    for g in range(rows // GRID_W):
        span = slice(g * GRID_W, (g + 1) * GRID_W)
        cos_full = col_ref[0] + row_ref[0, g : g + 1, :]
        sin_full = col_ref[1] + row_ref[1, g : g + 1, :]
        out_ref[span, :] = norm_rotate(k_ref[span, :], gain, cos_full, sin_full)
    out_ref[rows : 2 * rows, :] = v_ref[...]
    out_ref[2 * rows :, :] = doc_ref[...]


def query_kernel(q_ref, gain_ref, row_ref, col_ref, out_ref):
    rows, width = q_ref.shape
    gain = gain_ref[...]
    for g in range(rows // GRID_W):
        span = slice(g * GRID_W, (g + 1) * GRID_W)
        cos_full = col_ref[0] + row_ref[0, g : g + 1, :]
        sin_full = col_ref[1] + row_ref[1, g : g + 1, :]
        for h in range(width // HEAD):
            lanes = slice(h * HEAD, (h + 1) * HEAD)
            out_ref[span, lanes] = norm_rotate(q_ref[span, lanes], gain, cos_full, sin_full)


def attention_kernel(
    par_ref, edge_ref, q_ref, qdoc_ref, own, near, b1, b2, b3, b4, far, out_ref,
    k_scr, v_scr, d_scr, s_scr, mx_scr, l_scr, acc_scr,
):
    rows, width = q_ref.shape
    heads = width // HEAD
    par = par_ref[0]
    doc_rows = rows // HEAD
    slots = [
        (own, 3 + par), (near, 4 - par), (b1, 1 + par), (b2, 2 - par),
        (b3, 5 + par), (b4, 6 - par), (far, 7 * par),
    ]
    for src, slot in slots:
        at = pl.multiple_of(slot * rows, rows)
        k_scr[pl.ds(at, rows), :] = src[0:rows, :]
        v_scr[pl.ds(at, rows), :] = src[rows : 2 * rows, :]
        d_scr[slot] = src[2 * rows : 2 * rows + DOC_ROWS, :].astype(jnp.float32)
    d_scr[7 - 7 * par] = jnp.full((DOC_ROWS, HEAD), -1.0, jnp.float32)
    docs = d_scr[...]
    place = (
        lax.broadcasted_iota(jnp.int32, docs.shape, 0) * rows
        + lax.broadcasted_iota(jnp.int32, docs.shape, 1) * HEAD
        + lax.broadcasted_iota(jnp.int32, docs.shape, 2)
    )
    real = lax.broadcasted_iota(jnp.int32, docs.shape, 1) < doc_rows
    scale = HEAD ** (-0.5) * 1.4426950408889634
    block = rows // 4
    lanes = KB // HEAD
    per_slot = rows // KB
    for qs in range(4):
        first_doc = edge_ref[2 * qs]
        last_doc = edge_ref[2 * qs + 1]
        low = jnp.min(jnp.where((docs == first_doc) & real, place, 8 * rows))
        high = jnp.max(jnp.where((docs == last_doc) & real, place, -1))
        j0 = low // KB
        j1 = high // KB + 1
        span = slice(qs * block, (qs + 1) * block)
        q4 = jnp.concatenate([q_ref[span, h * HEAD : (h + 1) * HEAD] for h in range(heads)], 0)
        qdoc = qdoc_ref[span, :]
        mx_scr[...] = jnp.full(mx_scr.shape, LOW, jnp.float32)

        def scores(j, carry):
            at = pl.multiple_of(j * KB, KB)
            s = lax.dot_general(
                q4, k_scr[pl.ds(at, KB), :], (((1,), (1,)), ((), ())),
                preferred_element_type=jnp.float32,
            )
            slot = j // per_slot
            sub = (j % per_slot) * lanes
            keep = [qdoc == d_scr[slot, pl.ds(sub + t, 1), :] for t in range(lanes)]
            for h in range(heads):
                band = slice(h * block, (h + 1) * block)
                top = mx_scr[band, :]
                for t in range(lanes):
                    part = jnp.where(keep[t], s[band, t * HEAD : (t + 1) * HEAD], LOW)
                    s_scr[j, band, t * HEAD : (t + 1) * HEAD] = part
                    top = jnp.maximum(top, part)
                mx_scr[band, :] = top
            return carry

        lax.fori_loop(j0, j1, scores, 0)
        top = jnp.max(mx_scr[...], axis=1, keepdims=True) * scale
        mx_scr[...] = jnp.broadcast_to(top, mx_scr.shape)
        l_scr[...] = jnp.zeros(l_scr.shape, jnp.float32)
        acc_scr[...] = jnp.zeros(acc_scr.shape, jnp.float32)

        def weigh(j, carry):
            at = pl.multiple_of(j * KB, KB)
            top = mx_scr[...]
            parts = [
                jnp.exp2(s_scr[j, :, t * HEAD : (t + 1) * HEAD] * scale - top)
                for t in range(lanes)
            ]
            total = parts[0]
            for part in parts[1:]:
                total = total + part
            l_scr[...] += total
            p = jnp.concatenate([part.astype(jnp.bfloat16) for part in parts], axis=1)
            acc_scr[...] += jnp.dot(
                p, v_scr[pl.ds(at, KB), :], preferred_element_type=jnp.float32
            )
            return carry

        lax.fori_loop(j0, j1, weigh, 0)
        den = jnp.sum(l_scr[...], axis=1, keepdims=True)
        res = (acc_scr[...] / den).astype(jnp.bfloat16)
        for h in range(heads):
            out_ref[qs, :, h * HEAD : (h + 1) * HEAD] = res[h * block : (h + 1) * block, :]


def call(kernel, out_shape, name, scratch=(), smem=0, args=()):
    specs = [pl.BlockSpec(memory_space=pltpu.SMEM)] * smem
    specs += [pl.BlockSpec(memory_space=VMEM)] * (len(args) - smem)
    return pl.pallas_call(
        kernel,
        out_shape=out_shape,
        in_specs=specs,
        out_specs=jax.tree.map(lambda _: pl.BlockSpec(memory_space=VMEM), out_shape),
        scratch_shapes=list(scratch),
        name=name,
    )(*args)


def on_device(
    residual, query_proj, key_proj, value_proj, query_gain, key_gain, document_ids,
    output_weight, norm_gain, expert_ids, route_weights, gate_weight, up_weight, down_weight,
):
    bf16, f32 = jnp.bfloat16, jnp.float32
    sp = lax.axis_size("sp")
    index = lax.axis_index("sp")
    rows = query_proj.shape[0]
    row_tab, col_tab = rotary_tables(index * rows, rows)
    docs = document_ids.astype(bf16).reshape(rows // HEAD, HEAD)
    docs = jnp.pad(docs, ((0, DOC_ROWS - rows // HEAD), (0, 0)))
    packed = call(
        key_kernel,
        jax.ShapeDtypeStruct((2 * rows + DOC_ROWS, HEAD), bf16),
        "key_prep",
        args=(key_proj, value_proj, docs, key_gain.reshape(1, HEAD), row_tab, col_tab),
    )
    swap = [(i, i ^ 1) for i in range(sp)]
    cross = [(i, (i + 1) % sp) if i % 2 else (i, (i - 1) % sp) for i in range(sp)]
    right = [(i, (i + 2) % sp) for i in range(sp)]
    left = [(i, (i - 2) % sp) for i in range(sp)]
    par = index % 2
    from_left = lax.ppermute(packed, "sp", right)
    from_right = lax.ppermute(packed, "sp", left)
    near = lax.ppermute(packed, "sp", swap)
    far = lax.ppermute(jnp.where(par == 1, from_left, from_right), "sp", cross)
    left_pair = lax.ppermute(from_left, "sp", swap)
    right_pair = lax.ppermute(from_right, "sp", swap)

    query_norm = call(
        query_kernel,
        jax.ShapeDtypeStruct(query_proj.shape, bf16),
        "query_prep",
        args=(query_proj, query_gain.reshape(1, HEAD), row_tab, col_tab),
    )
    doc_f = document_ids.astype(f32)
    query_doc = jnp.broadcast_to(doc_f[:, None], (rows, HEAD))
    quarter = rows // 4
    edges = doc_f.reshape(4, quarter)[:, :: quarter - 1].reshape(8)
    width = query_proj.shape[1]
    attn = call(
        attention_kernel,
        jax.ShapeDtypeStruct((4, quarter, width), bf16),
        "attention",
        scratch=(
            VMEM((8 * rows, HEAD), bf16),
            VMEM((8 * rows, HEAD), bf16),
            VMEM((8, DOC_ROWS, HEAD), f32),
            VMEM((8 * rows // KB, rows, KB), f32),
            VMEM((rows, HEAD), f32),
            VMEM((rows, HEAD), f32),
            VMEM((rows, HEAD), f32),
        ),
        smem=2,
        args=(
            par.reshape(1).astype(jnp.int32), edges, query_norm, query_doc, packed, near,
            from_left, left_pair, from_right, right_pair, far,
        ),
    )
    token_rows = residual.shape[0]
    attn = attn.reshape(rows, width)
    all_heads = lax.all_to_all(attn, "tp", split_axis=0, concat_axis=1, tiled=True)
    projected = jnp.dot(all_heads, output_weight, preferred_element_type=f32)
    hidden = (residual.astype(f32) + projected).astype(bf16)
    hidden_wide = hidden.astype(f32)
    normed = (
        hidden_wide
        * lax.rsqrt(jnp.mean(hidden_wide * hidden_wide, axis=-1, keepdims=True) + norm_eps)
        * norm_gain
    ).astype(bf16)
    top_count = expert_ids.shape[1]
    experts_all = sp * lax.axis_size("tp")
    capacity = max(2, 2 * token_rows * top_count // experts_all)
    flat_ids = expert_ids.reshape(-1)
    onehot = (flat_ids[:, None] == jnp.arange(experts_all, dtype=jnp.int32)[None, :]).astype(
        jnp.int32
    )
    arrival = jnp.sum(jnp.cumsum(onehot, axis=0) * onehot, axis=1) - 1
    slot_grid = (flat_ids * capacity + arrival).reshape(token_rows, top_count)
    slots = experts_all * capacity
    hits = (
        jnp.arange(slots, dtype=jnp.int32)[:, None, None] == slot_grid[None]
    )
    placing = jnp.any(hits, axis=2).astype(bf16)
    gather = jnp.sum(jnp.where(hits, route_weights[None], 0.0), axis=2)
    gather_hi = gather.astype(bf16)
    gather_lo = (gather - gather_hi.astype(f32)).astype(bf16)
    outgoing = jnp.dot(placing, normed, preferred_element_type=f32).astype(bf16)
    outgoing = outgoing.reshape(experts_all, capacity, normed.shape[1])
    arrived = lax.all_to_all(outgoing, ("sp", "tp"), split_axis=0, concat_axis=0, tiled=True)
    sources, per, wide = arrived.shape
    flat_rows = arrived.reshape(sources * per, wide)
    gate_part = jnp.dot(flat_rows, gate_weight[0], preferred_element_type=f32)
    up_part = jnp.dot(flat_rows, up_weight[0], preferred_element_type=f32)
    activity = (jax.nn.silu(gate_part) * up_part).astype(bf16)
    expert_out = jnp.dot(activity, down_weight[0], preferred_element_type=f32).astype(bf16)
    returned = lax.all_to_all(
        expert_out.reshape(sources, per, wide), ("sp", "tp"), split_axis=0, concat_axis=0,
        tiled=True,
    ).reshape(slots, wide)
    dims = (((0,), (0,)), ((), ()))
    combined = lax.dot_general(gather_hi, returned, dims, preferred_element_type=f32)
    combined += lax.dot_general(gather_lo, returned, dims, preferred_element_type=f32)
    return (hidden_wide + combined).astype(bf16)


def solution(mesh):
    both = P(("sp", "tp"), None)
    in_specs = (
        both, P("sp", "tp"), P("sp", "tp"), P("sp", "tp"), P(), P(), P("sp"), P(), P(),
        both, both,
        P(("sp", "tp"), None, None), P(("sp", "tp"), None, None), P(("sp", "tp"), None, None),
    )
    return jax.shard_map(
        on_device, mesh=mesh, in_specs=in_specs, out_specs=both, check_vma=False
    )
```

time: 313 us -> 173 us (0.55)
  matrix products: 79.6 us -> 21.2 us
  starting transfers between devices: 69.7 us -> 21.9 us
  Pallas kernels: 0 us -> 24.8 us
  local copies, waits for them, and re-layouts: 43 us -> 20.7 us
  other arithmetic: 20.7 us -> 4.03 us
  waiting for transfers between devices: 58.7 us -> 42.2 us
    dot_general x18 -> x6, matrix products: 79.6 us -> 21.2 us  [the longest x1 6.23 us: on_device(): jnp.dot(activity, down_weight[0], preferred_element_type=f32).astype(bf16)]
    ppermute x18 -> x6, starting transfers between devices: 60.7 us -> 12.9 us  [the longest x1 4.91 us: on_device(): from_right = lax.ppermute(packed, 'sp', left)]
    pallas_call x0 -> x3, Pallas kernels: none -> 24.8 us  [call(): pl.pallas_call(kernel, out_shape=out_shape, in_specs=specs, out_specs=jax...]
    ppermute x18 -> x6, waiting for transfers between devices: 19.2 us -> 3.15 us  [the longest x1 3.13 us: on_device(): from_left = lax.ppermute(packed, 'sp', right)]
    unnamed x36 -> x20, local copies, waits for them, and re-layouts: 13.3 us -> 0.83 us
    reduce_sum x11 -> x1, other arithmetic: 12.4 us -> 0.06 us  [on_device(): gather = jnp.sum(jnp.where(hits, route_weights[None], 0.0), axis=2)]
    gather x1 -> x0, local copies, waits for them, and re-layouts: 5.19 us -> none  [on_device(): fetched = returned.reshape(experts_all * capacity, -1)[slot_index]]
    convert_element_type x3 -> x0, local copies, waits for them, and re-layouts: 4.76 us -> none  [the longest x1 3.36 us: on_device(): fetched = fetched.reshape(token_rows, top_count, -1).astype(jnp.float32)]
  transfers between devices with their start and end apart: 20 -> 8, of which waited for: 8 -> 3; matrix products, arithmetic and copies ran while one was open for 5% -> 2% of each run, Pallas kernels for 0% -> 3%
where the time goes in v1:
time: 173 us; the launch traced here: 172 us
  waiting for transfers between devices  42.2 us (24%)
  blocking collectives  37.3 us (22%)
  Pallas kernels  24.8 us (14%)
  starting transfers between devices  21.9 us (13%)
  matrix products  21.2 us (12%)
  local copies, waits for them, and re-layouts  20.7 us (12%)
  other arithmetic  4.03 us (2%)
    all_to_all x1, blocking collectives, on_device(): lax.all_to_all(outgoing, ('sp', 'tp'), split_axis=0, concat_axis=0, tiled...  37.3 us
    all_to_all x1, waiting for transfers between devices, on_device(): lax.all_to_all(expert_out.reshape(sources, per, wide), ('sp', 'tp'), spli...  30.5 us
    pallas_call x3, Pallas kernels, call(): pl.pallas_call(kernel, out_shape=out_shape, in_specs=specs, out_specs=jax...  24.8 us
    all_to_all x1, waiting for transfers between devices, on_device(): lax.all_to_all(attn, 'tp', split_axis=0, concat_axis=1, tiled=True)  8.56 us
    dot_general x1, matrix products, on_device(): jnp.dot(activity, down_weight[0], preferred_element_type=f32).astype(bf16)  6.23 us
    all_to_all x1, starting transfers between devices, on_device(): lax.all_to_all(expert_out.reshape(sources, per, wide), ('sp', 'tp'), spli...  4.97 us
    dot_general x1, matrix products, on_device(): projected = jnp.dot(all_heads, output_weight, preferred_element_type=f32)  4.95 us
    ppermute x1, starting transfers between devices, on_device(): from_right = lax.ppermute(packed, 'sp', left)  4.91 us
  transfers between devices with their start and end apart: 8, of which 3 were waited for; matrix products, arithmetic and copies ran while one was open for 2% of the time, Pallas kernels for 3%

profile of v1, /device:TPU:1, one launch (start us, length us, event | category | flops | bytes accessed | tf_op | source)
XLA Modules:
  0.0 172.3 jit_solution(7825031615364821846)
XLA Ops:
  0.0 0.0 copy-start
  0.1 0.1 multiply_cosine_fusion.1
  0.2 0.2 multiply_cosine_fusion
  0.4 0.9 convert_bitcast_fusion
  1.3 0.1 fusion.35
  1.3 0.6 pad_maximum_fusion.5.row_ref
  1.9 0.1 fusion.29
  2.0 0.6 pad_maximum_fusion.col_ref
  2.7 0.6 pad.4.doc_ref
  3.3 2.3 %key_prep.1.own = bf16[1040,128]{1,0:T(8,128)(2,1)} custom-call(bf16[512,128]{1,0:T(8,128)(2,1)} %k_ref.1, bf16[512,128]{1,0:T(8,128)(2,1)} %v_ref.1, bf16[16,128]{1,0:T(8,128)(2,1)} %pad.4.doc_ref, f32[1,128]{1,0:T(1,128)} %bitcast.56, f32[2,8,128]{2,1,0:T(8,128)} %pad_maximum_fusion.5.row_ref, f32[2,64,128]{2,1,0:T(8,128)} %pad_maximum_fusion.col_ref), custom_call_target="tpu_custom_call" | custom-call | tf_op jit(solution)/shard_map/key_prep/pallas_call | solution.py:165
  5.5 2.1 %collective-permute-start.1 = (bf16[1040,128]{1,0:T(8,128)(2,1)}, bf16[1040,128]{1,0:T(8,128)(2,1)S(1)}, u32[]{:S(2)}, u32[]{:S(2)}) collective-permute-start(bf16[1040,128]{1,0:T(8,128)(2,1)} %key_prep.1.own), channel_id=1, source_target_pairs={{0,8},{4,12},{8,16},{12,20},{16,24},{20,28},{24,32},{28,36},{32,40... | collective-permute-start | bytes 798728 | tf_op jit(solution)/shard_map/ppermute | solution.py:197
  7.6 4.9 %collective-permute-start.3 = (bf16[1040,128]{1,0:T(8,128)(2,1)}, bf16[1040,128]{1,0:T(8,128)(2,1)S(1)}, u32[]{:S(2)}, u32[]{:S(2)}) collective-permute-start(bf16[1040,128]{1,0:T(8,128)(2,1)} %key_prep.1.own), channel_id=1, source_target_pairs={{0,120},{4,124},{8,0},{12,4},{16,8},{20,12},{24,16},{28,20},{32,24... | collective-permute-start | bytes 798728 | tf_op jit(solution)/shard_map/ppermute | solution.py:198
  12.6 1.0 collective-permute-start
  13.5 0.8 copy.34
  14.3 0.1 eq.49
  14.4 0.1 copy.36
  14.6 0.2 fusion.21
  14.8 0.1 eq.45
  14.9 0.1 slice.9
  15.0 0.7 reshape.90.edge_ref
  15.7 3.1 %collective-permute-done.1.b1 = bf16[1040,128]{1,0:T(8,128)(2,1)S(1)} collective-permute-done((bf16[1040,128]{1,0:T(8,128)(2,1)}, bf16[1040,128]{1,0:T(8,128)(2,1)S(1)}, u32[]{:S(2)}, u32[]{:S(2)}) %collective-permute-start.1) | collective-permute-done | bytes 266272 | tf_op jit(solution)/shard_map/ppermute | solution.py:197
  18.9 0.0 collective-permute-done.3.b3
  18.9 0.8 broadcast_select_fusion
  19.7 0.0 collective-permute-start.5
  19.7 4.9 %collective-permute-start.2 = (bf16[1040,128]{1,0:T(8,128)(2,1)S(1)}, bf16[1040,128]{1,0:T(8,128)(2,1)}, u32[]{:S(2)}, u32[]{:S(2)}) collective-permute-start(bf16[1040,128]{1,0:T(8,128)(2,1)S(1)} %collective-permute-done.1.b1), channel_id=1, source_target_pairs={{0,4},{4,0},{8,12},{12,8},{16,20},{20,16},{24,28},{28,24},{32,36},... | collective-permute-start | bytes 798728 | tf_op jit(solution)/shard_map/ppermute | solution.py:201
  24.6 0.0 collective-permute-start.4
  24.6 5.1 %query_prep.1.q_ref = bf16[512,512]{1,0:T(8,128)(2,1)} custom-call(bf16[512,512]{1,0:T(8,128)(2,1)} %q_ref.1, f32[1,128]{1,0:T(1,128)} %bitcast.55, f32[2,8,128]{2,1,0:T(8,128)} %pad_maximum_fusion.5.row_ref, f32[2,64,128]{2,1,0:T(8,128)} %pad_maximum_fusion.col_ref), custom_call_target="tpu_custom_call" | custom-call | tf_op jit(solution)/shard_map/query_prep/pallas_call | solution.py:165
  29.7 0.2 fusion.22
  29.9 0.0 collective-permute-done.near
  29.9 0.0 copy-start.4
  29.9 0.0 collective-permute-done.5.far
  29.9 0.0 copy-start.5
  29.9 0.0 collective-permute-done.2.b2
  29.9 0.0 collective-permute-done.4.b4
  29.9 0.8 broadcast_in_dim.16.qdoc_ref
  30.8 0.0 copy-done.2
  30.8 0.0 copy-done.3
  30.8 0.0 copy-done.4
  30.8 0.0 copy-done.5
  30.8 0.0 copy-start.7
  30.8 17.4 %attention.1 = bf16[4,128,512]{2,1,0:T(8,128)(2,1)} custom-call(s32[1]{0:T(128)} %bitcast.par_ref, f32[8]{0:T(128)} %reshape.90.edge_ref, bf16[512,512]{1,0:T(8,128)(2,1)} %query_prep.1.q_ref, f32[512,128]{1,0:T(8,128)} %broadcast_in_dim.16.qdoc_ref, bf16[1040,128]{1,0:T(8,128)(2,1)} %key_prep.1.own, bf16[1040,128]{1,0:T(8,128)(2,1)} %copy-done.4, ...), custom_call_target="tpu_custom_call" | custom-call | tf_op jit(solution)/shard_map/attention/pallas_call | solution.py:165
  48.2 4.0 %all-to-all-start = ((bf16[4,128,512]{2,1,0:T(8,128)(2,1)}), bf16[4,128,512]{2,1,0:T(8,128)(2,1)S(1)}, u32[]{:S(2)}, u32[]{:S(2)}) async-start(bf16[4,128,512]{2,1,0:T(8,128)(2,1)} %attention.1), calls=%async_computation | async-start | bytes 1048576 | tf_op jit(solution)/shard_map/all_to_all | solution.py:236
  52.3 0.1 sub.15
  52.4 0.1 copy.38
  52.5 0.0 copy-done.7
  52.5 0.1 fusion.20
  52.6 8.6 %all-to-all-done = bf16[4,128,512]{2,1,0:T(8,128)(2,1)S(1)} async-done(((bf16[4,128,512]{2,1,0:T(8,128)(2,1)}), bf16[4,128,512]{2,1,0:T(8,128)(2,1)S(1)}, u32[]{:S(2)}, u32[]{:S(2)}) %all-to-all-start) | async-done | bytes 524320 | tf_op jit(solution)/shard_map/all_to_all | solution.py:236
  61.1 1.0 copy.33
  62.1 4.9 %multiply_reduce_fusion = (f32[128]{0:T(128)S(1)}, f32[128,2048]{1,0:T(8,128)S(1)}) fusion(bf16[128,2048]{0,1:T(8,128)(2,1)} %bitcast.50, bf16[2048,2048]{1,0:T(8,128)(2,1)} %param.21, bf16[128,2048]{1,0:T(8,128)(2,1)} %param.14), kind=kOutput, calls=%fused_computation.16 | convolution fusion | flops 1075314560 | bytes 10486272 | tf_op jit(solution)/shard_map/dot_general | solution.py:237
  67.1 2.1 %convolution_convert_fusion.1 = bf16[512,2048]{1,0:T(8,128)(2,1)} fusion(pred[512,128]{1,0:T(8,128)(4,1)S(1)} %fusion.20, f32[128,2048]{1,0:T(8,128)S(1)} %get-tuple-element.19, f32[2048]{0:T(1024)S(1)} %copy-done.6, f32[128]{0:T(128)S(1)} %add_rsqrt_fusion), kind=kOutput, calls=%fused_computation.1 | convolution fusion | flops 270270464 | bytes 3219968 | tf_op jit(solution)/shard_map/dot_general | solution.py:262
  69.2 4.1 %reshape.95 = bf16[128,4,2048]{2,1,0:T(4,128)(2,1)} reshape(bf16[512,2048]{1,0:T(8,128)(2,1)} %convolution_convert_fusion.1) | data formatting | bytes 4194304 | tf_op jit(solution)/shard_map/reshape | solution.py:263
  73.3 37.3 %all_to_all.26 = bf16[128,4,2048]{2,1,0:T(4,128)(2,1)} all-to-all(bf16[128,4,2048]{2,1,0:T(4,128)(2,1)} %reshape.95), channel_id=1, replica_groups=mesh['sp'=32,'tp'=4] {'sp','tp'}, dimensions={0} | all-to-all | bytes 4194304 | tf_op jit(solution)/shard_map/all_to_all | solution.py:264
  110.5 3.9 %reshape.96 = bf16[512,2048]{1,0:T(8,128)(2,1)} reshape(bf16[128,4,2048]{2,1,0:T(4,128)(2,1)} %all_to_all.26) | data formatting | bytes 4194304 | tf_op jit(solution)/shard_map/reshape | solution.py:266
  114.5 4.4 %fusion.7 = f32[512,512]{1,0:T(8,128)} fusion(bf16[512,2048]{1,0:T(8,128)(2,1)} %reshape.96, bf16[1,2048,512]{2,1,0:T(8,128)(2,1)} %param.25), kind=kOutput, calls=%fused_computation.11 | convolution fusion | flops 1073741824 | bytes 5242880 | tf_op jit(solution)/shard_map/dot_general | solution.py:267
  118.9 6.2 %convolution_convert_fusion = bf16[512,2048]{1,0:T(8,128)(2,1)} fusion(bf16[1,512,2048]{2,1,0:T(8,128)(2,1)S(1)} %copy-done, bf16[512,2048]{1,0:T(8,128)(2,1)} %reshape.96, bf16[1,2048,512]{2,1,0:T(8,128)(2,1)} %param.26, f32[512,512]{1,0:T(8,128)} %fusion.7), kind=kOutput, calls=%fused_computation | convolution fusion | flops 2150105088 | bytes 9437184 | tf_op jit(solution)/shard_map/dot_general | solution.py:270
  125.2 4.1 %reshape.97 = bf16[128,4,2048]{2,1,0:T(4,128)(2,1)} reshape(bf16[512,2048]{1,0:T(8,128)(2,1)} %convolution_convert_fusion) | data formatting | bytes 4194304 | tf_op jit(solution)/shard_map/reshape | solution.py:272
  129.3 5.0 %all-to-all-start.2 = ((bf16[128,4,2048]{2,1,0:T(4,128)(2,1)}), bf16[128,4,2048]{2,1,0:T(4,128)(2,1)}, u32[]{:S(2)}, u32[]{:S(2)}) async-start(bf16[128,4,2048]{2,1,0:T(4,128)(2,1)} %reshape.97), calls=%async_computation.2 | async-start | bytes 4194304 | tf_op jit(solution)/shard_map/all_to_all | solution.py:271
  134.2 0.0 copy-done.8
  134.2 0.1 select_reduce_fusion
  134.3 30.5 %all-to-all-done.2 = bf16[128,4,2048]{2,1,0:T(4,128)(2,1)} async-done(((bf16[128,4,2048]{2,1,0:T(4,128)(2,1)}), bf16[128,4,2048]{2,1,0:T(4,128)(2,1)}, u32[]{:S(2)}, u32[]{:S(2)}) %all-to-all-start.2) | async-done | bytes 2097184 | tf_op jit(solution)/shard_map/all_to_all | solution.py:271
  164.8 3.9 %reshape.98 = bf16[512,2048]{1,0:T(8,128)(2,1)} reshape(bf16[128,4,2048]{2,1,0:T(4,128)(2,1)} %all-to-all-done.2) | data formatting | bytes 4194304 | tf_op jit(solution)/shard_map/reshape | solution.py:274
  168.7 2.2 %fusion.25 = f32[128,2048]{1,0:T(8,128)S(1)} fusion(bf16[512,2048]{1,0:T(8,128)(2,1)} %reshape.98, f32[512,128]{1,0:T(8,128)S(1)} %select_reduce_fusion), kind=kOutput, calls=%fused_computation.33 | convolution fusion | flops 268500992 | bytes 3407872 | tf_op jit(solution)/shard_map/dot_general | solution.py:276
  170.9 0.0 copy-done.1
  171.0 1.3 fusion.3
  (21 shorter events, 0.1 us)
Async XLA Ops:
  0.0 118.9 %copy-start = (bf16[1,512,2048]{2,1,0:T(8,128)(2,1)S(1)}, bf16[1,512,2048]{2,1,0:T(8,128)(2,1)}, u32[]{:S(2)}) copy-start(bf16[1,512,2048]{2,1,0:T(8,128)(2,1)} %param.27) | copy-start | bytes 6291460
  5.5 13.3 %collective-permute-start.1 = (bf16[1040,128]{1,0:T(8,128)(2,1)}, bf16[1040,128]{1,0:T(8,128)(2,1)S(1)}, u32[]{:S(2)}, u32[]{:S(2)}) collective-permute-start(bf16[1040,128]{1,0:T(8,128)(2,1)} %key_prep.1.own), channel_id=1, source_target_pairs={{0,8},{4,12},{8,16},{12,20},{16,24},{20,28},{24,32},{28,36},{32,40... | collective-permute-start | bytes 798728 | tf_op jit(solution)/shard_map/ppermute | solution.py:197
  7.6 11.2 %collective-permute-start.3 = (bf16[1040,128]{1,0:T(8,128)(2,1)}, bf16[1040,128]{1,0:T(8,128)(2,1)S(1)}, u32[]{:S(2)}, u32[]{:S(2)}) collective-permute-start(bf16[1040,128]{1,0:T(8,128)(2,1)} %key_prep.1.own), channel_id=1, source_target_pairs={{0,120},{4,124},{8,0},{12,4},{16,8},{20,12},{24,16},{28,20},{32,24... | collective-permute-start | bytes 798728 | tf_op jit(solution)/shard_map/ppermute | solution.py:198
  12.6 17.3 %collective-permute-start = (bf16[1040,128]{1,0:T(8,128)(2,1)}, bf16[1040,128]{1,0:T(8,128)(2,1)S(1)}, u32[]{:S(2)}, u32[]{:S(2)}) collective-permute-start(bf16[1040,128]{1,0:T(8,128)(2,1)} %key_prep.1.own), channel_id=1, source_target_pairs={{0,4},{4,0},{8,12},{12,8},{16,20},{20,16},{24,28},{28,24},{32,36},... | collective-permute-start | bytes 798728 | tf_op jit(solution)/shard_map/ppermute | solution.py:199
  18.9 11.9 %copy-start.2 = (bf16[1040,128]{1,0:T(8,128)(2,1)}, bf16[1040,128]{1,0:T(8,128)(2,1)S(1)}, u32[]{:S(2)}) copy-start(bf16[1040,128]{1,0:T(8,128)(2,1)S(1)} %collective-permute-done.1.b1) | copy-start | bytes 798724
  18.9 11.9 %copy-start.3 = (bf16[1040,128]{1,0:T(8,128)(2,1)}, bf16[1040,128]{1,0:T(8,128)(2,1)S(1)}, u32[]{:S(2)}) copy-start(bf16[1040,128]{1,0:T(8,128)(2,1)S(1)} %collective-permute-done.3.b3) | copy-start | bytes 798724
  19.7 10.2 %collective-permute-start.5 = (bf16[1040,128]{1,0:T(8,128)(2,1)}, bf16[1040,128]{1,0:T(8,128)(2,1)S(1)}, u32[]{:S(2)}, u32[]{:S(2)}) collective-permute-start(bf16[1040,128]{1,0:T(8,128)(2,1)} %broadcast_select_fusion), channel_id=1, source_target_pairs={{0,124},{4,8},{8,4},{12,16},{16,12},{20,24},{24,20},{28,32},{32,28... | collective-permute-start | bytes 798728 | tf_op jit(solution)/shard_map/ppermute | solution.py:200
  19.7 10.2 %collective-permute-start.2 = (bf16[1040,128]{1,0:T(8,128)(2,1)S(1)}, bf16[1040,128]{1,0:T(8,128)(2,1)}, u32[]{:S(2)}, u32[]{:S(2)}) collective-permute-start(bf16[1040,128]{1,0:T(8,128)(2,1)S(1)} %collective-permute-done.1.b1), channel_id=1, source_target_pairs={{0,4},{4,0},{8,12},{12,8},{16,20},{20,16},{24,28},{28,24},{32,36},... | collective-permute-start | bytes 798728 | tf_op jit(solution)/shard_map/ppermute | solution.py:201
  24.6 5.4 %collective-permute-start.4 = (bf16[1040,128]{1,0:T(8,128)(2,1)S(1)}, bf16[1040,128]{1,0:T(8,128)(2,1)}, u32[]{:S(2)}, u32[]{:S(2)}) collective-permute-start(bf16[1040,128]{1,0:T(8,128)(2,1)S(1)} %collective-permute-done.3.b3), channel_id=1, source_target_pairs={{0,4},{4,0},{8,12},{12,8},{16,20},{20,16},{24,28},{28,24},{32,36},... | collective-permute-start | bytes 798728 | tf_op jit(solution)/shard_map/ppermute | solution.py:202
  29.9 0.9 copy-start.4
  29.9 0.9 copy-start.5
  30.8 21.7 %copy-start.7 = (s32[128,2]{0,1:T(2,128)S(1)}, s32[128,2]{0,1:T(2,128)}, u32[]{:S(2)}) copy-start(s32[128,2]{0,1:T(2,128)} %param.23) | copy-start | bytes 3076
  48.2 12.9 %all-to-all-start = ((bf16[4,128,512]{2,1,0:T(8,128)(2,1)}), bf16[4,128,512]{2,1,0:T(8,128)(2,1)S(1)}, u32[]{:S(2)}, u32[]{:S(2)}) async-start(bf16[4,128,512]{2,1,0:T(8,128)(2,1)} %attention.1), calls=%async_computation | async-start | bytes 1048576 | tf_op jit(solution)/shard_map/all_to_all | solution.py:236
  62.1 5.0 %copy-start.6 = (f32[2048]{0:T(1024)S(1)}, f32[2048]{0:T(1024)}, u32[]{:S(2)}) copy-start(f32[2048]{0:T(1024)} %param.22) | copy-start | bytes 24580
  129.3 5.0 %copy-start.8 = (f32[128,2]{0,1:T(2,128)S(1)}, f32[128,2]{0,1:T(2,128)}, u32[]{:S(2)}) copy-start(f32[128,2]{0,1:T(2,128)} %param.24) | copy-start | bytes 3076
  129.3 35.5 %all-to-all-start.2 = ((bf16[128,4,2048]{2,1,0:T(4,128)(2,1)}), bf16[128,4,2048]{2,1,0:T(4,128)(2,1)}, u32[]{:S(2)}, u32[]{:S(2)}) async-start(bf16[128,4,2048]{2,1,0:T(4,128)(2,1)} %reshape.97), calls=%async_computation.2 | async-start | bytes 4194304 | tf_op jit(solution)/shard_map/all_to_all | solution.py:271
  168.7 2.2 %copy-start.1 = (bf16[512,2048]{1,0:T(8,128)(2,1)S(1)}, bf16[512,2048]{1,0:T(8,128)(2,1)}, u32[]{:S(2)}) copy-start(bf16[512,2048]{1,0:T(8,128)(2,1)} %reshape.98) | copy-start | bytes 6291460

commit v2 on v1

--- a/solution.py
+++ b/solution.py
@@ -159,7 +159,90 @@
             out_ref[qs, :, h * HEAD : (h + 1) * HEAD] = res[h * block : (h + 1) * block, :]
 
 
-def call(kernel, out_shape, name, scratch=(), smem=0, args=()):
+def project_kernel(slot_ref, heads_ref, w_ref, res_ref, gain_ref, hid_ref, out_ref, n_scr):
+    groups, rows, part = heads_ref.shape
+    width = res_ref.shape[1]
+    fold = width // HEAD
+    acc = jnp.dot(heads_ref[0], w_ref[0:part, :], preferred_element_type=jnp.float32)
+    for g in range(1, groups):
+        acc += jnp.dot(
+            heads_ref[g], w_ref[g * part : (g + 1) * part, :], preferred_element_type=jnp.float32
+        )
+    hidden = (res_ref[...].astype(jnp.float32) + acc).astype(jnp.bfloat16)
+    hid_ref[...] = hidden
+    wide = hidden.astype(jnp.float32)
+    mean = jnp.mean(wide * wide, axis=-1, keepdims=True)
+    normed = wide * lax.rsqrt(mean + norm_eps) * gain_ref[...]
+    for c in range(fold):
+        n_scr[pl.ds(c, rows, stride=fold), :] = normed[:, c * HEAD : (c + 1) * HEAD]
+    zero = jnp.zeros((32,) + out_ref.shape[1:], jnp.bfloat16)
+    for b in range(out_ref.shape[0] // 32):
+        out_ref[b * 32 : (b + 1) * 32] = zero
+
+    def place(step, carry):
+        for u in range(8):
+            token = step * 8 + u
+            tile = n_scr[pl.ds(pl.multiple_of(token * fold, fold), fold), :].astype(jnp.bfloat16)
+            out_ref[slot_ref[2 * token]] = tile
+            out_ref[slot_ref[2 * token + 1]] = tile
+        return carry
+
+    lax.fori_loop(0, rows // 8, place, 0)
+
+
+def expert_kernel(in_ref, gate_ref, up_ref, down_ref, out_ref, f_scr, x_scr):
+    slots, fold, _ = in_ref.shape
+    part = slots // 4
+    for b in range(4):
+        band = slice(b * part, (b + 1) * part)
+        f_scr[b * part * fold : (b + 1) * part * fold, :] = (
+            in_ref[band].astype(jnp.float32).reshape(part * fold, HEAD)
+        )
+        for c in range(fold):
+            x_scr[band, c * HEAD : (c + 1) * HEAD] = f_scr[
+                pl.ds(b * part * fold + c, part, stride=fold), :
+            ].astype(jnp.bfloat16)
+    x = x_scr[...]
+    gate = jnp.dot(x, gate_ref[0], preferred_element_type=jnp.float32)
+    up = jnp.dot(x, up_ref[0], preferred_element_type=jnp.float32)
+    act = (jax.nn.silu(gate) * up).astype(jnp.bfloat16)
+    step = 2
+    for n in range(fold // step):
+        y = jnp.dot(
+            act, down_ref[0, :, n * step * HEAD : (n + 1) * step * HEAD],
+            preferred_element_type=jnp.float32,
+        )
+        for t in range(step):
+            f_scr[pl.ds(n * step + t, slots, stride=fold), :] = y[:, t * HEAD : (t + 1) * HEAD]
+    for b in range(4):
+        out_ref[b * part : (b + 1) * part] = (
+            f_scr[b * part * fold : (b + 1) * part * fold, :]
+            .reshape(part, fold, HEAD)
+            .astype(jnp.bfloat16)
+        )
+
+
+def combine_kernel(slot_ref, weight_ref, ret_ref, hid_ref, out_ref, c_scr):
+    rows, width = hid_ref.shape
+    fold = width // HEAD
+
+    def gather(step, carry):
+        for u in range(8):
+            token = step * 8 + u
+            one = ret_ref[slot_ref[2 * token]].astype(jnp.float32) * weight_ref[2 * token]
+            two = ret_ref[slot_ref[2 * token + 1]].astype(jnp.float32) * weight_ref[2 * token + 1]
+            c_scr[pl.ds(pl.multiple_of(token * fold, fold), fold), :] = one + two
+        return carry
+
+    lax.fori_loop(0, rows // 8, gather, 0)
+    for c in range(fold):
+        lanes = slice(c * HEAD, (c + 1) * HEAD)
+        out_ref[:, lanes] = (
+            hid_ref[:, lanes].astype(jnp.float32) + c_scr[pl.ds(c, rows, stride=fold), :]
+        ).astype(jnp.bfloat16)
+
+
+def call(kernel, out_shape, name, limit, scratch=(), smem=0, args=()):
     specs = [pl.BlockSpec(memory_space=pltpu.SMEM)] * smem
     specs += [pl.BlockSpec(memory_space=VMEM)] * (len(args) - smem)
     return pl.pallas_call(
@@ -169,6 +252,7 @@
         out_specs=jax.tree.map(lambda _: pl.BlockSpec(memory_space=VMEM), out_shape),
         scratch_shapes=list(scratch),
         name=name,
+        compiler_params=pltpu.CompilerParams(vmem_limit_bytes=limit * 2**20),
     )(*args)
 
 
@@ -186,7 +270,7 @@
     packed = call(
         key_kernel,
         jax.ShapeDtypeStruct((2 * rows + DOC_ROWS, HEAD), bf16),
-        "key_prep",
+        "key_prep", 8,
         args=(key_proj, value_proj, docs, key_gain.reshape(1, HEAD), row_tab, col_tab),
     )
     swap = [(i, i ^ 1) for i in range(sp)]
@@ -204,7 +288,7 @@
     query_norm = call(
         query_kernel,
         jax.ShapeDtypeStruct(query_proj.shape, bf16),
-        "query_prep",
+        "query_prep", 8,
         args=(query_proj, query_gain.reshape(1, HEAD), row_tab, col_tab),
     )
     doc_f = document_ids.astype(f32)
@@ -215,7 +299,7 @@
     attn = call(
         attention_kernel,
         jax.ShapeDtypeStruct((4, quarter, width), bf16),
-        "attention",
+        "attention", 20,
         scratch=(
             VMEM((8 * rows, HEAD), bf16),
             VMEM((8 * rows, HEAD), bf16),
@@ -231,51 +315,53 @@
             from_left, left_pair, from_right, right_pair, far,
         ),
     )
-    token_rows = residual.shape[0]
-    attn = attn.reshape(rows, width)
-    all_heads = lax.all_to_all(attn, "tp", split_axis=0, concat_axis=1, tiled=True)
-    projected = jnp.dot(all_heads, output_weight, preferred_element_type=f32)
-    hidden = (residual.astype(f32) + projected).astype(bf16)
-    hidden_wide = hidden.astype(f32)
-    normed = (
-        hidden_wide
-        * lax.rsqrt(jnp.mean(hidden_wide * hidden_wide, axis=-1, keepdims=True) + norm_eps)
-        * norm_gain
-    ).astype(bf16)
+    token_rows, wide = residual.shape
+    fold = wide // HEAD
     top_count = expert_ids.shape[1]
     experts_all = sp * lax.axis_size("tp")
     capacity = max(2, 2 * token_rows * top_count // experts_all)
+    slots = experts_all * capacity
     flat_ids = expert_ids.reshape(-1)
     onehot = (flat_ids[:, None] == jnp.arange(experts_all, dtype=jnp.int32)[None, :]).astype(
         jnp.int32
     )
     arrival = jnp.sum(jnp.cumsum(onehot, axis=0) * onehot, axis=1) - 1
-    slot_grid = (flat_ids * capacity + arrival).reshape(token_rows, top_count)
-    slots = experts_all * capacity
-    hits = (
-        jnp.arange(slots, dtype=jnp.int32)[:, None, None] == slot_grid[None]
-    )
-    placing = jnp.any(hits, axis=2).astype(bf16)
-    gather = jnp.sum(jnp.where(hits, route_weights[None], 0.0), axis=2)
-    gather_hi = gather.astype(bf16)
-    gather_lo = (gather - gather_hi.astype(f32)).astype(bf16)
-    outgoing = jnp.dot(placing, normed, preferred_element_type=f32).astype(bf16)
-    outgoing = outgoing.reshape(experts_all, capacity, normed.shape[1])
-    arrived = lax.all_to_all(outgoing, ("sp", "tp"), split_axis=0, concat_axis=0, tiled=True)
-    sources, per, wide = arrived.shape
-    flat_rows = arrived.reshape(sources * per, wide)
-    gate_part = jnp.dot(flat_rows, gate_weight[0], preferred_element_type=f32)
-    up_part = jnp.dot(flat_rows, up_weight[0], preferred_element_type=f32)
-    activity = (jax.nn.silu(gate_part) * up_part).astype(bf16)
-    expert_out = jnp.dot(activity, down_weight[0], preferred_element_type=f32).astype(bf16)
-    returned = lax.all_to_all(
-        expert_out.reshape(sources, per, wide), ("sp", "tp"), split_axis=0, concat_axis=0,
-        tiled=True,
-    ).reshape(slots, wide)
-    dims = (((0,), (0,)), ((), ()))
-    combined = lax.dot_general(gather_hi, returned, dims, preferred_element_type=f32)
-    combined += lax.dot_general(gather_lo, returned, dims, preferred_element_type=f32)
-    return (hidden_wide + combined).astype(bf16)
+    slot = flat_ids * capacity + arrival
+    heads = lax.all_to_all(attn, "tp", split_axis=0, concat_axis=0, tiled=True)
+    hidden, outgoing = call(
+        project_kernel,
+        (
+            jax.ShapeDtypeStruct((token_rows, wide), bf16),
+            jax.ShapeDtypeStruct((slots, fold, HEAD), bf16),
+        ),
+        "project", 24,
+        scratch=(VMEM((token_rows * fold, HEAD), f32),),
+        smem=1,
+        args=(slot, heads, output_weight, residual, norm_gain.reshape(1, wide)),
+    )
+
+    def exchange(x):
+        x = x.reshape(experts_all, capacity * fold, HEAD)
+        x = lax.all_to_all(x, ("sp", "tp"), split_axis=0, concat_axis=0, tiled=True)
+        return x.reshape(slots, fold, HEAD)
+
+    arrived = exchange(outgoing)
+    expert_out = call(
+        expert_kernel,
+        jax.ShapeDtypeStruct((slots, fold, HEAD), bf16),
+        "experts", 32,
+        scratch=(VMEM((slots * fold, HEAD), f32), VMEM((slots, wide), bf16)),
+        args=(arrived, gate_weight, up_weight, down_weight),
+    )
+    returned = exchange(expert_out)
+    return call(
+        combine_kernel,
+        jax.ShapeDtypeStruct((token_rows, wide), bf16),
+        "combine", 16,
+        scratch=(VMEM((token_rows * fold, HEAD), f32),),
+        smem=2,
+        args=(slot, route_weights.reshape(-1), returned, hidden),
+    )
 
 
 def solution(mesh):

time: 173 us -> 144 us (0.83)
  matrix products: 21.2 us -> 0 us
  local copies, waits for them, and re-layouts: 20.7 us -> 7.63 us
  blocking collectives: 37.3 us -> 43.7 us
  other arithmetic: 4.03 us -> 1.77 us
  Pallas kernels: 24.8 us -> 26.7 us
    dot_general x6 -> x0, matrix products: 21.2 us -> none  [the longest x1 6.23 us: on_device(): jnp.dot(activity, down_weight[0], preferred_element_type=f32).astype(bf16)]
    reshape x4 -> x2, local copies, waits for them, and re-layouts: 16.1 us -> 0.27 us  [the longest x1 0.14 us: on_device(): route_weights.reshape(-1)]
    all_to_all x1, blocking collectives: 37.3 us -> 43.7 us  [exchange(): x = lax.all_to_all(x, ('sp', 'tp'), split_axis=0, concat_axis=0, tiled=True)]
    unnamed x20 -> x27, local copies, waits for them, and re-layouts: 0.83 us -> 6.78 us
    pallas_call x3 -> x6, Pallas kernels: 24.8 us -> 26.7 us  [call(): pl.pallas_call(kernel, out_shape=out_shape, in_specs=specs, out_specs=jax...]
  transfers between devices with their start and end apart: 8 -> 8, of which waited for: 3 -> 3; matrix products, arithmetic and copies ran while one was open for 2% -> 1% of each run, Pallas kernels for 3% -> 2%
where the time goes in v2:
time: 144 us; the launch traced here: 143 us
  blocking collectives  43.7 us (30%)
  waiting for transfers between devices  42 us (29%)
  Pallas kernels  26.7 us (19%)
  starting transfers between devices  21.1 us (15%)
  local copies, waits for them, and re-layouts  7.63 us (5%)
  other arithmetic  1.77 us (1%)
    all_to_all x1, blocking collectives, exchange(): x = lax.all_to_all(x, ('sp', 'tp'), split_axis=0, concat_axis=0, tiled=True)  43.7 us
    all_to_all x1, waiting for transfers between devices, exchange(): x = lax.all_to_all(x, ('sp', 'tp'), split_axis=0, concat_axis=0, tiled=True)  30.6 us
    pallas_call x6, Pallas kernels, call(): pl.pallas_call(kernel, out_shape=out_shape, in_specs=specs, out_specs=jax...  26.7 us
    all_to_all x1, waiting for transfers between devices, on_device(): heads = lax.all_to_all(attn, 'tp', split_axis=0, concat_axis=0, tiled=True)  7.37 us
    unnamed x27, local copies, waits for them, and re-layouts  6.78 us
    ppermute x1, starting transfers between devices, on_device(): from_right = lax.ppermute(packed, 'sp', left)  4.99 us
    ppermute x1, starting transfers between devices, on_device(): left_pair = lax.ppermute(from_left, 'sp', swap)  4.96 us
    ppermute x1, waiting for transfers between devices, on_device(): from_left = lax.ppermute(packed, 'sp', right)  4.02 us
  transfers between devices with their start and end apart: 8, of which 3 were waited for; matrix products, arithmetic and copies ran while one was open for 1% of the time, Pallas kernels for 2%

profile of v2, /device:TPU:1, one launch (start us, length us, event | category | flops | bytes accessed | tf_op | source)
XLA Modules:
  0.0 143.2 jit_solution(9741569644799243480)
XLA Ops:
  0.0 0.0 copy-start.9
  0.0 0.0 copy-start.5
  0.1 0.1 multiply_cosine_fusion.1
  0.2 0.2 multiply_cosine_fusion
  0.4 0.8 convert_bitcast_fusion
  1.1 0.1 fusion.11
  1.2 0.1 fusion.5
  1.4 0.0 copy-start.6
  1.4 0.9 copy-done.6
  2.3 0.0 copy-start.7
  2.3 0.9 copy-done.7
  3.2 0.0 copy-start.10
  3.2 0.7 copy-done.10
  3.8 0.5 key_prep.1.own
  4.4 2.2 %collective-permute-start.1 = (bf16[1040,128]{1,0:T(8,128)(2,1)S(1)}, bf16[1040,128]{1,0:T(8,128)(2,1)S(1)}, u32[]{:S(2)}, u32[]{:S(2)}) collective-permute-start(bf16[1040,128]{1,0:T(8,128)(2,1)S(1)} %key_prep.1.own), channel_id=1, source_target_pairs={{0,8},{4,12},{8,16},{12,20},{16,24},{20,28},{24,32},{28,36},{32,40... | collective-permute-start | bytes 798728 | tf_op jit(solution)/shard_map/ppermute | solution.py:281
  6.6 5.0 %collective-permute-start.3 = (bf16[1040,128]{1,0:T(8,128)(2,1)S(1)}, bf16[1040,128]{1,0:T(8,128)(2,1)S(1)}, u32[]{:S(2)}, u32[]{:S(2)}) collective-permute-start(bf16[1040,128]{1,0:T(8,128)(2,1)S(1)} %key_prep.1.own), channel_id=1, source_target_pairs={{0,120},{4,124},{8,0},{12,4},{16,8},{20,12},{24,16},{28,20},{32,24... | collective-permute-start | bytes 798728 | tf_op jit(solution)/shard_map/ppermute | solution.py:282
  11.6 1.0 collective-permute-start
  12.5 0.8 copy.15
  13.3 0.1 eq.31
  13.4 0.1 copy.17
  13.6 4.0 %collective-permute-done.1.b1 = bf16[1040,128]{1,0:T(8,128)(2,1)S(1)} collective-permute-done((bf16[1040,128]{1,0:T(8,128)(2,1)S(1)}, bf16[1040,128]{1,0:T(8,128)(2,1)S(1)}, u32[]{:S(2)}, u32[]{:S(2)}) %collective-permute-start.1) | collective-permute-done | bytes 266272 | tf_op jit(solution)/shard_map/ppermute | solution.py:281
  17.6 0.0 collective-permute-done.3.b3
  17.6 0.1 collective-permute-start.5
  17.7 5.0 %collective-permute-start.2 = (bf16[1040,128]{1,0:T(8,128)(2,1)S(1)}, bf16[1040,128]{1,0:T(8,128)(2,1)S(1)}, u32[]{:S(2)}, u32[]{:S(2)}) collective-permute-start(bf16[1040,128]{1,0:T(8,128)(2,1)S(1)} %collective-permute-done.1.b1), channel_id=1, source_target_pairs={{0,4},{4,0},{8,12},{12,8},{16,20},{20,16},{24,28},{28,24},{32,36},... | collective-permute-start | bytes 798728 | tf_op jit(solution)/shard_map/ppermute | solution.py:285
  22.7 0.0 collective-permute-start.4
  22.7 0.2 fusion
  22.9 0.1 slice.11
  23.0 0.1 reshape.77.edge_ref
  23.1 0.0 copy-done.9
  23.1 0.0 copy-done.5
  23.1 3.2 %query_prep.1.q_ref = bf16[512,512]{1,0:T(8,128)(2,1)S(1)} custom-call(bf16[512,512]{1,0:T(8,128)(2,1)S(1)} %copy-done.5, f32[1,128]{1,0:T(1,128)S(1)} %bitcast.35, f32[2,8,128]{2,1,0:T(8,128)S(1)} %pad_maximum_fusion.5.row_ref, f32[2,64,128]{2,1,0:T(8,128)S(1)} %pad_maximum_fusion.col_ref), custom_call_target="tpu_custom_call" | custom-call | tf_op jit(solution)/shard_map/query_prep/pallas_call | solution.py:248
  26.4 0.0 collective-permute-done.near
  26.4 0.0 collective-permute-done.5.far
  26.4 0.0 collective-permute-done.2.b2
  26.4 0.0 collective-permute-done.4.b4
  26.4 0.1 broadcast_in_dim.8.qdoc_ref
  26.5 0.0 copy-start.4
  26.5 0.0 copy-start.8
  26.5 11.0 %attention.1 = bf16[4,128,512]{2,1,0:T(8,128)(2,1)} custom-call(s32[1]{0:T(128)} %bitcast.3.par_ref, f32[8]{0:T(128)S(1)} %reshape.77.edge_ref, bf16[512,512]{1,0:T(8,128)(2,1)S(1)} %query_prep.1.q_ref, f32[512,128]{1,0:T(8,128)S(1)} %broadcast_in_dim.8.qdoc_ref, bf16[1040,128]{1,0:T(8,128)(2,1)S(1)} %key_prep.1.own, ...), custom_call_target="tpu_custom_call" | custom-call | tf_op jit(solution)/shard_map/attention/pallas_call | solution.py:248
  37.6 4.0 %all-to-all-start = ((bf16[4,128,512]{2,1,0:T(8,128)(2,1)}), bf16[4,128,512]{2,1,0:T(8,128)(2,1)S(1)}, u32[]{:S(2)}, u32[]{:S(2)}) async-start(bf16[4,128,512]{2,1,0:T(8,128)(2,1)} %attention.1), calls=%async_computation | async-start | bytes 1048576 | tf_op jit(solution)/shard_map/all_to_all | solution.py:330
  41.6 0.1 reshape.72
  41.8 0.2 fusion.1
  42.0 7.4 %all-to-all-done.heads_ref = bf16[4,128,512]{2,1,0:T(8,128)(2,1)S(1)} async-done(((bf16[4,128,512]{2,1,0:T(8,128)(2,1)}), bf16[4,128,512]{2,1,0:T(8,128)(2,1)S(1)}, u32[]{:S(2)}, u32[]{:S(2)}) %all-to-all-start) | async-done | bytes 524320 | tf_op jit(solution)/shard_map/all_to_all | solution.py:330
  49.3 0.0 copy-done.4
  49.3 0.0 copy-done.8
  49.3 0.0 copy-start
  49.3 3.4 %copy-done = bf16[2048,2048]{1,0:T(8,128)(2,1)S(1)} copy-done((bf16[2048,2048]{1,0:T(8,128)(2,1)S(1)}, bf16[2048,2048]{1,0:T(8,128)(2,1)}, u32[]{:S(2)}) %copy-start) | copy-done | bytes 8388632
  52.7 0.0 copy-start.3
  52.7 2.9 %project.1 = (bf16[128,2048]{1,0:T(8,128)(2,1)S(1)}, bf16[512,16,128]{2,1,0:T(8,128)(2,1)S(1)}) custom-call(s32[256]{0:T(256)S(1)} %add_add_fusion.slot_ref, bf16[4,128,512]{2,1,0:T(8,128)(2,1)S(1)} %all-to-all-done.heads_ref, bf16[2048,2048]{1,0:T(8,128)(2,1)S(1)} %copy-done, bf16[128,2048]{1,0:T(8,128)(2,1)S(1)} %copy-done.4, f32[1,2048]{1,0:T(1,128)S(1)} %bitcast.34), custom_call_target="tpu_custom_call" | custom-call | tf_op jit(solution)/shard_map/project/pallas_call | solution.py:248
  55.6 0.0 copy-start.1
  55.6 0.0 copy-start.2
  55.6 43.7 %all_to_all.15 = bf16[128,64,128]{2,1,0:T(8,128)(2,1)S(1)} all-to-all(bf16[128,64,128]{2,1,0:T(8,128)(2,1)S(1)} %bitcast.33), channel_id=1, replica_groups=mesh['sp'=32,'tp'=4] {'sp','tp'}, dimensions={0} | all-to-all | bytes 4194304 | tf_op jit(solution)/shard_map/all_to_all | solution.py:345
  99.3 0.0 copy-done.3
  99.3 0.0 copy-done.1
  99.3 0.0 copy-done.2
  99.3 6.8 %experts.1 = bf16[512,16,128]{2,1,0:T(8,128)(2,1)} custom-call(bf16[512,16,128]{2,1,0:T(8,128)(2,1)S(1)} %bitcast.31, bf16[1,2048,512]{2,1,0:T(8,128)(2,1)S(1)} %copy-done.1, bf16[1,2048,512]{2,1,0:T(8,128)(2,1)S(1)} %copy-done.2, bf16[1,512,2048]{2,1,0:T(8,128)(2,1)S(1)} %copy-done.3), custom_call_target="tpu_custom_call" | custom-call | tf_op jit(solution)/shard_map/experts/pallas_call | solution.py:248
  106.1 0.0 copy-start.11
  106.1 3.9 %all-to-all-start.2 = ((bf16[128,64,128]{2,1,0:T(8,128)(2,1)}), bf16[128,64,128]{2,1,0:T(8,128)(2,1)S(1)}, u32[]{:S(2)}, u32[]{:S(2)}) async-start(bf16[128,64,128]{2,1,0:T(8,128)(2,1)} %bitcast.15), calls=%async_computation.2 | async-start | bytes 4194304 | tf_op jit(solution)/shard_map/all_to_all | solution.py:345
  110.0 0.0 copy-done.11
  110.0 0.1 copy.19
  110.1 0.1 reshape.74.weight_ref
  110.3 30.6 %all-to-all-done.2 = bf16[128,64,128]{2,1,0:T(8,128)(2,1)S(1)} async-done(((bf16[128,64,128]{2,1,0:T(8,128)(2,1)}), bf16[128,64,128]{2,1,0:T(8,128)(2,1)S(1)}, u32[]{:S(2)}, u32[]{:S(2)}) %all-to-all-start.2) | async-done | bytes 2097184 | tf_op jit(solution)/shard_map/all_to_all | solution.py:345
  140.9 2.3 %combine.1 = bf16[128,2048]{1,0:T(8,128)(2,1)} custom-call(s32[256]{0:T(256)S(1)} %add_add_fusion.slot_ref, f32[256]{0:T(256)S(1)} %reshape.74.weight_ref, bf16[512,16,128]{2,1,0:T(8,128)(2,1)S(1)} %bitcast.32, bf16[128,2048]{1,0:T(8,128)(2,1)S(1)} %get-tuple-element.8.hid_ref), custom_call_target="tpu_custom_call" | custom-call | tf_op jit(solution)/shard_map/combine/pallas_call | solution.py:248
  (16 shorter events, 0.2 us)
Async XLA Ops:
  0.0 23.1 %copy-start.9 = (f32[128]{0:T(128)S(1)}, f32[128]{0:T(128)}, u32[]{:S(2)}) copy-start(f32[128]{0:T(128)} %param.18) | copy-start | bytes 1540
  0.0 23.1 %copy-start.5 = (bf16[512,512]{1,0:T(8,128)(2,1)S(1)}, bf16[512,512]{1,0:T(8,128)(2,1)}, u32[]{:S(2)}) copy-start(bf16[512,512]{1,0:T(8,128)(2,1)} %q_ref.1) | copy-start | bytes 1572868
  1.4 0.9 copy-start.6
  2.3 0.9 copy-start.7
  3.2 0.7 copy-start.10
  4.4 13.2 %collective-permute-start.1 = (bf16[1040,128]{1,0:T(8,128)(2,1)S(1)}, bf16[1040,128]{1,0:T(8,128)(2,1)S(1)}, u32[]{:S(2)}, u32[]{:S(2)}) collective-permute-start(bf16[1040,128]{1,0:T(8,128)(2,1)S(1)} %key_prep.1.own), channel_id=1, source_target_pairs={{0,8},{4,12},{8,16},{12,20},{16,24},{20,28},{24,32},{28,36},{32,40... | collective-permute-start | bytes 798728 | tf_op jit(solution)/shard_map/ppermute | solution.py:281
  6.6 11.0 %collective-permute-start.3 = (bf16[1040,128]{1,0:T(8,128)(2,1)S(1)}, bf16[1040,128]{1,0:T(8,128)(2,1)S(1)}, u32[]{:S(2)}, u32[]{:S(2)}) collective-permute-start(bf16[1040,128]{1,0:T(8,128)(2,1)S(1)} %key_prep.1.own), channel_id=1, source_target_pairs={{0,120},{4,124},{8,0},{12,4},{16,8},{20,12},{24,16},{28,20},{32,24... | collective-permute-start | bytes 798728 | tf_op jit(solution)/shard_map/ppermute | solution.py:282
  11.6 14.8 %collective-permute-start = (bf16[1040,128]{1,0:T(8,128)(2,1)S(1)}, bf16[1040,128]{1,0:T(8,128)(2,1)S(1)}, u32[]{:S(2)}, u32[]{:S(2)}) collective-permute-start(bf16[1040,128]{1,0:T(8,128)(2,1)S(1)} %key_prep.1.own), channel_id=1, source_target_pairs={{0,4},{4,0},{8,12},{12,8},{16,20},{20,16},{24,28},{28,24},{32,36},... | collective-permute-start | bytes 798728 | tf_op jit(solution)/shard_map/ppermute | solution.py:283
  17.6 8.7 %collective-permute-start.5 = (bf16[1040,128]{1,0:T(8,128)(2,1)S(1)}, bf16[1040,128]{1,0:T(8,128)(2,1)S(1)}, u32[]{:S(2)}, u32[]{:S(2)}) collective-permute-start(bf16[1040,128]{1,0:T(8,128)(2,1)S(1)} %broadcast_select_fusion), channel_id=1, source_target_pairs={{0,124},{4,8},{8,4},{12,16},{16,12},{20,24},{24,20},{28,32},{32,28... | collective-permute-start | bytes 798728 | tf_op jit(solution)/shard_map/ppermute | solution.py:284
  17.7 8.7 %collective-permute-start.2 = (bf16[1040,128]{1,0:T(8,128)(2,1)S(1)}, bf16[1040,128]{1,0:T(8,128)(2,1)S(1)}, u32[]{:S(2)}, u32[]{:S(2)}) collective-permute-start(bf16[1040,128]{1,0:T(8,128)(2,1)S(1)} %collective-permute-done.1.b1), channel_id=1, source_target_pairs={{0,4},{4,0},{8,12},{12,8},{16,20},{20,16},{24,28},{28,24},{32,36},... | collective-permute-start | bytes 798728 | tf_op jit(solution)/shard_map/ppermute | solution.py:285
  22.7 3.7 %collective-permute-start.4 = (bf16[1040,128]{1,0:T(8,128)(2,1)S(1)}, bf16[1040,128]{1,0:T(8,128)(2,1)S(1)}, u32[]{:S(2)}, u32[]{:S(2)}) collective-permute-start(bf16[1040,128]{1,0:T(8,128)(2,1)S(1)} %collective-permute-done.3.b3), channel_id=1, source_target_pairs={{0,4},{4,0},{8,12},{12,8},{16,20},{20,16},{24,28},{28,24},{32,36},... | collective-permute-start | bytes 798728 | tf_op jit(solution)/shard_map/ppermute | solution.py:286
  26.5 22.8 %copy-start.4 = (bf16[128,2048]{1,0:T(8,128)(2,1)S(1)}, bf16[128,2048]{1,0:T(8,128)(2,1)}, u32[]{:S(2)}) copy-start(bf16[128,2048]{1,0:T(8,128)(2,1)} %res_ref.1) | copy-start | bytes 1572868
  26.5 22.8 %copy-start.8 = (f32[2048]{0:T(1024)S(1)}, f32[2048]{0:T(1024)}, u32[]{:S(2)}) copy-start(f32[2048]{0:T(1024)} %param.22) | copy-start | bytes 24580
  37.6 11.7 %all-to-all-start = ((bf16[4,128,512]{2,1,0:T(8,128)(2,1)}), bf16[4,128,512]{2,1,0:T(8,128)(2,1)S(1)}, u32[]{:S(2)}, u32[]{:S(2)}) async-start(bf16[4,128,512]{2,1,0:T(8,128)(2,1)} %attention.1), calls=%async_computation | async-start | bytes 1048576 | tf_op jit(solution)/shard_map/all_to_all | solution.py:330
  49.3 3.4 %copy-start = (bf16[2048,2048]{1,0:T(8,128)(2,1)S(1)}, bf16[2048,2048]{1,0:T(8,128)(2,1)}, u32[]{:S(2)}) copy-start(bf16[2048,2048]{1,0:T(8,128)(2,1)} %w_ref.1) | copy-start | bytes 25165828
  52.7 46.6 %copy-start.3 = (bf16[1,512,2048]{2,1,0:T(8,128)(2,1)S(1)}, bf16[1,512,2048]{2,1,0:T(8,128)(2,1)}, u32[]{:S(2)}) copy-start(bf16[1,512,2048]{2,1,0:T(8,128)(2,1)} %down_ref.1) | copy-start | bytes 6291460
  55.6 43.7 %copy-start.1 = (bf16[1,2048,512]{2,1,0:T(8,128)(2,1)S(1)}, bf16[1,2048,512]{2,1,0:T(8,128)(2,1)}, u32[]{:S(2)}) copy-start(bf16[1,2048,512]{2,1,0:T(8,128)(2,1)} %gate_ref.1) | copy-start | bytes 6291460
  55.6 43.7 %copy-start.2 = (bf16[1,2048,512]{2,1,0:T(8,128)(2,1)S(1)}, bf16[1,2048,512]{2,1,0:T(8,128)(2,1)}, u32[]{:S(2)}) copy-start(bf16[1,2048,512]{2,1,0:T(8,128)(2,1)} %up_ref.1) | copy-start | bytes 6291460
  106.1 3.9 %copy-start.11 = (f32[128,2]{0,1:T(2,128)S(1)}, f32[128,2]{0,1:T(2,128)}, u32[]{:S(2)}) copy-start(f32[128,2]{0,1:T(2,128)} %param.24) | copy-start | bytes 3076
  106.1 34.8 %all-to-all-start.2 = ((bf16[128,64,128]{2,1,0:T(8,128)(2,1)}), bf16[128,64,128]{2,1,0:T(8,128)(2,1)S(1)}, u32[]{:S(2)}, u32[]{:S(2)}) async-start(bf16[128,64,128]{2,1,0:T(8,128)(2,1)} %bitcast.15), calls=%async_computation.2 | async-start | bytes 4194304 | tf_op jit(solution)/shard_map/all_to_all | solution.py:345

commit v3 on v2

v3 whole, which is shorter than its diff:
```python
import functools

import jax
import jax.numpy as jnp
from jax import lax
from jax.experimental import pallas as pl
from jax.experimental.pallas import tpu as pltpu
from jax.sharding import PartitionSpec as P


HEAD = 128
HALF = HEAD // 2
GRID_W = 64
norm_eps = 1e-06
rope_base = 10000.0
LOW = -1e30
KB = 512
DOC_ROWS = 16
VMEM = pltpu.VMEM


def rotary_tables(first_row, length):
    count = HEAD // 4
    inverse = 1.0 / rope_base ** (jnp.arange(count, dtype=jnp.float32) / count)
    rows = (first_row // GRID_W + jnp.arange(length // GRID_W, dtype=jnp.int32)).astype(jnp.float32)
    cols = jnp.arange(GRID_W, dtype=jnp.int32).astype(jnp.float32)
    row_angle = rows[:, None] * inverse[None, :]
    col_angle = cols[:, None] * inverse[None, :]
    rz = jnp.zeros_like(row_angle)
    cz = jnp.zeros_like(col_angle)
    rc, rs = jnp.cos(row_angle), jnp.sin(row_angle)
    cc, cs = jnp.cos(col_angle), jnp.sin(col_angle)
    row_tab = jnp.stack(
        [jnp.concatenate([rc, rz, rc, rz], 1), jnp.concatenate([-rs, rz, rs, rz], 1)]
    )
    col_tab = jnp.stack(
        [jnp.concatenate([cz, cc, cz, cc], 1), jnp.concatenate([cz, -cs, cz, cs], 1)]
    )
    return row_tab, col_tab


def norm_rotate(x, gain, cos_full, sin_full):
    wide = x.astype(jnp.float32)
    mean = jnp.mean(wide * wide, axis=-1, keepdims=True)
    scaled = wide * lax.rsqrt(mean + norm_eps) * gain
    return (scaled * cos_full + pltpu.roll(scaled, HALF, 1) * sin_full).astype(jnp.bfloat16)


def key_kernel(
    k_hbm, v_hbm, doc_hbm, gain_hbm, row_ref, col_ref, out_ref, k_ref, doc_ref, gain_ref, sems
):
    rows = k_ref.shape[0]
    copies = [
        pltpu.make_async_copy(k_hbm, k_ref, sems.at[0]),
        pltpu.make_async_copy(gain_hbm, gain_ref, sems.at[1]),
        pltpu.make_async_copy(doc_hbm, doc_ref, sems.at[2]),
        pltpu.make_async_copy(v_hbm, out_ref.at[pl.ds(rows, rows), :], sems.at[3]),
    ]
    for copy in copies:
        copy.start()
    for copy in copies[:3]:
        copy.wait()
    docs = doc_ref[...].astype(jnp.float32).astype(jnp.bfloat16)
    pad = jnp.zeros((DOC_ROWS - docs.shape[0], HEAD), jnp.bfloat16)
    out_ref[2 * rows :, :] = jnp.concatenate([docs, pad], 0)
    gain = gain_ref[...]
    for g in range(rows // GRID_W):
        span = slice(g * GRID_W, (g + 1) * GRID_W)
        cos_full = col_ref[0] + row_ref[0, g : g + 1, :]
        sin_full = col_ref[1] + row_ref[1, g : g + 1, :]
        out_ref[span, :] = norm_rotate(k_ref[span, :], gain, cos_full, sin_full)
    copies[3].wait()


def query_kernel(
    q_hbm, ids_hbm, doc_hbm, gain_hbm, row_ref, col_ref, out_ref, qdoc_ref, slot_ref,
    q_ref, ids_ref, doc_ref, gain_ref, sems, *, capacity,
):
    copies = [
        pltpu.make_async_copy(src, dst, sems.at[n])
        for n, (src, dst) in enumerate(
            [(q_hbm, q_ref), (gain_hbm, gain_ref), (doc_hbm, doc_ref), (ids_hbm, ids_ref)]
        )
    ]
    for copy in copies:
        copy.start()
    for copy in copies:
        copy.wait()
    rows, width = q_ref.shape
    gain = gain_ref[...]
    for g in range(rows // GRID_W):
        span = slice(g * GRID_W, (g + 1) * GRID_W)
        cos_full = col_ref[0] + row_ref[0, g : g + 1, :]
        sin_full = col_ref[1] + row_ref[1, g : g + 1, :]
        for h in range(width // HEAD):
            lanes = slice(h * HEAD, (h + 1) * HEAD)
            out_ref[span, lanes] = norm_rotate(q_ref[span, lanes], gain, cos_full, sin_full)
    for t in range(doc_ref.shape[0]):
        line = jnp.broadcast_to(doc_ref[t : t + 1, :].astype(jnp.float32), (HEAD, HEAD))
        qdoc_ref[t * HEAD : (t + 1) * HEAD, :] = line.T
    choices, tokens = ids_ref.shape
    sub = lax.broadcasted_iota(jnp.int32, (HEAD, tokens), 0)
    lane = lax.broadcasted_iota(jnp.int32, (tokens, tokens), 1)
    upper = (lax.broadcasted_iota(jnp.int32, (tokens, tokens), 0) <= lane).astype(jnp.float32)
    upper = upper.astype(jnp.bfloat16)
    before = jnp.zeros((HEAD, 1), jnp.float32)
    for k in range(choices):
        ids = ids_ref[k : k + 1, :]
        hit = (sub == ids).astype(jnp.float32)
        running = before + jnp.dot(
            hit.astype(jnp.bfloat16), upper, preferred_element_type=jnp.float32
        )
        arrival = jnp.sum(running * hit, axis=0, keepdims=True) - 1.0
        slot_ref[k : k + 1, :] = ids * capacity + arrival.astype(jnp.int32)
        before = before + jnp.sum(hit, axis=1, keepdims=True)


def attention_kernel(
    par_ref, edge_ref, w_hbm, q_ref, qdoc_ref, own, near, b1, b2, b3, b4, far, out_ref, w_ref,
    k_scr, v_scr, d_scr, s_even, s_odd, mx_even, mx_odd, l_scr, acc_scr, sem,
):
    fetch = pltpu.make_async_copy(w_hbm, w_ref, sem)
    fetch.start()
    rows, width = q_ref.shape
    heads = width // HEAD
    par = par_ref[0]
    tiles = rows // HEAD
    slots = [
        (own, 3 + par), (near, 4 - par), (b1, 1 + par), (b2, 2 - par),
        (b3, 5 + par), (b4, 6 - par), (far, 7 * par),
    ]
    for src, slot in slots:
        at = pl.multiple_of(slot * rows, rows)
        k_scr[pl.ds(at, rows), :] = src[0:rows, :]
        v_scr[pl.ds(at, rows), :] = src[rows : 2 * rows, :]
        docs = src[2 * rows : 2 * rows + DOC_ROWS, :].astype(jnp.float32)
        for t in range(tiles):
            d_scr[slot * tiles + t] = jnp.broadcast_to(docs[t : t + 1, :], (8, HEAD))
    for slot in (7 - 7 * par, 8):
        at = pl.multiple_of(slot * rows, rows)
        k_scr[pl.ds(at, rows), :] = jnp.zeros((rows, HEAD), jnp.bfloat16)
        v_scr[pl.ds(at, rows), :] = jnp.zeros((rows, HEAD), jnp.bfloat16)
        for t in range(tiles):
            d_scr[slot * tiles + t] = jnp.full((8, HEAD), -1.0, jnp.float32)
    docs = d_scr[...]
    place = lax.broadcasted_iota(jnp.int32, docs.shape, 0) * HEAD + lax.broadcasted_iota(
        jnp.int32, docs.shape, 2
    )
    scale = HEAD ** (-0.5) * 1.4426950408889634
    block = rows // 4
    parts = KB // HEAD
    pieces = block // 16
    starts, counts = [], []
    for qs in range(4):
        first = edge_ref[qs, 0].astype(jnp.float32)
        last = edge_ref[qs, block - 1].astype(jnp.float32)
        low = jnp.min(jnp.where(docs == first, place, 8 * rows))
        high = jnp.max(jnp.where(docs == last, place, -1))
        start = (low // HEAD) * HEAD
        starts.append(start)
        counts.append((high - start) // KB + 1)
    s_refs = (s_even, s_odd)
    mx_refs = (mx_even, mx_odd)
    spare = s_even.shape[0] - 2
    for ref in s_refs:
        ref[spare] = jnp.full(ref.shape[1:], LOW, jnp.float32)

    def scores(qs, i):
        s_ref, mx_ref = s_refs[qs % 2], mx_refs[qs % 2]
        at = pl.multiple_of(jnp.minimum(starts[qs] + i * KB, 8 * rows), HEAD)
        index = jnp.where(i < counts[qs], i, spare + 1)
        base = qs * block
        q4 = jnp.concatenate(
            [
                q_ref[base + r * 16 : base + (r + 1) * 16, h * HEAD : (h + 1) * HEAD]
                for r in range(pieces)
                for h in range(heads)
            ],
            0,
        )
        s = lax.dot_general(
            q4, k_scr[pl.ds(at, KB), :], (((1,), (1,)), ((), ())),
            preferred_element_type=jnp.float32,
        )
        tile = at // HEAD
        key_docs = [d_scr[tile + t] for t in range(parts)]
        key_docs = [jnp.concatenate([d, d], 0) for d in key_docs]
        for r in range(pieces):
            qdoc = qdoc_ref[base + r * 16 : base + (r + 1) * 16, :]
            keep = [qdoc == d for d in key_docs]
            for h in range(heads):
                band = slice((r * heads + h) * 16, (r * heads + h + 1) * 16)
                top = mx_ref[band, :]
                for t in range(parts):
                    lanes = slice(t * HEAD, (t + 1) * HEAD)
                    part = jnp.where(keep[t], s[band, lanes], LOW)
                    s_ref[index, band, lanes] = part
                    top = jnp.maximum(top, part)
                mx_ref[band, :] = top

    def weigh(qs, i):
        s_ref, mx_ref = s_refs[qs % 2], mx_refs[qs % 2]
        at = pl.multiple_of(jnp.minimum(starts[qs] + i * KB, 8 * rows), HEAD)
        index = jnp.where(i < counts[qs], i, spare)
        top = mx_ref[...]
        probs = []
        total = l_scr[...]
        for t in range(parts):
            e = jnp.exp2(s_ref[index, :, t * HEAD : (t + 1) * HEAD] * scale - top)
            total = total + e
            probs.append(e.astype(jnp.bfloat16))
        l_scr[...] = total
        acc_scr[...] += jnp.dot(
            jnp.concatenate(probs, axis=1), v_scr[pl.ds(at, KB), :],
            preferred_element_type=jnp.float32,
        )

    for step in range(5):
        trip = counts[step] if step == 0 else counts[step - 1]
        if 0 < step < 4:
            trip = jnp.maximum(trip, counts[step])
        if step < 4:
            mx_refs[step % 2][...] = jnp.full(mx_even.shape, LOW, jnp.float32)
        if step > 0:
            l_scr[...] = jnp.zeros(l_scr.shape, jnp.float32)
            acc_scr[...] = jnp.zeros(acc_scr.shape, jnp.float32)

        def body(i, carry, step=step):
            if step > 0:
                weigh(step - 1, i)
            if step < 4:
                scores(step, i)
            return carry

        lax.fori_loop(0, trip, body, 0)
        if step < 4:
            ref = mx_refs[step % 2]
            ref[...] = jnp.broadcast_to(
                jnp.max(ref[...], axis=1, keepdims=True) * scale, ref.shape
            )
        if step > 0:
            den = jnp.sum(l_scr[...], axis=1, keepdims=True)
            res = (acc_scr[...] / den).astype(jnp.bfloat16)
            for r in range(pieces):
                for h in range(heads):
                    at = (r * heads + h) * 16
                    out_ref[step - 1, r * 16 : (r + 1) * 16, h * HEAD : (h + 1) * HEAD] = res[
                        at : at + 16, :
                    ]
    fetch.wait()


def project_kernel(slot_ref, heads_ref, w_ref, res_ref, gain_ref, hid_ref, out_ref, n_scr):
    groups, rows, part = heads_ref.shape
    width = res_ref.shape[1]
    fold = width // HEAD
    acc = jnp.dot(heads_ref[0], w_ref[0:part, :], preferred_element_type=jnp.float32)
    for g in range(1, groups):
        acc += jnp.dot(
            heads_ref[g], w_ref[g * part : (g + 1) * part, :], preferred_element_type=jnp.float32
        )
    hidden = (res_ref[...].astype(jnp.float32) + acc).astype(jnp.bfloat16)
    hid_ref[...] = hidden
    wide = hidden.astype(jnp.float32)
    mean = jnp.mean(wide * wide, axis=-1, keepdims=True)
    normed = wide * lax.rsqrt(mean + norm_eps) * gain_ref[...]
    for c in range(fold):
        n_scr[pl.ds(c, rows, stride=fold), :] = normed[:, c * HEAD : (c + 1) * HEAD]
    zero = jnp.zeros((32,) + out_ref.shape[1:], jnp.bfloat16)
    for b in range(out_ref.shape[0] // 32):
        out_ref[b * 32 : (b + 1) * 32] = zero

    def place(step, carry):
        for u in range(8):
            token = step * 8 + u
            tile = n_scr[pl.ds(pl.multiple_of(token * fold, fold), fold), :].astype(jnp.bfloat16)
            out_ref[slot_ref[0, token]] = tile
            out_ref[slot_ref[1, token]] = tile
        return carry

    lax.fori_loop(0, rows // 8, place, 0)


def expert_kernel(in_ref, gate_ref, up_ref, down_ref, out_ref, f_scr, x_scr):
    slots, fold, _ = in_ref.shape
    part = slots // 4
    for b in range(4):
        band = slice(b * part, (b + 1) * part)
        f_scr[b * part * fold : (b + 1) * part * fold, :] = (
            in_ref[band].astype(jnp.float32).reshape(part * fold, HEAD)
        )
        for c in range(fold):
            x_scr[band, c * HEAD : (c + 1) * HEAD] = f_scr[
                pl.ds(b * part * fold + c, part, stride=fold), :
            ].astype(jnp.bfloat16)
    x = x_scr[...]
    gate = jnp.dot(x, gate_ref[0], preferred_element_type=jnp.float32)
    up = jnp.dot(x, up_ref[0], preferred_element_type=jnp.float32)
    act = (jax.nn.silu(gate) * up).astype(jnp.bfloat16)
    step = 2
    for n in range(fold // step):
        y = jnp.dot(
            act, down_ref[0, :, n * step * HEAD : (n + 1) * step * HEAD],
            preferred_element_type=jnp.float32,
        )
        for t in range(step):
            f_scr[pl.ds(n * step + t, slots, stride=fold), :] = y[:, t * HEAD : (t + 1) * HEAD]
    for b in range(4):
        out_ref[b * part : (b + 1) * part] = (
            f_scr[b * part * fold : (b + 1) * part * fold, :]
            .reshape(part, fold, HEAD)
            .astype(jnp.bfloat16)
        )


def combine_kernel(slot_ref, weight_ref, ret_ref, hid_ref, out_ref, c_scr):
    rows, width = hid_ref.shape
    fold = width // HEAD

    def gather(step, carry):
        for u in range(8):
            token = step * 8 + u
            one = ret_ref[slot_ref[0, token]].astype(jnp.float32) * weight_ref[0, token]
            two = ret_ref[slot_ref[1, token]].astype(jnp.float32) * weight_ref[1, token]
            c_scr[pl.ds(pl.multiple_of(token * fold, fold), fold), :] = one + two
        return carry

    lax.fori_loop(0, rows // 8, gather, 0)
    for c in range(fold):
        lanes = slice(c * HEAD, (c + 1) * HEAD)
        out_ref[:, lanes] = (
            hid_ref[:, lanes].astype(jnp.float32) + c_scr[pl.ds(c, rows, stride=fold), :]
        ).astype(jnp.bfloat16)


def in_hbm(x):
    return pltpu.with_memory_space_constraint(x, pltpu.HBM)


def call(kernel, out_shape, limit, scratch=(), smem=0, args=(), hbm=0):
    specs = [pl.BlockSpec(memory_space=pltpu.SMEM)] * smem
    specs += [pl.BlockSpec(memory_space=pltpu.HBM)] * hbm
    specs += [pl.BlockSpec(memory_space=VMEM)] * (len(args) - smem - hbm)
    return pl.pallas_call(
        kernel,
        out_shape=out_shape,
        in_specs=specs,
        out_specs=jax.tree.map(lambda _: pl.BlockSpec(memory_space=VMEM), out_shape),
        scratch_shapes=list(scratch),
        compiler_params=pltpu.CompilerParams(vmem_limit_bytes=limit * 2**20),
    )(*args)


def on_device(
    residual, query_proj, key_proj, value_proj, query_gain, key_gain, document_ids,
    output_weight, norm_gain, expert_ids, route_weights, gate_weight, up_weight, down_weight,
):
    bf16, f32 = jnp.bfloat16, jnp.float32
    sp = lax.axis_size("sp")
    index = lax.axis_index("sp")
    rows = query_proj.shape[0]
    row_tab, col_tab = rotary_tables(index * rows, rows)
    doc_lines = document_ids.reshape(rows // HEAD, HEAD)
    packed = pl.pallas_call(
        key_kernel,
        out_shape=jax.ShapeDtypeStruct((2 * rows + DOC_ROWS, HEAD), bf16),
        in_specs=[pl.BlockSpec(memory_space=pltpu.HBM)] * 4
        + [pl.BlockSpec(memory_space=VMEM)] * 2,
        out_specs=pl.BlockSpec(memory_space=VMEM),
        scratch_shapes=[
            VMEM((rows, HEAD), bf16),
            VMEM((rows // HEAD, HEAD), jnp.int32),
            VMEM((1, HEAD), f32),
            pltpu.SemaphoreType.DMA((4,)),
        ],
        name="key_prep",
        compiler_params=pltpu.CompilerParams(vmem_limit_bytes=8 * 2**20),
    )(
        in_hbm(key_proj), in_hbm(value_proj), in_hbm(doc_lines),
        in_hbm(key_gain.reshape(1, HEAD)), row_tab, col_tab,
    )
    swap = [(i, i ^ 1) for i in range(sp)]
    cross = [(i, (i + 1) % sp) if i % 2 else (i, (i - 1) % sp) for i in range(sp)]
    right = [(i, (i + 2) % sp) for i in range(sp)]
    left = [(i, (i - 2) % sp) for i in range(sp)]
    par = index % 2
    from_left = lax.ppermute(packed, "sp", right)
    from_right = lax.ppermute(packed, "sp", left)
    near = lax.ppermute(packed, "sp", swap)
    far = lax.ppermute(jnp.where(par == 1, from_left, from_right), "sp", cross)
    left_pair = lax.ppermute(from_left, "sp", swap)
    right_pair = lax.ppermute(from_right, "sp", swap)

    quarter = rows // 4
    width = query_proj.shape[1]
    token_rows, wide = residual.shape
    fold = wide // HEAD
    top_count = expert_ids.shape[1]
    experts_all = sp * lax.axis_size("tp")
    capacity = max(2, 2 * token_rows * top_count // experts_all)
    slots = experts_all * capacity
    query_norm, query_doc, slot = call(
        functools.partial(query_kernel, capacity=capacity),
        (
            jax.ShapeDtypeStruct(query_proj.shape, bf16),
            jax.ShapeDtypeStruct((rows, HEAD), f32),
            jax.ShapeDtypeStruct((top_count, token_rows), jnp.int32),
        ),
        8,
        scratch=(
            VMEM(query_proj.shape, bf16),
            VMEM((top_count, token_rows), jnp.int32),
            VMEM(doc_lines.shape, jnp.int32),
            VMEM((1, HEAD), f32),
            pltpu.SemaphoreType.DMA((4,)),
        ),
        hbm=4,
        args=(
            in_hbm(query_proj), in_hbm(expert_ids.T), in_hbm(doc_lines),
            in_hbm(query_gain.reshape(1, HEAD)), row_tab, col_tab,
        ),
    )
    anywhere = pl.BlockSpec(memory_space=pltpu.HBM)
    smem = pl.BlockSpec(memory_space=pltpu.SMEM)
    vmem = pl.BlockSpec(memory_space=VMEM)
    attn, weight_near = pl.pallas_call(
        attention_kernel,
        out_shape=(
            jax.ShapeDtypeStruct((4, quarter, width), bf16),
            jax.ShapeDtypeStruct(output_weight.shape, bf16),
        ),
        in_specs=[smem, smem, anywhere] + [vmem] * 9,
        out_specs=(vmem, vmem),
        scratch_shapes=[
            VMEM((9 * rows, HEAD), bf16),
            VMEM((9 * rows, HEAD), bf16),
            VMEM((9 * rows // HEAD, 8, HEAD), f32),
            VMEM((10, rows, KB), f32),
            VMEM((10, rows, KB), f32),
            VMEM((rows, HEAD), f32),
            VMEM((rows, HEAD), f32),
            VMEM((rows, HEAD), f32),
            VMEM((rows, HEAD), f32),
            pltpu.SemaphoreType.DMA,
        ],
        name="attention",
        compiler_params=pltpu.CompilerParams(vmem_limit_bytes=40 * 2**20),
    )(
        par.reshape(1).astype(jnp.int32), doc_lines, in_hbm(output_weight), query_norm, query_doc, packed,
        near, from_left, left_pair, from_right, right_pair, far,
    )
    heads = lax.all_to_all(attn, "tp", split_axis=0, concat_axis=0, tiled=True)
    hidden, outgoing = call(
        project_kernel,
        (
            jax.ShapeDtypeStruct((token_rows, wide), bf16),
            jax.ShapeDtypeStruct((slots, fold, HEAD), bf16),
        ),
        24,
        scratch=(VMEM((token_rows * fold, HEAD), f32),),
        smem=1,
        args=(slot, heads, weight_near, residual, norm_gain.reshape(1, wide)),
    )

    def exchange(x):
        x = x.reshape(experts_all, capacity * fold, HEAD)
        x = lax.all_to_all(x, ("sp", "tp"), split_axis=0, concat_axis=0, tiled=True)
        return x.reshape(slots, fold, HEAD)

    arrived = exchange(outgoing)
    expert_out = call(
        expert_kernel,
        jax.ShapeDtypeStruct((slots, fold, HEAD), bf16),
        32,
        scratch=(VMEM((slots * fold, HEAD), f32), VMEM((slots, wide), bf16)),
        args=(arrived, gate_weight, up_weight, down_weight),
    )
    returned = exchange(expert_out)
    return call(
        combine_kernel,
        jax.ShapeDtypeStruct((token_rows, wide), bf16),
        16,
        scratch=(VMEM((token_rows * fold, HEAD), f32),),
        smem=2,
        args=(slot, route_weights.T, returned, hidden),
    )


def solution(mesh):
    both = P(("sp", "tp"), None)
    in_specs = (
        both, P("sp", "tp"), P("sp", "tp"), P("sp", "tp"), P(), P(), P("sp"), P(), P(),
        both, both,
        P(("sp", "tp"), None, None), P(("sp", "tp"), None, None), P(("sp", "tp"), None, None),
    )

    return jax.shard_map(on_device, mesh=mesh, in_specs=in_specs, out_specs=both, check_vma=False)
```

time: 144 us -> 130 us (0.903)
  blocking collectives: 43.7 us -> 83.9 us
  waiting for transfers between devices: 42 us -> 7.84 us
  starting transfers between devices: 21.1 us -> 11.9 us
  local copies, waits for them, and re-layouts: 7.63 us -> 0.04 us
  Pallas kernels: 26.7 us -> 25 us
    all_to_all x2 -> x0, waiting for transfers between devices: 38 us -> none  [the longest x1 30.6 us: exchange(): x = lax.all_to_all(x, ('sp', 'tp'), split_axis=0, concat_axis=0, tiled=True)]
    all_to_all x1 -> x2, blocking collectives: 43.7 us -> 73.1 us  [exchange(): x = lax.all_to_all(x, ('sp', 'tp'), split_axis=0, concat_axis=0, tiled=True)]
    pallas_call x6 -> x4, Pallas kernels: 26.7 us -> 15.4 us  [call(): pl.pallas_call(kernel, out_shape=out_shape, in_specs=specs, out_specs=jax...]
    all_to_all x0 -> x1, blocking collectives: none -> 10.7 us  [on_device(): heads = lax.all_to_all(attn, 'tp', split_axis=0, concat_axis=0, tiled=True)]
    pallas_call x0 -> x2, Pallas kernels: none -> 9.59 us  [the longest x1 8.1 us: on_device(): pl.pallas_call(attention_kernel, out_shape=(jax.ShapeDtypeStruct((4, quar...]
    all_to_all x2 -> x0, starting transfers between devices: 7.93 us -> none  [the longest x1 4.01 us: on_device(): heads = lax.all_to_all(attn, 'tp', split_axis=0, concat_axis=0, tiled=True)]
    unnamed x27 -> x14, local copies, waits for them, and re-layouts: 6.78 us -> 0.04 us
    ppermute x1, waiting for transfers between devices: 0.01 us -> 4.12 us  [on_device(): from_right = lax.ppermute(packed, 'sp', left)]
  transfers between devices with their start and end apart: 8 -> 6, of which waited for: 3 -> 2; matrix products, arithmetic and copies ran while one was open for 1% -> 0% of each run, Pallas kernels for 2% -> 4%
where the time goes in v3:
time: 130 us; the launch traced here: 129 us
  blocking collectives  83.9 us (65%)
  Pallas kernels  25 us (19%)
  starting transfers between devices  11.9 us (9%)
  waiting for transfers between devices  7.84 us (6%)
    all_to_all x2, blocking collectives, exchange(): x = lax.all_to_all(x, ('sp', 'tp'), split_axis=0, concat_axis=0, tiled=True)  73.1 us
    pallas_call x4, Pallas kernels, call(): pl.pallas_call(kernel, out_shape=out_shape, in_specs=specs, out_specs=jax...  15.4 us
    all_to_all x1, blocking collectives, on_device(): heads = lax.all_to_all(attn, 'tp', split_axis=0, concat_axis=0, tiled=True)  10.7 us
    pallas_call x1, Pallas kernels, on_device(): pl.pallas_call(attention_kernel, out_shape=(jax.ShapeDtypeStruct((4, quar...  8.1 us
    ppermute x1, starting transfers between devices, on_device(): from_right = lax.ppermute(packed, 'sp', left)  7.09 us
    ppermute x1, waiting for transfers between devices, on_device(): from_right = lax.ppermute(packed, 'sp', left)  4.12 us
    ppermute x1, waiting for transfers between devices, on_device(): from_left = lax.ppermute(packed, 'sp', right)  3.71 us
  transfers between devices with their start and end apart: 6, of which 2 were waited for; matrix products, arithmetic and copies ran while one was open for 0% of the time, Pallas kernels for 4%

profile of v3, /device:TPU:1, one launch (start us, length us, event | category | flops | bytes accessed | tf_op | source)
XLA Modules:
  0.0 129.4 jit_solution(5051299394237395014)
XLA Ops:
  0.0 0.0 copy-start.4
  0.0 0.1 multiply_cosine_fusion.1
  0.2 0.2 multiply_cosine_fusion
  0.4 0.1 fusion.7
  0.5 0.1 fusion.1
  0.6 1.5 %key_prep.1.own = bf16[1040,128]{1,0:T(8,128)(2,1)S(1)} custom-call(bf16[512,128]{1,0:T(8,128)(2,1)} %k_hbm.1, bf16[512,128]{1,0:T(8,128)(2,1)} %v_hbm.1, s32[4,128]{1,0:T(4,128)} %bitcast.23, f32[1,128]{1,0:T(1,128)} %bitcast.29, f32[2,8,128]{2,1,0:T(8,128)S(1)} %pad_maximum_fusion.5.row_ref, f32[2,64,128]{2,1,0:T(8,128)S(1)} %pad_maximum_fusion.col_ref), custom_call_target="tpu_custom_call" | custom-call | tf_op jit(solution)/shard_map/key_prep/pallas_call | solution.py:364
  2.1 7.1 %collective-permute-start.3 = (bf16[1040,128]{1,0:T(8,128)(2,1)S(1)}, bf16[1040,128]{1,0:T(8,128)(2,1)S(1)}, u32[]{:S(2)}, u32[]{:S(2)}) collective-permute-start(bf16[1040,128]{1,0:T(8,128)(2,1)S(1)} %key_prep.1.own), channel_id=1, source_target_pairs={{0,120},{4,124},{8,0},{12,4},{16,8},{20,12},{24,16},{28,20},{32,24... | collective-permute-start | bytes 798728 | tf_op jit(solution)/shard_map/ppermute | solution.py:388
  9.2 0.0 collective-permute-start.1
  9.2 1.0 collective-permute-start
  10.1 4.1 %collective-permute-done.3.b3 = bf16[1040,128]{1,0:T(8,128)(2,1)S(1)} collective-permute-done((bf16[1040,128]{1,0:T(8,128)(2,1)S(1)}, bf16[1040,128]{1,0:T(8,128)(2,1)S(1)}, u32[]{:S(2)}, u32[]{:S(2)}) %collective-permute-start.3) | collective-permute-done | bytes 266272 | tf_op jit(solution)/shard_map/ppermute | solution.py:388
  14.3 1.5 %collective-permute-start.4 = (bf16[1040,128]{1,0:T(8,128)(2,1)S(1)}, bf16[1040,128]{1,0:T(8,128)(2,1)S(1)}, u32[]{:S(2)}, u32[]{:S(2)}) collective-permute-start(bf16[1040,128]{1,0:T(8,128)(2,1)S(1)} %collective-permute-done.3.b3), channel_id=1, source_target_pairs={{0,4},{4,0},{8,12},{12,8},{16,20},{20,16},{24,28},{28,24},{32,36},... | collective-permute-start | bytes 798728 | tf_op jit(solution)/shard_map/ppermute | solution.py:392
  15.8 3.7 %collective-permute-done.1.b1 = bf16[1040,128]{1,0:T(8,128)(2,1)S(1)} collective-permute-done((bf16[1040,128]{1,0:T(8,128)(2,1)S(1)}, bf16[1040,128]{1,0:T(8,128)(2,1)S(1)}, u32[]{:S(2)}, u32[]{:S(2)}) %collective-permute-start.1) | collective-permute-done | bytes 266272 | tf_op jit(solution)/shard_map/ppermute | solution.py:387
  19.5 0.1 collective-permute-start.5
  19.6 2.2 %collective-permute-start.2 = (bf16[1040,128]{1,0:T(8,128)(2,1)S(1)}, bf16[1040,128]{1,0:T(8,128)(2,1)S(1)}, u32[]{:S(2)}, u32[]{:S(2)}) collective-permute-start(bf16[1040,128]{1,0:T(8,128)(2,1)S(1)} %collective-permute-done.1.b1), channel_id=1, source_target_pairs={{0,4},{4,0},{8,12},{12,8},{16,20},{20,16},{24,28},{28,24},{32,36},... | collective-permute-start | bytes 798728 | tf_op jit(solution)/shard_map/ppermute | solution.py:391
  21.8 4.6 %shard_map.136 = (bf16[512,512]{1,0:T(8,128)(2,1)S(1)}, f32[512,128]{1,0:T(8,128)S(1)}, s32[2,128]{1,0:T(2,128)S(1)}) custom-call(bf16[512,512]{1,0:T(8,128)(2,1)} %q_hbm.1, s32[2,128]{1,0:T(2,128)} %bitcast.28, s32[4,128]{1,0:T(4,128)} %bitcast.24, f32[1,128]{1,0:T(1,128)} %bitcast.30, f32[2,8,128]{2,1,0:T(8,128)S(1)} %pad_maximum_fusion.5.row_ref, ...), custom_call_target="tpu_custom_call" | custom-call | tf_op jit(solution)/shard_map/pallas_call | solution.py:344
  26.5 0.0 collective-permute-done.near
  26.5 0.0 collective-permute-done.4.b4
  26.5 0.0 collective-permute-done.5.far
  26.5 0.0 collective-permute-done.2.b2
  26.5 0.0 copy-done.4
  26.5 0.0 copy-start.3
  26.5 0.0 copy-start.5
  26.6 8.1 %attention.1 = (bf16[4,128,512]{2,1,0:T(8,128)(2,1)S(1)}, bf16[2048,2048]{1,0:T(8,128)(2,1)S(1)}) custom-call(s32[1]{0:T(128)} %bitcast.8.par_ref, s32[4,128]{1,0:T(4,128)S(1)} %bitcast.25, bf16[2048,2048]{1,0:T(8,128)(2,1)} %w_hbm.1, bf16[512,512]{1,0:T(8,128)(2,1)S(1)} %get-tuple-element.13.q_ref, f32[512,128]{1,0:T(8,128)S(1)} %get-tuple-element.14.qdoc_ref, ...), custom_call_target="tpu_custom_call" | custom-call | tf_op jit(solution)/shard_map/attention/pallas_call | solution.py:426
  34.7 10.7 %all_to_all.15.heads_ref = bf16[4,128,512]{2,1,0:T(8,128)(2,1)S(1)} all-to-all(bf16[4,128,512]{2,1,0:T(8,128)(2,1)S(1)} %get-tuple-element.15), channel_id=1, replica_groups=mesh['sp'=32,'tp'=4] {'tp'}, dimensions={0} | all-to-all | bytes 1048576 | tf_op jit(solution)/shard_map/all_to_all | solution.py:452
  45.4 0.0 copy-done.3
  45.4 0.0 copy-done.5
  45.4 0.0 copy-start.2
  45.4 3.0 %shard_map.137 = (bf16[128,2048]{1,0:T(8,128)(2,1)S(1)}, bf16[512,16,128]{2,1,0:T(8,128)(2,1)S(1)}) custom-call(s32[2,128]{1,0:T(2,128)S(1)} %get-tuple-element.12.slot_ref, bf16[4,128,512]{2,1,0:T(8,128)(2,1)S(1)} %all_to_all.15.heads_ref, bf16[2048,2048]{1,0:T(8,128)(2,1)S(1)} %get-tuple-element.16.w_ref, bf16[128,2048]{1,0:T(8,128)(2,1)S(1)} %copy-done.3, ...), custom_call_target="tpu_custom_call" | custom-call | tf_op jit(solution)/shard_map/pallas_call | solution.py:344
  48.4 0.0 copy-start
  48.4 0.0 copy-start.1
  48.4 39.0 %all_to_all.16 = bf16[128,64,128]{2,1,0:T(8,128)(2,1)S(1)} all-to-all(bf16[128,64,128]{2,1,0:T(8,128)(2,1)S(1)} %bitcast.22), channel_id=1, replica_groups=mesh['sp'=32,'tp'=4] {'sp','tp'}, dimensions={0} | all-to-all | bytes 4194304 | tf_op jit(solution)/shard_map/all_to_all | solution.py:467
  87.4 0.0 copy-done.2
  87.4 0.0 copy-done
  87.4 0.0 copy-done.1
  87.4 5.4 %shard_map.138 = bf16[512,16,128]{2,1,0:T(8,128)(2,1)S(1)} custom-call(bf16[512,16,128]{2,1,0:T(8,128)(2,1)S(1)} %bitcast.19, bf16[1,2048,512]{2,1,0:T(8,128)(2,1)S(1)} %copy-done, bf16[1,2048,512]{2,1,0:T(8,128)(2,1)S(1)} %copy-done.1, bf16[1,512,2048]{2,1,0:T(8,128)(2,1)S(1)} %copy-done.2), custom_call_target="tpu_custom_call" | custom-call | tf_op jit(solution)/shard_map/pallas_call | solution.py:344
  92.8 0.0 copy-start.6
  92.8 34.2 %all_to_all.17 = bf16[128,64,128]{2,1,0:T(8,128)(2,1)S(1)} all-to-all(bf16[128,64,128]{2,1,0:T(8,128)(2,1)S(1)} %bitcast.20), channel_id=1, replica_groups=mesh['sp'=32,'tp'=4] {'sp','tp'}, dimensions={0} | all-to-all | bytes 4194304 | tf_op jit(solution)/shard_map/all_to_all | solution.py:467
  127.0 0.0 copy-done.6
  127.0 2.4 %shard_map.139 = bf16[128,2048]{1,0:T(8,128)(2,1)} custom-call(s32[2,128]{1,0:T(2,128)S(1)} %get-tuple-element.12.slot_ref, f32[2,128]{1,0:T(2,128)S(1)} %bitcast.27, bf16[512,16,128]{2,1,0:T(8,128)(2,1)S(1)} %bitcast.21, bf16[128,2048]{1,0:T(8,128)(2,1)S(1)} %get-tuple-element.18.hid_ref), custom_call_target="tpu_custom_call" | custom-call | tf_op jit(solution)/shard_map/pallas_call | solution.py:344
  (8 shorter events, 0.1 us)
Async XLA Ops:
  0.0 26.5 %copy-start.4 = (s32[512]{0:T(512)S(1)}, s32[512]{0:T(512)}, u32[]{:S(2)}) copy-start(s32[512]{0:T(512)} %param.20) | copy-start | bytes 6148
  2.1 12.2 %collective-permute-start.3 = (bf16[1040,128]{1,0:T(8,128)(2,1)S(1)}, bf16[1040,128]{1,0:T(8,128)(2,1)S(1)}, u32[]{:S(2)}, u32[]{:S(2)}) collective-permute-start(bf16[1040,128]{1,0:T(8,128)(2,1)S(1)} %key_prep.1.own), channel_id=1, source_target_pairs={{0,120},{4,124},{8,0},{12,4},{16,8},{20,12},{24,16},{28,20},{32,24... | collective-permute-start | bytes 798728 | tf_op jit(solution)/shard_map/ppermute | solution.py:388
  9.2 10.3 %collective-permute-start.1 = (bf16[1040,128]{1,0:T(8,128)(2,1)S(1)}, bf16[1040,128]{1,0:T(8,128)(2,1)S(1)}, u32[]{:S(2)}, u32[]{:S(2)}) collective-permute-start(bf16[1040,128]{1,0:T(8,128)(2,1)S(1)} %key_prep.1.own), channel_id=1, source_target_pairs={{0,8},{4,12},{8,16},{12,20},{16,24},{20,28},{24,32},{28,36},{32,40... | collective-permute-start | bytes 798728 | tf_op jit(solution)/shard_map/ppermute | solution.py:387
  9.2 17.3 %collective-permute-start = (bf16[1040,128]{1,0:T(8,128)(2,1)S(1)}, bf16[1040,128]{1,0:T(8,128)(2,1)S(1)}, u32[]{:S(2)}, u32[]{:S(2)}) collective-permute-start(bf16[1040,128]{1,0:T(8,128)(2,1)S(1)} %key_prep.1.own), channel_id=1, source_target_pairs={{0,4},{4,0},{8,12},{12,8},{16,20},{20,16},{24,28},{28,24},{32,36},... | collective-permute-start | bytes 798728 | tf_op jit(solution)/shard_map/ppermute | solution.py:389
  14.3 12.2 %collective-permute-start.4 = (bf16[1040,128]{1,0:T(8,128)(2,1)S(1)}, bf16[1040,128]{1,0:T(8,128)(2,1)S(1)}, u32[]{:S(2)}, u32[]{:S(2)}) collective-permute-start(bf16[1040,128]{1,0:T(8,128)(2,1)S(1)} %collective-permute-done.3.b3), channel_id=1, source_target_pairs={{0,4},{4,0},{8,12},{12,8},{16,20},{20,16},{24,28},{28,24},{32,36},... | collective-permute-start | bytes 798728 | tf_op jit(solution)/shard_map/ppermute | solution.py:392
  19.5 7.0 %collective-permute-start.5 = (bf16[1040,128]{1,0:T(8,128)(2,1)S(1)}, bf16[1040,128]{1,0:T(8,128)(2,1)S(1)}, u32[]{:S(2)}, u32[]{:S(2)}) collective-permute-start(bf16[1040,128]{1,0:T(8,128)(2,1)S(1)} %broadcast_select_fusion), channel_id=1, source_target_pairs={{0,124},{4,8},{8,4},{12,16},{16,12},{20,24},{24,20},{28,32},{32,28... | collective-permute-start | bytes 798728 | tf_op jit(solution)/shard_map/ppermute | solution.py:390
  19.6 6.9 %collective-permute-start.2 = (bf16[1040,128]{1,0:T(8,128)(2,1)S(1)}, bf16[1040,128]{1,0:T(8,128)(2,1)S(1)}, u32[]{:S(2)}, u32[]{:S(2)}) collective-permute-start(bf16[1040,128]{1,0:T(8,128)(2,1)S(1)} %collective-permute-done.1.b1), channel_id=1, source_target_pairs={{0,4},{4,0},{8,12},{12,8},{16,20},{20,16},{24,28},{28,24},{32,36},... | collective-permute-start | bytes 798728 | tf_op jit(solution)/shard_map/ppermute | solution.py:391
  26.5 18.9 %copy-start.3 = (bf16[128,2048]{1,0:T(8,128)(2,1)S(1)}, bf16[128,2048]{1,0:T(8,128)(2,1)}, u32[]{:S(2)}) copy-start(bf16[128,2048]{1,0:T(8,128)(2,1)} %res_ref.1) | copy-start | bytes 1572868
  26.5 18.9 %copy-start.5 = (f32[2048]{0:T(1024)S(1)}, f32[2048]{0:T(1024)}, u32[]{:S(2)}) copy-start(f32[2048]{0:T(1024)} %param.22) | copy-start | bytes 24580
  45.4 42.0 %copy-start.2 = (bf16[1,512,2048]{2,1,0:T(8,128)(2,1)S(1)}, bf16[1,512,2048]{2,1,0:T(8,128)(2,1)}, u32[]{:S(2)}) copy-start(bf16[1,512,2048]{2,1,0:T(8,128)(2,1)} %down_ref.1) | copy-start | bytes 6291460
  48.4 39.0 %copy-start = (bf16[1,2048,512]{2,1,0:T(8,128)(2,1)S(1)}, bf16[1,2048,512]{2,1,0:T(8,128)(2,1)}, u32[]{:S(2)}) copy-start(bf16[1,2048,512]{2,1,0:T(8,128)(2,1)} %gate_ref.1) | copy-start | bytes 6291460
  48.4 39.0 %copy-start.1 = (bf16[1,2048,512]{2,1,0:T(8,128)(2,1)S(1)}, bf16[1,2048,512]{2,1,0:T(8,128)(2,1)}, u32[]{:S(2)}) copy-start(bf16[1,2048,512]{2,1,0:T(8,128)(2,1)} %up_ref.1) | copy-start | bytes 6291460
  92.8 34.2 %copy-start.6 = (f32[128,2]{0,1:T(2,128)S(1)}, f32[128,2]{0,1:T(2,128)}, u32[]{:S(2)}) copy-start(f32[128,2]{0,1:T(2,128)} %param.24) | copy-start | bytes 3076

commit v4 on v3

--- a/solution.py
+++ b/solution.py
@@ -14,7 +14,6 @@
 norm_eps = 1e-06
 rope_base = 10000.0
 LOW = -1e30
-KB = 512
 DOC_ROWS = 16
 VMEM = pltpu.VMEM
 
@@ -60,7 +59,7 @@
         copy.start()
     for copy in copies[:3]:
         copy.wait()
-    docs = doc_ref[...].astype(jnp.float32).astype(jnp.bfloat16)
+    docs = (doc_ref[...].astype(jnp.float32) + 1.0).astype(jnp.bfloat16)
     pad = jnp.zeros((DOC_ROWS - docs.shape[0], HEAD), jnp.bfloat16)
     out_ref[2 * rows :, :] = jnp.concatenate([docs, pad], 0)
     gain = gain_ref[...]
@@ -96,7 +95,7 @@
             lanes = slice(h * HEAD, (h + 1) * HEAD)
             out_ref[span, lanes] = norm_rotate(q_ref[span, lanes], gain, cos_full, sin_full)
     for t in range(doc_ref.shape[0]):
-        line = jnp.broadcast_to(doc_ref[t : t + 1, :].astype(jnp.float32), (HEAD, HEAD))
+        line = jnp.broadcast_to(doc_ref[t : t + 1, :].astype(jnp.float32) + 1.0, (HEAD, HEAD))
         qdoc_ref[t * HEAD : (t + 1) * HEAD, :] = line.T
     choices, tokens = ids_ref.shape
     sub = lax.broadcasted_iota(jnp.int32, (HEAD, tokens), 0)
@@ -115,150 +114,186 @@
         before = before + jnp.sum(hit, axis=1, keepdims=True)
 
 
-def attention_kernel(
-    par_ref, edge_ref, w_hbm, q_ref, qdoc_ref, own, near, b1, b2, b3, b4, far, out_ref, w_ref,
-    k_scr, v_scr, d_scr, s_even, s_odd, mx_even, mx_odd, l_scr, acc_scr, sem,
-):
-    fetch = pltpu.make_async_copy(w_hbm, w_ref, sem)
-    fetch.start()
+def attend(
+    quarters, edge_ref, q_ref, qdoc_ref, sources, state, out_refs,
+    k_ref, v_ref, d_ref, list_ref, s_even, s_odd, mx_even, mx_odd, l_scr, acc_scr,
+):
     rows, width = q_ref.shape
     heads = width // HEAD
-    par = par_ref[0]
     tiles = rows // HEAD
-    slots = [
-        (own, 3 + par), (near, 4 - par), (b1, 1 + par), (b2, 2 - par),
-        (b3, 5 + par), (b4, 6 - par), (far, 7 * par),
-    ]
-    for src, slot in slots:
-        at = pl.multiple_of(slot * rows, rows)
-        k_scr[pl.ds(at, rows), :] = src[0:rows, :]
-        v_scr[pl.ds(at, rows), :] = src[rows : 2 * rows, :]
+    block = rows // 4
+    pieces = block // 16
+    total = len(quarters)
+    scale = HEAD ** (-0.5) * 1.4426950408889634
+    spans = []
+    for n, src in enumerate(sources):
+        k_ref[n] = src[0:rows, :]
+        v_ref[n] = src[rows : 2 * rows, :]
         docs = src[2 * rows : 2 * rows + DOC_ROWS, :].astype(jnp.float32)
         for t in range(tiles):
-            d_scr[slot * tiles + t] = jnp.broadcast_to(docs[t : t + 1, :], (8, HEAD))
-    for slot in (7 - 7 * par, 8):
-        at = pl.multiple_of(slot * rows, rows)
-        k_scr[pl.ds(at, rows), :] = jnp.zeros((rows, HEAD), jnp.bfloat16)
-        v_scr[pl.ds(at, rows), :] = jnp.zeros((rows, HEAD), jnp.bfloat16)
-        for t in range(tiles):
-            d_scr[slot * tiles + t] = jnp.full((8, HEAD), -1.0, jnp.float32)
-    docs = d_scr[...]
-    place = lax.broadcasted_iota(jnp.int32, docs.shape, 0) * HEAD + lax.broadcasted_iota(
-        jnp.int32, docs.shape, 2
-    )
-    scale = HEAD ** (-0.5) * 1.4426950408889634
-    block = rows // 4
-    parts = KB // HEAD
-    pieces = block // 16
-    starts, counts = [], []
-    for qs in range(4):
-        first = edge_ref[qs, 0].astype(jnp.float32)
-        last = edge_ref[qs, block - 1].astype(jnp.float32)
-        low = jnp.min(jnp.where(docs == first, place, 8 * rows))
-        high = jnp.max(jnp.where(docs == last, place, -1))
-        start = (low // HEAD) * HEAD
-        starts.append(start)
-        counts.append((high - start) // KB + 1)
+            d_ref[n * tiles + t] = jnp.broadcast_to(docs[t : t + 1, :], (8, HEAD))
+        spans.append((jnp.min(docs[0:1, :]), jnp.max(docs[tiles - 1 : tiles, :])))
+    counts = []
+    for n, qs in enumerate(quarters):
+        first = edge_ref[qs, 0].astype(jnp.float32) + 1.0
+        last = edge_ref[qs, block - 1].astype(jnp.float32) + 1.0
+        count = jnp.int32(0)
+        for m in range(len(sources) + 1):
+            list_ref[n, m] = 0
+        for m, (low, high) in enumerate(spans):
+            list_ref[n, count] = m
+            count = count + ((low <= last) & (high >= first)).astype(jnp.int32)
+        counts.append(count)
     s_refs = (s_even, s_odd)
     mx_refs = (mx_even, mx_odd)
-    spare = s_even.shape[0] - 2
+    spare = len(sources)
     for ref in s_refs:
         ref[spare] = jnp.full(ref.shape[1:], LOW, jnp.float32)
 
-    def scores(qs, i):
-        s_ref, mx_ref = s_refs[qs % 2], mx_refs[qs % 2]
-        at = pl.multiple_of(jnp.minimum(starts[qs] + i * KB, 8 * rows), HEAD)
-        index = jnp.where(i < counts[qs], i, spare + 1)
-        base = qs * block
+    def scores(n, i):
+        s_ref, mx_ref = s_refs[n % 2], mx_refs[n % 2]
+        slot = list_ref[n, i]
+        index = jnp.where(i < counts[n], i, spare + 1)
+
+        def line(r):
+            return pl.ds(pl.multiple_of(quarters[n] * block + r * 16, 16), 16)
+
         q4 = jnp.concatenate(
             [
-                q_ref[base + r * 16 : base + (r + 1) * 16, h * HEAD : (h + 1) * HEAD]
+                q_ref[line(r), h * HEAD : (h + 1) * HEAD]
                 for r in range(pieces)
                 for h in range(heads)
             ],
             0,
         )
         s = lax.dot_general(
-            q4, k_scr[pl.ds(at, KB), :], (((1,), (1,)), ((), ())),
-            preferred_element_type=jnp.float32,
-        )
-        tile = at // HEAD
-        key_docs = [d_scr[tile + t] for t in range(parts)]
+            q4, k_ref[slot], (((1,), (1,)), ((), ())), preferred_element_type=jnp.float32
+        )
+        key_docs = [d_ref[slot * tiles + t] for t in range(tiles)]
         key_docs = [jnp.concatenate([d, d], 0) for d in key_docs]
         for r in range(pieces):
-            qdoc = qdoc_ref[base + r * 16 : base + (r + 1) * 16, :]
+            qdoc = qdoc_ref[line(r), :]
             keep = [qdoc == d for d in key_docs]
             for h in range(heads):
                 band = slice((r * heads + h) * 16, (r * heads + h + 1) * 16)
                 top = mx_ref[band, :]
-                for t in range(parts):
+                for t in range(tiles):
                     lanes = slice(t * HEAD, (t + 1) * HEAD)
                     part = jnp.where(keep[t], s[band, lanes], LOW)
                     s_ref[index, band, lanes] = part
                     top = jnp.maximum(top, part)
                 mx_ref[band, :] = top
 
-    def weigh(qs, i):
-        s_ref, mx_ref = s_refs[qs % 2], mx_refs[qs % 2]
-        at = pl.multiple_of(jnp.minimum(starts[qs] + i * KB, 8 * rows), HEAD)
-        index = jnp.where(i < counts[qs], i, spare)
+    def weigh(n, i):
+        s_ref, mx_ref = s_refs[n % 2], mx_refs[n % 2]
+        slot = list_ref[n, i]
+        index = jnp.where(i < counts[n], i, spare)
         top = mx_ref[...]
         probs = []
-        total = l_scr[...]
-        for t in range(parts):
+        run = l_scr[...]
+        for t in range(tiles):
             e = jnp.exp2(s_ref[index, :, t * HEAD : (t + 1) * HEAD] * scale - top)
-            total = total + e
+            run = run + e
             probs.append(e.astype(jnp.bfloat16))
-        l_scr[...] = total
+        l_scr[...] = run
         acc_scr[...] += jnp.dot(
-            jnp.concatenate(probs, axis=1), v_scr[pl.ds(at, KB), :],
-            preferred_element_type=jnp.float32,
-        )
-
-    for step in range(5):
+            jnp.concatenate(probs, axis=1), v_ref[slot], preferred_element_type=jnp.float32
+        )
+
+    m_ref, l_ref, acc_ref = state
+    for step in range(total + 1):
         trip = counts[step] if step == 0 else counts[step - 1]
-        if 0 < step < 4:
+        if 0 < step < total:
             trip = jnp.maximum(trip, counts[step])
-        if step < 4:
-            mx_refs[step % 2][...] = jnp.full(mx_even.shape, LOW, jnp.float32)
+        if step < total:
+            if out_refs is None:
+                mx_refs[step % 2][...] = jnp.full(mx_even.shape, LOW, jnp.float32)
+            else:
+                mx_refs[step % 2][...] = m_ref[quarters[step]]
         if step > 0:
-            l_scr[...] = jnp.zeros(l_scr.shape, jnp.float32)
-            acc_scr[...] = jnp.zeros(acc_scr.shape, jnp.float32)
+            if out_refs is None:
+                l_scr[...] = jnp.zeros(l_scr.shape, jnp.float32)
+                acc_scr[...] = jnp.zeros(acc_scr.shape, jnp.float32)
+            else:
+                before = quarters[step - 1]
+                shrink = jnp.exp2(m_ref[before] * scale - mx_refs[(step - 1) % 2][...])
+                l_scr[...] = l_ref[before] * shrink
+                acc_scr[...] = acc_ref[before] * shrink
 
         def body(i, carry, step=step):
             if step > 0:
                 weigh(step - 1, i)
-            if step < 4:
+            if step < total:
                 scores(step, i)
             return carry
 
         lax.fori_loop(0, trip, body, 0)
-        if step < 4:
+        if step < total:
             ref = mx_refs[step % 2]
-            ref[...] = jnp.broadcast_to(
-                jnp.max(ref[...], axis=1, keepdims=True) * scale, ref.shape
-            )
-        if step > 0:
+            top = jnp.broadcast_to(jnp.max(ref[...], axis=1, keepdims=True), ref.shape)
+            if out_refs is None:
+                m_ref[quarters[step]] = top
+            ref[...] = top * scale
+        if step > 0 and out_refs is None:
+            l_ref[quarters[step - 1]] = l_scr[...]
+            acc_ref[quarters[step - 1]] = acc_scr[...]
+        elif step > 0:
             den = jnp.sum(l_scr[...], axis=1, keepdims=True)
             res = (acc_scr[...] / den).astype(jnp.bfloat16)
             for r in range(pieces):
                 for h in range(heads):
                     at = (r * heads + h) * 16
-                    out_ref[step - 1, r * 16 : (r + 1) * 16, h * HEAD : (h + 1) * HEAD] = res[
+                    out_refs[step - 1][r * 16 : (r + 1) * 16, h * HEAD : (h + 1) * HEAD] = res[
                         at : at + 16, :
                     ]
+
+
+def early_attention(
+    edge_ref, w_hbm, q_ref, qdoc_ref, own, near, b1, b3, m_ref, l_ref, acc_ref, w_ref, *scratch
+):
+    fetch = pltpu.make_async_copy(w_hbm, w_ref, scratch[-1])
+    fetch.start()
+    state = (m_ref, l_ref, acc_ref)
+    sources = (own, near, b1, b3)
+    attend(range(4), edge_ref, q_ref, qdoc_ref, sources, state, None, *scratch[:-1])
     fetch.wait()
 
 
-def project_kernel(slot_ref, heads_ref, w_ref, res_ref, gain_ref, hid_ref, out_ref, n_scr):
-    groups, rows, part = heads_ref.shape
-    width = res_ref.shape[1]
+def late_attention(
+    where_ref, edge_ref, q_ref, qdoc_ref, b2, b4, far, m_ref, l_ref, acc_ref, out_a, out_b,
+    *scratch, ahead,
+):
+    quarters = [(where_ref[1] + k) % 4 for k in ahead]
+    state = (m_ref, l_ref, acc_ref)
+    sources = (b2, b4, far)
+    attend(quarters, edge_ref, q_ref, qdoc_ref, sources, state, (out_a, out_b), *scratch)
+
+
+def weight_rows(w_ref, group, part):
+    return w_ref[pl.ds(pl.multiple_of(group * part, part), part), :]
+
+
+def project_part_kernel(where_ref, h0_ref, h2_ref, h3_ref, w_ref, acc_ref):
+    part = h0_ref.shape[1]
+    home = where_ref[1]
+    acc = jnp.dot(h0_ref[...], weight_rows(w_ref, home, part), preferred_element_type=jnp.float32)
+    for ref, back in ((h2_ref, 2), (h3_ref, 3)):
+        acc += jnp.dot(
+            ref[...], weight_rows(w_ref, (home + 4 - back) % 4, part),
+            preferred_element_type=jnp.float32,
+        )
+    acc_ref[...] = acc
+
+
+def project_kernel(
+    where_ref, slot_ref, h1_ref, acc_ref, w_ref, res_ref, gain_ref, hid_ref, out_ref, n_scr
+):
+    rows, width = res_ref.shape
     fold = width // HEAD
-    acc = jnp.dot(heads_ref[0], w_ref[0:part, :], preferred_element_type=jnp.float32)
-    for g in range(1, groups):
-        acc += jnp.dot(
-            heads_ref[g], w_ref[g * part : (g + 1) * part, :], preferred_element_type=jnp.float32
-        )
+    acc = acc_ref[...] + jnp.dot(
+        h1_ref[...], weight_rows(w_ref, (where_ref[1] + 3) % 4, h1_ref.shape[1]),
+        preferred_element_type=jnp.float32,
+    )
     hidden = (res_ref[...].astype(jnp.float32) + acc).astype(jnp.bfloat16)
     hid_ref[...] = hidden
     wide = hidden.astype(jnp.float32)
@@ -420,46 +455,74 @@
             in_hbm(query_gain.reshape(1, HEAD)), row_tab, col_tab,
         ),
     )
-    anywhere = pl.BlockSpec(memory_space=pltpu.HBM)
-    smem = pl.BlockSpec(memory_space=pltpu.SMEM)
-    vmem = pl.BlockSpec(memory_space=VMEM)
-    attn, weight_near = pl.pallas_call(
-        attention_kernel,
-        out_shape=(
-            jax.ShapeDtypeStruct((4, quarter, width), bf16),
-            jax.ShapeDtypeStruct(output_weight.shape, bf16),
-        ),
-        in_specs=[smem, smem, anywhere] + [vmem] * 9,
-        out_specs=(vmem, vmem),
-        scratch_shapes=[
-            VMEM((9 * rows, HEAD), bf16),
-            VMEM((9 * rows, HEAD), bf16),
-            VMEM((9 * rows // HEAD, 8, HEAD), f32),
-            VMEM((10, rows, KB), f32),
-            VMEM((10, rows, KB), f32),
+    where = jnp.stack([par, lax.axis_index("tp")]).astype(jnp.int32)
+
+    def attention_scratch(count):
+        return (
+            VMEM((count, rows, HEAD), bf16),
+            VMEM((count, rows, HEAD), bf16),
+            VMEM((count * rows // HEAD, 8, HEAD), f32),
+            pltpu.SMEM((4, count + 1), jnp.int32),
+            VMEM((count + 2, rows, rows), f32),
+            VMEM((count + 2, rows, rows), f32),
             VMEM((rows, HEAD), f32),
             VMEM((rows, HEAD), f32),
             VMEM((rows, HEAD), f32),
             VMEM((rows, HEAD), f32),
-            pltpu.SemaphoreType.DMA,
-        ],
-        name="attention",
-        compiler_params=pltpu.CompilerParams(vmem_limit_bytes=40 * 2**20),
-    )(
-        par.reshape(1).astype(jnp.int32), doc_lines, in_hbm(output_weight), query_norm, query_doc, packed,
-        near, from_left, left_pair, from_right, right_pair, far,
-    )
-    heads = lax.all_to_all(attn, "tp", split_axis=0, concat_axis=0, tiled=True)
+        )
+
+    part_shape = jax.ShapeDtypeStruct((quarter, width), bf16)
+    state_shape = jax.ShapeDtypeStruct((4, rows, HEAD), f32)
+    top, sums, values, weight_near = call(
+        early_attention,
+        (
+            state_shape,
+            state_shape,
+            state_shape,
+            jax.ShapeDtypeStruct(output_weight.shape, bf16),
+        ),
+        24,
+        scratch=attention_scratch(4) + (pltpu.SemaphoreType.DMA,),
+        smem=1,
+        hbm=1,
+        args=(
+            doc_lines, in_hbm(output_weight), query_norm, query_doc, packed, near, from_left,
+            from_right,
+        ),
+    )
+
+    def late(ahead):
+        return call(
+            functools.partial(late_attention, ahead=ahead), (part_shape, part_shape), 24,
+            scratch=attention_scratch(3), smem=2,
+            args=(
+                where, doc_lines, query_norm, query_doc, left_pair, right_pair, far, top, sums,
+                values,
+            ),
+        )
+
+    def ahead_by(x, k):
+        return lax.ppermute(x, "tp", [(i, (i + k) % 4) for i in range(4)])
+
+    ahead_2, ahead_3 = late((2, 3))
+    heads_2 = ahead_by(ahead_2, 2)
+    heads_3 = ahead_by(ahead_3, 3)
+    ahead_1, at_home = late((1, 0))
+    heads_1 = ahead_by(ahead_1, 1)
+    partial = call(
+        project_part_kernel, jax.ShapeDtypeStruct((token_rows, wide), f32), 16,
+        smem=1, args=(where, at_home, heads_2, heads_3, weight_near),
+    )
     hidden, outgoing = call(
         project_kernel,
         (
             jax.ShapeDtypeStruct((token_rows, wide), bf16),
             jax.ShapeDtypeStruct((slots, fold, HEAD), bf16),
         ),
-        24,
+        16,
         scratch=(VMEM((token_rows * fold, HEAD), f32),),
-        smem=1,
-        args=(slot, heads, weight_near, residual, norm_gain.reshape(1, wide)),
+        smem=2,
+        args=(where, slot, heads_1, partial, weight_near, residual, norm_gain.reshape(1, wide)),
     )
 
     def exchange(x):

time: 130 us -> 128 us (0.985)
  blocking collectives: 83.9 us -> 72.5 us
  starting transfers between devices: 11.9 us -> 17.7 us
  Pallas kernels: 25 us -> 28.7 us
    pallas_call x4 -> x8, Pallas kernels: 15.4 us -> 27.3 us  [call(): pl.pallas_call(kernel, out_shape=out_shape, in_specs=specs, out_specs=jax...]
    all_to_all x1 -> x0, blocking collectives: 10.7 us -> none  [on_device(): heads = lax.all_to_all(attn, 'tp', split_axis=0, concat_axis=0, tiled=True)]
    pallas_call x1 -> x0, Pallas kernels: 8.1 us -> none  [on_device(): pl.pallas_call(attention_kernel, out_shape=(jax.ShapeDtypeStruct((4, quar...]
    ppermute x0 -> x3, starting transfers between devices: none -> 4.56 us  [ahead_by(): return lax.ppermute(x, 'tp', [(i, (i + k) % 4) for i in range(4)])]
    ppermute x1, waiting for transfers between devices: 4.12 us -> 0.01 us  [on_device(): from_right = lax.ppermute(packed, 'sp', left)]
    ppermute x0 -> x3, waiting for transfers between devices: none -> 3 us  [ahead_by(): return lax.ppermute(x, 'tp', [(i, (i + k) % 4) for i in range(4)])]
    ppermute x1, starting transfers between devices: 2.2 us -> 4.96 us  [on_device(): left_pair = lax.ppermute(from_left, 'sp', swap)]
    ppermute x1, starting transfers between devices: 0.01 us -> 2.18 us  [on_device(): from_left = lax.ppermute(packed, 'sp', right)]
  transfers between devices with their start and end apart: 6 -> 9, of which waited for: 2 -> 3; matrix products, arithmetic and copies ran while one was open for 0% -> 0% of each run, Pallas kernels for 4% -> 12%
where the time goes in v4:
time: 128 us
  blocking collectives  72.5 us (57%)
  Pallas kernels  28.7 us (22%)
  starting transfers between devices  17.7 us (14%)
  waiting for transfers between devices  8.08 us (6%)
    all_to_all x2, blocking collectives, exchange(): x = lax.all_to_all(x, ('sp', 'tp'), split_axis=0, concat_axis=0, tiled=True)  72.5 us
    pallas_call x8, Pallas kernels, call(): pl.pallas_call(kernel, out_shape=out_shape, in_specs=specs, out_specs=jax...  27.3 us
    ppermute x1, waiting for transfers between devices, on_device(): from_left = lax.ppermute(packed, 'sp', right)  5.06 us
    ppermute x1, starting transfers between devices, on_device(): from_right = lax.ppermute(packed, 'sp', left)  4.99 us
    ppermute x1, starting transfers between devices, on_device(): left_pair = lax.ppermute(from_left, 'sp', swap)  4.96 us
    ppermute x3, starting transfers between devices, ahead_by(): return lax.ppermute(x, 'tp', [(i, (i + k) % 4) for i in range(4)])  4.56 us
    ppermute x3, waiting for transfers between devices, ahead_by(): return lax.ppermute(x, 'tp', [(i, (i + k) % 4) for i in range(4)])  3 us
  transfers between devices with their start and end apart: 9, of which 3 were waited for; matrix products, arithmetic and copies ran while one was open for 0% of the time, Pallas kernels for 12%

profile of v4, /device:TPU:1, one launch (start us, length us, event | category | flops | bytes accessed | tf_op | source)
XLA Modules:
  0.0 127.9 jit_solution(1194371928134716777)
XLA Ops:
  0.0 0.0 copy-start.4
  0.0 0.1 multiply_cosine_fusion.1
  0.2 0.2 multiply_cosine_fusion
  0.4 0.1 fusion.7
  0.5 0.1 fusion.1
  0.6 1.5 %key_prep.1.own = bf16[1040,128]{1,0:T(8,128)(2,1)S(1)} custom-call(bf16[512,128]{1,0:T(8,128)(2,1)} %k_hbm.1, bf16[512,128]{1,0:T(8,128)(2,1)} %v_hbm.1, s32[4,128]{1,0:T(4,128)} %bitcast.24, f32[1,128]{1,0:T(1,128)} %bitcast.32, f32[2,8,128]{2,1,0:T(8,128)S(1)} %pad_maximum_fusion.5.row_ref, f32[2,64,128]{2,1,0:T(8,128)S(1)} %pad_maximum_fusion.col_ref), custom_call_target="tpu_custom_call" | custom-call | tf_op jit(solution)/shard_map/key_prep/pallas_call | solution.py:399
  2.1 2.2 %collective-permute-start = (bf16[1040,128]{1,0:T(8,128)(2,1)S(1)}, bf16[1040,128]{1,0:T(8,128)(2,1)S(1)}, u32[]{:S(2)}, u32[]{:S(2)}) collective-permute-start(bf16[1040,128]{1,0:T(8,128)(2,1)S(1)} %key_prep.1.own), channel_id=1, source_target_pairs={{0,8},{4,12},{8,16},{12,20},{16,24},{20,28},{24,32},{28,36},{32,40... | collective-permute-start | bytes 798728 | tf_op jit(solution)/shard_map/ppermute | solution.py:422
  4.3 5.0 %collective-permute-start.2 = (bf16[1040,128]{1,0:T(8,128)(2,1)S(1)}, bf16[1040,128]{1,0:T(8,128)(2,1)S(1)}, u32[]{:S(2)}, u32[]{:S(2)}) collective-permute-start(bf16[1040,128]{1,0:T(8,128)(2,1)S(1)} %key_prep.1.own), channel_id=1, source_target_pairs={{0,120},{4,124},{8,0},{12,4},{16,8},{20,12},{24,16},{28,20},{32,24... | collective-permute-start | bytes 798728 | tf_op jit(solution)/shard_map/ppermute | solution.py:423
  9.3 1.0 collective-permute-start.5
  10.2 5.1 %collective-permute-done.b1 = bf16[1040,128]{1,0:T(8,128)(2,1)S(1)} collective-permute-done((bf16[1040,128]{1,0:T(8,128)(2,1)S(1)}, bf16[1040,128]{1,0:T(8,128)(2,1)S(1)}, u32[]{:S(2)}, u32[]{:S(2)}) %collective-permute-start) | collective-permute-done | bytes 266272 | tf_op jit(solution)/shard_map/ppermute | solution.py:422
  15.3 0.0 collective-permute-done.2.b3
  15.3 0.1 collective-permute-start.4
  15.4 5.0 %collective-permute-start.1 = (bf16[1040,128]{1,0:T(8,128)(2,1)S(1)}, bf16[1040,128]{1,0:T(8,128)(2,1)S(1)}, u32[]{:S(2)}, u32[]{:S(2)}) collective-permute-start(bf16[1040,128]{1,0:T(8,128)(2,1)S(1)} %collective-permute-done.b1), channel_id=1, source_target_pairs={{0,4},{4,0},{8,12},{12,8},{16,20},{20,16},{24,28},{28,24},{32,36},... | collective-permute-start | bytes 798728 | tf_op jit(solution)/shard_map/ppermute | solution.py:426
  20.4 0.0 collective-permute-start.3
  20.4 4.6 %shard_map.136 = (bf16[512,512]{1,0:T(8,128)(2,1)S(1)}, f32[512,128]{1,0:T(8,128)S(1)}, s32[2,128]{1,0:T(2,128)S(1)}) custom-call(bf16[512,512]{1,0:T(8,128)(2,1)} %q_hbm.1, s32[2,128]{1,0:T(2,128)} %bitcast.31, s32[4,128]{1,0:T(4,128)} %bitcast.25, f32[1,128]{1,0:T(1,128)} %bitcast.33, f32[2,8,128]{2,1,0:T(8,128)S(1)} %pad_maximum_fusion.5.row_ref, ...), custom_call_target="tpu_custom_call" | custom-call | tf_op jit(solution)/shard_map/pallas_call | solution.py:379
  25.0 0.1 pad_add_fusion.where_ref
  25.1 0.0 collective-permute-done.5.near
  25.1 0.0 copy-done.4
  25.1 6.4 %shard_map.137 = (f32[4,512,128]{2,1,0:T(8,128)S(1)}, f32[4,512,128]{2,1,0:T(8,128)S(1)}, f32[4,512,128]{2,1,0:T(8,128)S(1)}, bf16[2048,2048]{1,0:T(8,128)(2,1)S(1)}) custom-call(s32[4,128]{1,0:T(4,128)S(1)} %bitcast.26, bf16[2048,2048]{1,0:T(8,128)(2,1)} %w_hbm.1, bf16[512,512]{1,0:T(8,128)(2,1)S(1)} %get-tuple-element.19.q_ref, ...), custom_call_target="tpu_custom_call" | custom-call | tf_op jit(solution)/shard_map/pallas_call | solution.py:379
  31.6 0.0 collective-permute-done.4.far
  31.6 0.0 collective-permute-done.1.b2
  31.6 0.0 collective-permute-done.3.b4
  31.6 2.5 %shard_map.139 = (bf16[128,512]{1,0:T(8,128)(2,1)S(1)}, bf16[128,512]{1,0:T(8,128)(2,1)S(1)}) custom-call(s32[2]{0:T(128)S(1)} %pad_add_fusion.where_ref, s32[4,128]{1,0:T(4,128)S(1)} %bitcast.27, bf16[512,512]{1,0:T(8,128)(2,1)S(1)} %get-tuple-element.19.q_ref, f32[512,128]{1,0:T(8,128)S(1)} %get-tuple-element.20.qdoc_ref, ...), custom_call_target="tpu_custom_call" | custom-call | tf_op jit(solution)/shard_map/pallas_call | solution.py:379
  34.1 2.5 %collective-permute-start.7 = (bf16[128,512]{1,0:T(8,128)(2,1)S(1)}, bf16[128,512]{1,0:T(8,128)(2,1)S(1)}, u32[]{:S(2)}, u32[]{:S(2)}) collective-permute-start(bf16[128,512]{1,0:T(8,128)(2,1)S(1)} %get-tuple-element.26), channel_id=1, source_target_pairs={{0,2},{1,3},{2,0},{3,1},{4,6},{5,7},{6,4},{7,5},{8,10},{9,11},{10,... | collective-permute-start | bytes 393224 | tf_op jit(solution)/shard_map/ppermute | solution.py:505
  36.6 0.8 collective-permute-start.8
  37.5 2.1 %shard_map.138 = (bf16[128,512]{1,0:T(8,128)(2,1)S(1)}, bf16[128,512]{1,0:T(8,128)(2,1)S(1)}) custom-call(s32[2]{0:T(128)S(1)} %pad_add_fusion.where_ref, s32[4,128]{1,0:T(4,128)S(1)} %bitcast.28, bf16[512,512]{1,0:T(8,128)(2,1)S(1)} %get-tuple-element.19.q_ref, f32[512,128]{1,0:T(8,128)S(1)} %get-tuple-element.20.qdoc_ref, ...), custom_call_target="tpu_custom_call" | custom-call | tf_op jit(solution)/shard_map/pallas_call | solution.py:379
  39.6 1.2 collective-permute-start.6
  40.8 0.0 collective-permute-done.7.h2_ref
  40.8 2.2 %collective-permute-done.8.h3_ref = bf16[128,512]{1,0:T(8,128)(2,1)S(1)} collective-permute-done((bf16[128,512]{1,0:T(8,128)(2,1)S(1)}, bf16[128,512]{1,0:T(8,128)(2,1)S(1)}, u32[]{:S(2)}, u32[]{:S(2)}) %collective-permute-start.8) | collective-permute-done | bytes 131104 | tf_op jit(solution)/shard_map/ppermute | solution.py:505
  43.0 0.0 copy-start.3
  43.0 0.0 copy-start.5
  43.0 1.5 %shard_map.140.acc_ref = f32[128,2048]{1,0:T(8,128)S(1)} custom-call(s32[2]{0:T(128)S(1)} %pad_add_fusion.where_ref, bf16[128,512]{1,0:T(8,128)(2,1)S(1)} %get-tuple-element.25.h0_ref, bf16[128,512]{1,0:T(8,128)(2,1)S(1)} %collective-permute-done.7.h2_ref, bf16[128,512]{1,0:T(8,128)(2,1)S(1)} %collective-permute-done.8.h3_ref, ...), custom_call_target="tpu_custom_call" | custom-call | tf_op jit(solution)/shard_map/pallas_call | solution.py:379
  44.6 0.8 collective-permute-done.6.h1_ref
  45.3 0.0 copy-done.3
  45.4 0.0 copy-done.5
  45.4 0.0 copy-start.2
  45.4 2.2 %shard_map.141 = (bf16[128,2048]{1,0:T(8,128)(2,1)S(1)}, bf16[512,16,128]{2,1,0:T(8,128)(2,1)S(1)}) custom-call(s32[2]{0:T(128)S(1)} %pad_add_fusion.where_ref, s32[2,128]{1,0:T(2,128)S(1)} %get-tuple-element.18.slot_ref, bf16[128,512]{1,0:T(8,128)(2,1)S(1)} %collective-permute-done.6.h1_ref, f32[128,2048]{1,0:T(8,128)S(1)} %shard_map.140.acc_ref, ...), custom_call_target="tpu_custom_call" | custom-call | tf_op jit(solution)/shard_map/pallas_call | solution.py:379
  47.6 0.0 copy-start
  47.6 0.0 copy-start.1
  47.6 38.3 %all_to_all.10 = bf16[128,64,128]{2,1,0:T(8,128)(2,1)S(1)} all-to-all(bf16[128,64,128]{2,1,0:T(8,128)(2,1)S(1)} %bitcast.23), channel_id=1, replica_groups=mesh['sp'=32,'tp'=4] {'sp','tp'}, dimensions={0} | all-to-all | bytes 4194304 | tf_op jit(solution)/shard_map/all_to_all | solution.py:530
  85.9 0.0 copy-done.2
  85.9 0.0 copy-done
  85.9 0.0 copy-done.1
  85.9 5.4 %shard_map.142 = bf16[512,16,128]{2,1,0:T(8,128)(2,1)S(1)} custom-call(bf16[512,16,128]{2,1,0:T(8,128)(2,1)S(1)} %bitcast.20, bf16[1,2048,512]{2,1,0:T(8,128)(2,1)S(1)} %copy-done, bf16[1,2048,512]{2,1,0:T(8,128)(2,1)S(1)} %copy-done.1, bf16[1,512,2048]{2,1,0:T(8,128)(2,1)S(1)} %copy-done.2), custom_call_target="tpu_custom_call" | custom-call | tf_op jit(solution)/shard_map/pallas_call | solution.py:379
  91.4 0.0 copy-start.6
  91.4 34.2 %all_to_all.11 = bf16[128,64,128]{2,1,0:T(8,128)(2,1)S(1)} all-to-all(bf16[128,64,128]{2,1,0:T(8,128)(2,1)S(1)} %bitcast.21), channel_id=1, replica_groups=mesh['sp'=32,'tp'=4] {'sp','tp'}, dimensions={0} | all-to-all | bytes 4194304 | tf_op jit(solution)/shard_map/all_to_all | solution.py:530
  125.5 0.0 copy-done.6
  125.5 2.4 %shard_map.143 = bf16[128,2048]{1,0:T(8,128)(2,1)} custom-call(s32[2,128]{1,0:T(2,128)S(1)} %get-tuple-element.18.slot_ref, f32[2,128]{1,0:T(2,128)S(1)} %bitcast.30, bf16[512,16,128]{2,1,0:T(8,128)(2,1)S(1)} %bitcast.22, bf16[128,2048]{1,0:T(8,128)(2,1)S(1)} %get-tuple-element.30.hid_ref), custom_call_target="tpu_custom_call" | custom-call | tf_op jit(solution)/shard_map/pallas_call | solution.py:379
  (8 shorter events, 0.1 us)
Async XLA Ops:
  0.0 25.1 %copy-start.4 = (s32[512]{0:T(512)S(1)}, s32[512]{0:T(512)}, u32[]{:S(2)}) copy-start(s32[512]{0:T(512)} %param.20) | copy-start | bytes 6148
  2.1 13.2 %collective-permute-start = (bf16[1040,128]{1,0:T(8,128)(2,1)S(1)}, bf16[1040,128]{1,0:T(8,128)(2,1)S(1)}, u32[]{:S(2)}, u32[]{:S(2)}) collective-permute-start(bf16[1040,128]{1,0:T(8,128)(2,1)S(1)} %key_prep.1.own), channel_id=1, source_target_pairs={{0,8},{4,12},{8,16},{12,20},{16,24},{20,28},{24,32},{28,36},{32,40... | collective-permute-start | bytes 798728 | tf_op jit(solution)/shard_map/ppermute | solution.py:422
  4.3 11.0 %collective-permute-start.2 = (bf16[1040,128]{1,0:T(8,128)(2,1)S(1)}, bf16[1040,128]{1,0:T(8,128)(2,1)S(1)}, u32[]{:S(2)}, u32[]{:S(2)}) collective-permute-start(bf16[1040,128]{1,0:T(8,128)(2,1)S(1)} %key_prep.1.own), channel_id=1, source_target_pairs={{0,120},{4,124},{8,0},{12,4},{16,8},{20,12},{24,16},{28,20},{32,24... | collective-permute-start | bytes 798728 | tf_op jit(solution)/shard_map/ppermute | solution.py:423
  9.3 15.9 %collective-permute-start.5 = (bf16[1040,128]{1,0:T(8,128)(2,1)S(1)}, bf16[1040,128]{1,0:T(8,128)(2,1)S(1)}, u32[]{:S(2)}, u32[]{:S(2)}) collective-permute-start(bf16[1040,128]{1,0:T(8,128)(2,1)S(1)} %key_prep.1.own), channel_id=1, source_target_pairs={{0,4},{4,0},{8,12},{12,8},{16,20},{20,16},{24,28},{28,24},{32,36},... | collective-permute-start | bytes 798728 | tf_op jit(solution)/shard_map/ppermute | solution.py:424
  15.3 16.2 %collective-permute-start.4 = (bf16[1040,128]{1,0:T(8,128)(2,1)S(1)}, bf16[1040,128]{1,0:T(8,128)(2,1)S(1)}, u32[]{:S(2)}, u32[]{:S(2)}) collective-permute-start(bf16[1040,128]{1,0:T(8,128)(2,1)S(1)} %broadcast_select_fusion), channel_id=1, source_target_pairs={{0,124},{4,8},{8,4},{12,16},{16,12},{20,24},{24,20},{28,32},{32,28... | collective-permute-start | bytes 798728 | tf_op jit(solution)/shard_map/ppermute | solution.py:425
  15.4 16.2 %collective-permute-start.1 = (bf16[1040,128]{1,0:T(8,128)(2,1)S(1)}, bf16[1040,128]{1,0:T(8,128)(2,1)S(1)}, u32[]{:S(2)}, u32[]{:S(2)}) collective-permute-start(bf16[1040,128]{1,0:T(8,128)(2,1)S(1)} %collective-permute-done.b1), channel_id=1, source_target_pairs={{0,4},{4,0},{8,12},{12,8},{16,20},{20,16},{24,28},{28,24},{32,36},... | collective-permute-start | bytes 798728 | tf_op jit(solution)/shard_map/ppermute | solution.py:426
  20.4 11.2 %collective-permute-start.3 = (bf16[1040,128]{1,0:T(8,128)(2,1)S(1)}, bf16[1040,128]{1,0:T(8,128)(2,1)S(1)}, u32[]{:S(2)}, u32[]{:S(2)}) collective-permute-start(bf16[1040,128]{1,0:T(8,128)(2,1)S(1)} %collective-permute-done.2.b3), channel_id=1, source_target_pairs={{0,4},{4,0},{8,12},{12,8},{16,20},{20,16},{24,28},{28,24},{32,36},... | collective-permute-start | bytes 798728 | tf_op jit(solution)/shard_map/ppermute | solution.py:427
  34.1 6.7 %collective-permute-start.7 = (bf16[128,512]{1,0:T(8,128)(2,1)S(1)}, bf16[128,512]{1,0:T(8,128)(2,1)S(1)}, u32[]{:S(2)}, u32[]{:S(2)}) collective-permute-start(bf16[128,512]{1,0:T(8,128)(2,1)S(1)} %get-tuple-element.26), channel_id=1, source_target_pairs={{0,2},{1,3},{2,0},{3,1},{4,6},{5,7},{6,4},{7,5},{8,10},{9,11},{10,... | collective-permute-start | bytes 393224 | tf_op jit(solution)/shard_map/ppermute | solution.py:505
  36.6 6.4 %collective-permute-start.8 = (bf16[128,512]{1,0:T(8,128)(2,1)S(1)}, bf16[128,512]{1,0:T(8,128)(2,1)S(1)}, u32[]{:S(2)}, u32[]{:S(2)}) collective-permute-start(bf16[128,512]{1,0:T(8,128)(2,1)S(1)} %get-tuple-element.27), channel_id=1, source_target_pairs={{0,3},{1,0},{2,1},{3,2},{4,7},{5,4},{6,5},{7,6},{8,11},{9,8},{10,9... | collective-permute-start | bytes 393224 | tf_op jit(solution)/shard_map/ppermute | solution.py:505
  39.6 5.7 %collective-permute-start.6 = (bf16[128,512]{1,0:T(8,128)(2,1)S(1)}, bf16[128,512]{1,0:T(8,128)(2,1)S(1)}, u32[]{:S(2)}, u32[]{:S(2)}) collective-permute-start(bf16[128,512]{1,0:T(8,128)(2,1)S(1)} %get-tuple-element.24), channel_id=1, source_target_pairs={{0,1},{1,2},{2,3},{3,0},{4,5},{5,6},{6,7},{7,4},{8,9},{9,10},{10,1... | collective-permute-start | bytes 393224 | tf_op jit(solution)/shard_map/ppermute | solution.py:505
  43.0 2.3 %copy-start.3 = (bf16[128,2048]{1,0:T(8,128)(2,1)S(1)}, bf16[128,2048]{1,0:T(8,128)(2,1)}, u32[]{:S(2)}) copy-start(bf16[128,2048]{1,0:T(8,128)(2,1)} %res_ref.1) | copy-start | bytes 1572868
  43.0 2.3 %copy-start.5 = (f32[2048]{0:T(1024)S(1)}, f32[2048]{0:T(1024)}, u32[]{:S(2)}) copy-start(f32[2048]{0:T(1024)} %param.22) | copy-start | bytes 24580
  45.4 40.6 %copy-start.2 = (bf16[1,512,2048]{2,1,0:T(8,128)(2,1)S(1)}, bf16[1,512,2048]{2,1,0:T(8,128)(2,1)}, u32[]{:S(2)}) copy-start(bf16[1,512,2048]{2,1,0:T(8,128)(2,1)} %down_ref.1) | copy-start | bytes 6291460
  47.6 38.4 %copy-start = (bf16[1,2048,512]{2,1,0:T(8,128)(2,1)S(1)}, bf16[1,2048,512]{2,1,0:T(8,128)(2,1)}, u32[]{:S(2)}) copy-start(bf16[1,2048,512]{2,1,0:T(8,128)(2,1)} %gate_ref.1) | copy-start | bytes 6291460
  47.6 38.4 %copy-start.1 = (bf16[1,2048,512]{2,1,0:T(8,128)(2,1)S(1)}, bf16[1,2048,512]{2,1,0:T(8,128)(2,1)}, u32[]{:S(2)}) copy-start(bf16[1,2048,512]{2,1,0:T(8,128)(2,1)} %up_ref.1) | copy-start | bytes 6291460
  91.4 34.2 %copy-start.6 = (f32[128,2]{0,1:T(2,128)S(1)}, f32[128,2]{0,1:T(2,128)}, u32[]{:S(2)}) copy-start(f32[128,2]{0,1:T(2,128)} %param.24) | copy-start | bytes 3076

commit v5 on v4

--- a/solution.py
+++ b/solution.py
@@ -40,7 +40,14 @@
 
 def norm_rotate(x, gain, cos_full, sin_full):
     wide = x.astype(jnp.float32)
-    mean = jnp.mean(wide * wide, axis=-1, keepdims=True)
+    square = wide * wide
+    high = square.astype(jnp.bfloat16)
+    low = (square - high.astype(jnp.float32)).astype(jnp.bfloat16)
+    ones = jnp.ones((HEAD, HEAD), jnp.bfloat16)
+    mean = (
+        jnp.dot(high, ones, preferred_element_type=jnp.float32)
+        + jnp.dot(low, ones, preferred_element_type=jnp.float32)
+    ) * (1.0 / HEAD)
     scaled = wide * lax.rsqrt(mean + norm_eps) * gain
     return (scaled * cos_full + pltpu.roll(scaled, HALF, 1) * sin_full).astype(jnp.bfloat16)
 
@@ -71,8 +78,18 @@
     copies[3].wait()
 
 
+def pick_kernel(edge_ref, left_ref, right_ref, out_ref):
+    @pl.when(edge_ref[edge_ref.shape[0] - 2, 0] == 1)
+    def _():
+        out_ref[...] = left_ref[...]
+
+    @pl.when(edge_ref[edge_ref.shape[0] - 2, 0] == 0)
+    def _():
+        out_ref[...] = right_ref[...]
+
+
 def query_kernel(
-    q_hbm, ids_hbm, doc_hbm, gain_hbm, row_ref, col_ref, out_ref, qdoc_ref, slot_ref,
+    where_ref, q_hbm, ids_hbm, doc_hbm, gain_hbm, row_ref, col_ref, out_ref, qdoc_ref, slot_ref, edge_ref,
     q_ref, ids_ref, doc_ref, gain_ref, sems, *, capacity,
 ):
     copies = [
@@ -85,6 +102,10 @@
         copy.start()
     for copy in copies:
         copy.wait()
+    tiles = doc_ref.shape[0]
+    edge_ref[0:tiles, :] = doc_ref[...]
+    for n in range(2):
+        edge_ref[tiles + n : tiles + n + 1, :] = jnp.full((1, HEAD), where_ref[n], jnp.int32)
     rows, width = q_ref.shape
     gain = gain_ref[...]
     for g in range(rows // GRID_W):
@@ -115,7 +136,7 @@
 
 
 def attend(
-    quarters, edge_ref, q_ref, qdoc_ref, sources, state, out_refs,
+    quarters, edge_ref, q_ref, qdoc_ref, sources, state, store, out_refs,
     k_ref, v_ref, d_ref, list_ref, s_even, s_odd, mx_even, mx_odd, l_scr, acc_scr,
 ):
     rows, width = q_ref.shape
@@ -146,14 +167,10 @@
         counts.append(count)
     s_refs = (s_even, s_odd)
     mx_refs = (mx_even, mx_odd)
-    spare = len(sources)
-    for ref in s_refs:
-        ref[spare] = jnp.full(ref.shape[1:], LOW, jnp.float32)
 
     def scores(n, i):
         s_ref, mx_ref = s_refs[n % 2], mx_refs[n % 2]
         slot = list_ref[n, i]
-        index = jnp.where(i < counts[n], i, spare + 1)
 
         def line(r):
             return pl.ds(pl.multiple_of(quarters[n] * block + r * 16, 16), 16)
@@ -180,19 +197,18 @@
                 for t in range(tiles):
                     lanes = slice(t * HEAD, (t + 1) * HEAD)
                     part = jnp.where(keep[t], s[band, lanes], LOW)
-                    s_ref[index, band, lanes] = part
+                    s_ref[i, band, lanes] = part
                     top = jnp.maximum(top, part)
                 mx_ref[band, :] = top
 
     def weigh(n, i):
         s_ref, mx_ref = s_refs[n % 2], mx_refs[n % 2]
         slot = list_ref[n, i]
-        index = jnp.where(i < counts[n], i, spare)
         top = mx_ref[...]
         probs = []
         run = l_scr[...]
         for t in range(tiles):
-            e = jnp.exp2(s_ref[index, :, t * HEAD : (t + 1) * HEAD] * scale - top)
+            e = jnp.exp2(s_ref[i, :, t * HEAD : (t + 1) * HEAD] * scale - top)
             run = run + e
             probs.append(e.astype(jnp.bfloat16))
         l_scr[...] = run
@@ -200,18 +216,15 @@
             jnp.concatenate(probs, axis=1), v_ref[slot], preferred_element_type=jnp.float32
         )
 
-    m_ref, l_ref, acc_ref = state
+    m_ref, l_ref, acc_ref = state or (None,) * 3
     for step in range(total + 1):
-        trip = counts[step] if step == 0 else counts[step - 1]
-        if 0 < step < total:
-            trip = jnp.maximum(trip, counts[step])
         if step < total:
-            if out_refs is None:
+            if state is None:
                 mx_refs[step % 2][...] = jnp.full(mx_even.shape, LOW, jnp.float32)
             else:
                 mx_refs[step % 2][...] = m_ref[quarters[step]]
         if step > 0:
-            if out_refs is None:
+            if state is None:
                 l_scr[...] = jnp.zeros(l_scr.shape, jnp.float32)
                 acc_scr[...] = jnp.zeros(acc_scr.shape, jnp.float32)
             else:
@@ -220,23 +233,36 @@
                 l_scr[...] = l_ref[before] * shrink
                 acc_scr[...] = acc_ref[before] * shrink
 
-        def body(i, carry, step=step):
-            if step > 0:
-                weigh(step - 1, i)
-            if step < total:
-                scores(step, i)
+        def both(i, carry, step=step):
+            weigh(step - 1, i)
+            scores(step, i)
             return carry
 
-        lax.fori_loop(0, trip, body, 0)
+        def behind(i, carry, step=step):
+            weigh(step - 1, i)
+            return carry
+
+        def ahead(i, carry, step=step):
+            scores(step, i)
+            return carry
+
+        shared = 0
+        if 0 < step < total:
+            shared = jnp.minimum(counts[step - 1], counts[step])
+            lax.fori_loop(0, shared, both, 0)
+        if step > 0:
+            lax.fori_loop(shared, counts[step - 1], behind, 0)
+        if step < total:
+            lax.fori_loop(shared, counts[step], ahead, 0)
         if step < total:
             ref = mx_refs[step % 2]
             top = jnp.broadcast_to(jnp.max(ref[...], axis=1, keepdims=True), ref.shape)
-            if out_refs is None:
-                m_ref[quarters[step]] = top
+            if store is not None:
+                store[0][quarters[step]] = top
             ref[...] = top * scale
-        if step > 0 and out_refs is None:
-            l_ref[quarters[step - 1]] = l_scr[...]
-            acc_ref[quarters[step - 1]] = acc_scr[...]
+        if step > 0 and store is not None:
+            store[1][quarters[step - 1]] = l_scr[...]
+            store[2][quarters[step - 1]] = acc_scr[...]
         elif step > 0:
             den = jnp.sum(l_scr[...], axis=1, keepdims=True)
             res = (acc_scr[...] / den).astype(jnp.bfloat16)
@@ -248,34 +274,42 @@
                     ]
 
 
-def early_attention(
-    edge_ref, w_hbm, q_ref, qdoc_ref, own, near, b1, b3, m_ref, l_ref, acc_ref, w_ref, *scratch
-):
+def home_attention(edge_ref, w_hbm, q_ref, qdoc_ref, own, near, m_ref, l_ref, acc_ref, w_ref, *scratch):
     fetch = pltpu.make_async_copy(w_hbm, w_ref, scratch[-1])
     fetch.start()
-    state = (m_ref, l_ref, acc_ref)
-    sources = (own, near, b1, b3)
-    attend(range(4), edge_ref, q_ref, qdoc_ref, sources, state, None, *scratch[:-1])
+    store = (m_ref, l_ref, acc_ref)
+    attend(range(4), edge_ref, q_ref, qdoc_ref, (own, near), None, store, None, *scratch[:-1])
     fetch.wait()
 
 
+def early_attention(
+    edge_ref, q_ref, qdoc_ref, b1, b3, m_in, l_in, acc_in, m_ref, l_ref, acc_ref, *scratch
+):
+    state, store = (m_in, l_in, acc_in), (m_ref, l_ref, acc_ref)
+    attend(range(4), edge_ref, q_ref, qdoc_ref, (b1, b3), state, store, None, *scratch)
+
+
+def home_index(edge_ref):
+    return edge_ref[edge_ref.shape[0] - 1, 0]
+
+
 def late_attention(
-    where_ref, edge_ref, q_ref, qdoc_ref, b2, b4, far, m_ref, l_ref, acc_ref, out_a, out_b,
+    edge_ref, q_ref, qdoc_ref, b2, b4, far, m_ref, l_ref, acc_ref, out_a, out_b,
     *scratch, ahead,
 ):
-    quarters = [(where_ref[1] + k) % 4 for k in ahead]
+    quarters = [(home_index(edge_ref) + k) % 4 for k in ahead]
     state = (m_ref, l_ref, acc_ref)
     sources = (b2, b4, far)
-    attend(quarters, edge_ref, q_ref, qdoc_ref, sources, state, (out_a, out_b), *scratch)
+    attend(quarters, edge_ref, q_ref, qdoc_ref, sources, state, None, (out_a, out_b), *scratch)
 
 
 def weight_rows(w_ref, group, part):
     return w_ref[pl.ds(pl.multiple_of(group * part, part), part), :]
 
 
-def project_part_kernel(where_ref, h0_ref, h2_ref, h3_ref, w_ref, acc_ref):
+def project_part_kernel(edge_ref, h0_ref, h2_ref, h3_ref, w_ref, acc_ref):
     part = h0_ref.shape[1]
-    home = where_ref[1]
+    home = home_index(edge_ref)
     acc = jnp.dot(h0_ref[...], weight_rows(w_ref, home, part), preferred_element_type=jnp.float32)
     for ref, back in ((h2_ref, 2), (h3_ref, 3)):
         acc += jnp.dot(
@@ -286,12 +320,12 @@
 
 
 def project_kernel(
-    where_ref, slot_ref, h1_ref, acc_ref, w_ref, res_ref, gain_ref, hid_ref, out_ref, n_scr
+    edge_ref, slot_ref, h1_ref, acc_ref, w_ref, res_ref, gain_ref, hid_ref, out_ref, n_scr
 ):
     rows, width = res_ref.shape
     fold = width // HEAD
     acc = acc_ref[...] + jnp.dot(
-        h1_ref[...], weight_rows(w_ref, (where_ref[1] + 3) % 4, h1_ref.shape[1]),
+        h1_ref[...], weight_rows(w_ref, (home_index(edge_ref) + 3) % 4, h1_ref.shape[1]),
         preferred_element_type=jnp.float32,
     )
     hidden = (res_ref[...].astype(jnp.float32) + acc).astype(jnp.bfloat16)
@@ -301,9 +335,6 @@
     normed = wide * lax.rsqrt(mean + norm_eps) * gain_ref[...]
     for c in range(fold):
         n_scr[pl.ds(c, rows, stride=fold), :] = normed[:, c * HEAD : (c + 1) * HEAD]
-    zero = jnp.zeros((32,) + out_ref.shape[1:], jnp.bfloat16)
-    for b in range(out_ref.shape[0] // 32):
-        out_ref[b * 32 : (b + 1) * 32] = zero
 
     def place(step, carry):
         for u in range(8):
@@ -422,9 +453,6 @@
     from_left = lax.ppermute(packed, "sp", right)
     from_right = lax.ppermute(packed, "sp", left)
     near = lax.ppermute(packed, "sp", swap)
-    far = lax.ppermute(jnp.where(par == 1, from_left, from_right), "sp", cross)
-    left_pair = lax.ppermute(from_left, "sp", swap)
-    right_pair = lax.ppermute(from_right, "sp", swap)
 
     quarter = rows // 4
     width = query_proj.shape[1]
@@ -434,12 +462,13 @@
     experts_all = sp * lax.axis_size("tp")
     capacity = max(2, 2 * token_rows * top_count // experts_all)
     slots = experts_all * capacity
-    query_norm, query_doc, slot = call(
+    query_norm, query_doc, slot, edges = call(
         functools.partial(query_kernel, capacity=capacity),
         (
             jax.ShapeDtypeStruct(query_proj.shape, bf16),
             jax.ShapeDtypeStruct((rows, HEAD), f32),
             jax.ShapeDtypeStruct((top_count, token_rows), jnp.int32),
+            jax.ShapeDtypeStruct((doc_lines.shape[0] + 2, HEAD), jnp.int32),
         ),
         8,
         scratch=(
@@ -449,13 +478,20 @@
             VMEM((1, HEAD), f32),
             pltpu.SemaphoreType.DMA((4,)),
         ),
+        smem=1,
         hbm=4,
         args=(
-            in_hbm(query_proj), in_hbm(expert_ids.T), in_hbm(doc_lines),
+            jnp.stack([par, lax.axis_index("tp")]).astype(jnp.int32), in_hbm(query_proj), in_hbm(expert_ids.T), in_hbm(doc_lines),
             in_hbm(query_gain.reshape(1, HEAD)), row_tab, col_tab,
         ),
     )
-    where = jnp.stack([par, lax.axis_index("tp")]).astype(jnp.int32)
+    passed = call(
+        pick_kernel, jax.ShapeDtypeStruct(packed.shape, bf16), 4, smem=1,
+        args=(edges, from_left, from_right),
+    )
+    far = lax.ppermute(passed, "sp", cross)
+    left_pair = lax.ppermute(from_left, "sp", swap)
+    right_pair = lax.ppermute(from_right, "sp", swap)
 
     def attention_scratch(count):
         return (
@@ -463,8 +499,8 @@
             VMEM((count, rows, HEAD), bf16),
             VMEM((count * rows // HEAD, 8, HEAD), f32),
             pltpu.SMEM((4, count + 1), jnp.int32),
-            VMEM((count + 2, rows, rows), f32),
-            VMEM((count + 2, rows, rows), f32),
+            VMEM((count, rows, rows), f32),
+            VMEM((count, rows, rows), f32),
             VMEM((rows, HEAD), f32),
             VMEM((rows, HEAD), f32),
             VMEM((rows, HEAD), f32),
@@ -474,7 +510,7 @@
     part_shape = jax.ShapeDtypeStruct((quarter, width), bf16)
     state_shape = jax.ShapeDtypeStruct((4, rows, HEAD), f32)
     top, sums, values, weight_near = call(
-        early_attention,
+        home_attention,
         (
             state_shape,
             state_shape,
@@ -482,21 +518,24 @@
             jax.ShapeDtypeStruct(output_weight.shape, bf16),
         ),
         24,
-        scratch=attention_scratch(4) + (pltpu.SemaphoreType.DMA,),
+        scratch=attention_scratch(2) + (pltpu.SemaphoreType.DMA,),
         smem=1,
         hbm=1,
-        args=(
-            doc_lines, in_hbm(output_weight), query_norm, query_doc, packed, near, from_left,
-            from_right,
-        ),
+        args=(edges, in_hbm(output_weight), query_norm, query_doc, packed, near),
+    )
+    top, sums, values = call(
+        early_attention, (state_shape, state_shape, state_shape), 24,
+        scratch=attention_scratch(2),
+        smem=1,
+        args=(edges, query_norm, query_doc, from_left, from_right, top, sums, values),
     )
 
     def late(ahead):
         return call(
             functools.partial(late_attention, ahead=ahead), (part_shape, part_shape), 24,
-            scratch=attention_scratch(3), smem=2,
+            scratch=attention_scratch(3), smem=1,
             args=(
-                where, doc_lines, query_norm, query_doc, left_pair, right_pair, far, top, sums,
+                edges, query_norm, query_doc, left_pair, right_pair, far, top, sums,
                 values,
             ),
         )
@@ -511,7 +550,7 @@
     heads_1 = ahead_by(ahead_1, 1)
     partial = call(
         project_part_kernel, jax.ShapeDtypeStruct((token_rows, wide), f32), 16,
-        smem=1, args=(where, at_home, heads_2, heads_3, weight_near),
+        smem=1, args=(edges, at_home, heads_2, heads_3, weight_near),
     )
     hidden, outgoing = call(
         project_kernel,
@@ -522,7 +561,7 @@
         16,
         scratch=(VMEM((token_rows * fold, HEAD), f32),),
         smem=2,
-        args=(where, slot, heads_1, partial, weight_near, residual, norm_gain.reshape(1, wide)),
+        args=(edges, slot, heads_1, partial, weight_near, residual, norm_gain.reshape(1, wide)),
     )
 
     def exchange(x):

time: 128 us -> 125 us (0.977)
  waiting for transfers between devices: 8.08 us -> 5.91 us
    ppermute x1, waiting for transfers between devices: 5.06 us -> 2.52 us  [on_device(): from_left = lax.ppermute(packed, 'sp', right)]
    pallas_call x8 -> x10, Pallas kernels: 27.3 us -> 26.5 us  [call(): pl.pallas_call(kernel, out_shape=out_shape, in_specs=specs, out_specs=jax...]
  transfers between devices with their start and end apart: 9 -> 9, of which waited for: 3 -> 3; matrix products, arithmetic and copies ran while one was open for 0% -> 0% of each run, Pallas kernels for 12% -> 11%
where the time goes in v5:
time: 125 us
  blocking collectives  72.8 us (58%)
  Pallas kernels  27.8 us (22%)
  starting transfers between devices  17.6 us (14%)
  waiting for transfers between devices  5.91 us (5%)
    all_to_all x2, blocking collectives, exchange(): x = lax.all_to_all(x, ('sp', 'tp'), split_axis=0, concat_axis=0, tiled=True)  72.8 us
    pallas_call x10, Pallas kernels, call(): pl.pallas_call(kernel, out_shape=out_shape, in_specs=specs, out_specs=jax...  26.5 us
    ppermute x1, starting transfers between devices, on_device(): from_right = lax.ppermute(packed, 'sp', left)  4.99 us
    ppermute x1, starting transfers between devices, on_device(): left_pair = lax.ppermute(from_left, 'sp', swap)  4.96 us
    ppermute x3, starting transfers between devices, ahead_by(): return lax.ppermute(x, 'tp', [(i, (i + k) % 4) for i in range(4)])  4.38 us
    ppermute x3, waiting for transfers between devices, ahead_by(): return lax.ppermute(x, 'tp', [(i, (i + k) % 4) for i in range(4)])  3.38 us
    ppermute x1, waiting for transfers between devices, on_device(): from_left = lax.ppermute(packed, 'sp', right)  2.52 us
  transfers between devices with their start and end apart: 9, of which 3 were waited for; matrix products, arithmetic and copies ran while one was open for 0% of the time, Pallas kernels for 11%

profile of v5, /device:TPU:1, one launch (start us, length us, event | category | flops | bytes accessed | tf_op | source)
XLA Modules:
  0.0 124.9 jit_solution(896033668090437740)
XLA Ops:
  0.0 0.1 multiply_cosine_fusion.1
  0.2 0.2 multiply_cosine_fusion
  0.4 0.1 fusion.7
  0.5 0.1 fusion.1
  0.6 1.3 %key_prep.1.own = bf16[1040,128]{1,0:T(8,128)(2,1)S(1)} custom-call(bf16[512,128]{1,0:T(8,128)(2,1)} %k_hbm.1, bf16[512,128]{1,0:T(8,128)(2,1)} %v_hbm.1, s32[4,128]{1,0:T(4,128)} %bitcast.26, f32[1,128]{1,0:T(1,128)} %bitcast.30, f32[2,8,128]{2,1,0:T(8,128)S(1)} %pad_maximum_fusion.5.row_ref, f32[2,64,128]{2,1,0:T(8,128)S(1)} %pad_maximum_fusion.col_ref), custom_call_target="tpu_custom_call" | custom-call | tf_op jit(solution)/shard_map/key_prep/pallas_call | solution.py:430
  1.9 2.2 %collective-permute-start = (bf16[1040,128]{1,0:T(8,128)(2,1)S(1)}, bf16[1040,128]{1,0:T(8,128)(2,1)S(1)}, u32[]{:S(2)}, u32[]{:S(2)}) collective-permute-start(bf16[1040,128]{1,0:T(8,128)(2,1)S(1)} %key_prep.1.own), channel_id=1, source_target_pairs={{0,8},{4,12},{8,16},{12,20},{16,24},{20,28},{24,32},{28,36},{32,40... | collective-permute-start | bytes 798728 | tf_op jit(solution)/shard_map/ppermute | solution.py:453
  4.1 5.0 %collective-permute-start.2 = (bf16[1040,128]{1,0:T(8,128)(2,1)S(1)}, bf16[1040,128]{1,0:T(8,128)(2,1)S(1)}, u32[]{:S(2)}, u32[]{:S(2)}) collective-permute-start(bf16[1040,128]{1,0:T(8,128)(2,1)S(1)} %key_prep.1.own), channel_id=1, source_target_pairs={{0,120},{4,124},{8,0},{12,4},{16,8},{20,12},{24,16},{28,20},{32,24... | collective-permute-start | bytes 798728 | tf_op jit(solution)/shard_map/ppermute | solution.py:454
  9.1 1.0 collective-permute-start.5
  10.0 0.1 pad_add_fusion.where_ref
  10.1 2.5 %shard_map.136 = (bf16[512,512]{1,0:T(8,128)(2,1)S(1)}, f32[512,128]{1,0:T(8,128)S(1)}, s32[2,128]{1,0:T(2,128)S(1)}, s32[6,128]{1,0:T(8,128)S(1)}) custom-call(s32[2]{0:T(128)S(1)} %pad_add_fusion.where_ref, bf16[512,512]{1,0:T(8,128)(2,1)} %q_hbm.1, s32[2,128]{1,0:T(2,128)} %bitcast.28, s32[4,128]{1,0:T(4,128)} %bitcast.27, f32[1,128]{1,0:T(1,128)} %bitcast.29, ...), custom_call_target="tpu_custom_call" | custom-call | tf_op jit(solution)/shard_map/pallas_call | solution.py:410
  12.6 2.5 %collective-permute-done.left_ref.b1 = bf16[1040,128]{1,0:T(8,128)(2,1)S(1)} collective-permute-done((bf16[1040,128]{1,0:T(8,128)(2,1)S(1)}, bf16[1040,128]{1,0:T(8,128)(2,1)S(1)}, u32[]{:S(2)}, u32[]{:S(2)}) %collective-permute-start) | collective-permute-done | bytes 266272 | tf_op jit(solution)/shard_map/ppermute | solution.py:453
  15.1 0.0 collective-permute-done.2.right_ref.b3
  15.1 0.6 shard_map.137
  15.7 0.1 collective-permute-start.4
  15.8 5.0 %collective-permute-start.1 = (bf16[1040,128]{1,0:T(8,128)(2,1)S(1)}, bf16[1040,128]{1,0:T(8,128)(2,1)S(1)}, u32[]{:S(2)}, u32[]{:S(2)}) collective-permute-start(bf16[1040,128]{1,0:T(8,128)(2,1)S(1)} %collective-permute-done.left_ref.b1), channel_id=1, source_target_pairs={{0,4},{4,0},{8,12},{12,8},{16,20},{20,16},{24,28},{28,24},{32,36},... | collective-permute-start | bytes 798728 | tf_op jit(solution)/shard_map/ppermute | solution.py:493
  20.8 0.0 collective-permute-start.3
  20.8 0.0 collective-permute-done.5.near
  20.8 4.5 %shard_map.138 = (f32[4,512,128]{2,1,0:T(8,128)S(1)}, f32[4,512,128]{2,1,0:T(8,128)S(1)}, f32[4,512,128]{2,1,0:T(8,128)S(1)}, bf16[2048,2048]{1,0:T(8,128)(2,1)S(1)}) custom-call(s32[6,128]{1,0:T(8,128)S(1)} %get-tuple-element.23.edge_ref, bf16[2048,2048]{1,0:T(8,128)(2,1)} %w_hbm.1, bf16[512,512]{1,0:T(8,128)(2,1)S(1)} %get-tuple-element.24.q_ref, ...), custom_call_target="tpu_custom_call" | custom-call | tf_op jit(solution)/shard_map/pallas_call | solution.py:410
  25.3 3.0 %shard_map.139 = (f32[4,512,128]{2,1,0:T(8,128)S(1)}, f32[4,512,128]{2,1,0:T(8,128)S(1)}, f32[4,512,128]{2,1,0:T(8,128)S(1)}) custom-call(s32[6,128]{1,0:T(8,128)S(1)} %get-tuple-element.23.edge_ref, bf16[512,512]{1,0:T(8,128)(2,1)S(1)} %get-tuple-element.24.q_ref, f32[512,128]{1,0:T(8,128)S(1)} %get-tuple-element.25.qdoc_ref, ...), custom_call_target="tpu_custom_call" | custom-call | tf_op jit(solution)/shard_map/pallas_call | solution.py:410
  28.2 0.0 collective-permute-done.4.far
  28.3 0.0 collective-permute-done.1.b2
  28.3 0.0 collective-permute-done.3.b4
  28.3 2.6 %shard_map.141 = (bf16[128,512]{1,0:T(8,128)(2,1)S(1)}, bf16[128,512]{1,0:T(8,128)(2,1)S(1)}) custom-call(s32[6,128]{1,0:T(8,128)S(1)} %get-tuple-element.23.edge_ref, bf16[512,512]{1,0:T(8,128)(2,1)S(1)} %get-tuple-element.24.q_ref, f32[512,128]{1,0:T(8,128)S(1)} %get-tuple-element.25.qdoc_ref, bf16[1040,128]{1,0:T(8,128)(2,1)S(1)} %collective-permute-done.1.b2, ...), custom_call_target="tpu_custom_call" | custom-call | tf_op jit(solution)/shard_map/pallas_call | solution.py:410
  30.8 2.4 %collective-permute-start.7 = (bf16[128,512]{1,0:T(8,128)(2,1)S(1)}, bf16[128,512]{1,0:T(8,128)(2,1)S(1)}, u32[]{:S(2)}, u32[]{:S(2)}) collective-permute-start(bf16[128,512]{1,0:T(8,128)(2,1)S(1)} %get-tuple-element.34), channel_id=1, source_target_pairs={{0,2},{1,3},{2,0},{3,1},{4,6},{5,7},{6,4},{7,5},{8,10},{9,11},{10,... | collective-permute-start | bytes 393224 | tf_op jit(solution)/shard_map/ppermute | solution.py:544
  33.2 0.8 collective-permute-start.8
  34.1 1.9 %shard_map.140 = (bf16[128,512]{1,0:T(8,128)(2,1)S(1)}, bf16[128,512]{1,0:T(8,128)(2,1)S(1)}) custom-call(s32[6,128]{1,0:T(8,128)S(1)} %get-tuple-element.23.edge_ref, bf16[512,512]{1,0:T(8,128)(2,1)S(1)} %get-tuple-element.24.q_ref, f32[512,128]{1,0:T(8,128)S(1)} %get-tuple-element.25.qdoc_ref, bf16[1040,128]{1,0:T(8,128)(2,1)S(1)} %collective-permute-done.1.b2, ...), custom_call_target="tpu_custom_call" | custom-call | tf_op jit(solution)/shard_map/pallas_call | solution.py:410
  36.0 1.2 collective-permute-start.6
  37.1 0.0 collective-permute-done.7.h2_ref
  37.1 3.0 %collective-permute-done.8.h3_ref = bf16[128,512]{1,0:T(8,128)(2,1)S(1)} collective-permute-done((bf16[128,512]{1,0:T(8,128)(2,1)S(1)}, bf16[128,512]{1,0:T(8,128)(2,1)S(1)}, u32[]{:S(2)}, u32[]{:S(2)}) %collective-permute-start.8) | collective-permute-done | bytes 131104 | tf_op jit(solution)/shard_map/ppermute | solution.py:544
  40.1 0.0 copy-start.3
  40.1 0.0 copy-start.4
  40.1 1.6 %shard_map.142.acc_ref = f32[128,2048]{1,0:T(8,128)S(1)} custom-call(s32[6,128]{1,0:T(8,128)S(1)} %get-tuple-element.23.edge_ref, bf16[128,512]{1,0:T(8,128)(2,1)S(1)} %get-tuple-element.33.h0_ref, bf16[128,512]{1,0:T(8,128)(2,1)S(1)} %collective-permute-done.7.h2_ref, bf16[128,512]{1,0:T(8,128)(2,1)S(1)} %collective-permute-done.8.h3_ref, ...), custom_call_target="tpu_custom_call" | custom-call | tf_op jit(solution)/shard_map/pallas_call | solution.py:410
  41.7 0.4 collective-permute-done.6.h1_ref
  42.1 0.0 copy-done.3
  42.1 0.0 copy-done.4
  42.1 0.0 copy-start.2
  42.1 2.0 %shard_map.143 = (bf16[128,2048]{1,0:T(8,128)(2,1)S(1)}, bf16[512,16,128]{2,1,0:T(8,128)(2,1)S(1)}) custom-call(s32[6,128]{1,0:T(8,128)S(1)} %get-tuple-element.23.edge_ref, s32[2,128]{1,0:T(2,128)S(1)} %get-tuple-element.22.slot_ref, bf16[128,512]{1,0:T(8,128)(2,1)S(1)} %collective-permute-done.6.h1_ref, f32[128,2048]{1,0:T(8,128)S(1)} %shard_map.142.acc_ref, ...), custom_call_target="tpu_custom_call" | custom-call | tf_op jit(solution)/shard_map/pallas_call | solution.py:410
  44.2 0.0 copy-start
  44.2 0.0 copy-start.1
  44.2 38.7 %all_to_all.10 = bf16[128,64,128]{2,1,0:T(8,128)(2,1)S(1)} all-to-all(bf16[128,64,128]{2,1,0:T(8,128)(2,1)S(1)} %bitcast.23), channel_id=1, replica_groups=mesh['sp'=32,'tp'=4] {'sp','tp'}, dimensions={0} | all-to-all | bytes 4194304 | tf_op jit(solution)/shard_map/all_to_all | solution.py:569
  82.9 0.0 copy-done.2
  82.9 0.0 copy-done
  82.9 0.0 copy-done.1
  82.9 5.4 %shard_map.144 = bf16[512,16,128]{2,1,0:T(8,128)(2,1)S(1)} custom-call(bf16[512,16,128]{2,1,0:T(8,128)(2,1)S(1)} %bitcast.20, bf16[1,2048,512]{2,1,0:T(8,128)(2,1)S(1)} %copy-done, bf16[1,2048,512]{2,1,0:T(8,128)(2,1)S(1)} %copy-done.1, bf16[1,512,2048]{2,1,0:T(8,128)(2,1)S(1)} %copy-done.2), custom_call_target="tpu_custom_call" | custom-call | tf_op jit(solution)/shard_map/pallas_call | solution.py:410
  88.3 0.0 copy-start.5
  88.3 34.2 %all_to_all.11 = bf16[128,64,128]{2,1,0:T(8,128)(2,1)S(1)} all-to-all(bf16[128,64,128]{2,1,0:T(8,128)(2,1)S(1)} %bitcast.21), channel_id=1, replica_groups=mesh['sp'=32,'tp'=4] {'sp','tp'}, dimensions={0} | all-to-all | bytes 4194304 | tf_op jit(solution)/shard_map/all_to_all | solution.py:569
  122.5 0.0 copy-done.5
  122.5 2.4 %shard_map.145 = bf16[128,2048]{1,0:T(8,128)(2,1)} custom-call(s32[2,128]{1,0:T(2,128)S(1)} %get-tuple-element.22.slot_ref, f32[2,128]{1,0:T(2,128)S(1)} %bitcast.25, bf16[512,16,128]{2,1,0:T(8,128)(2,1)S(1)} %bitcast.22, bf16[128,2048]{1,0:T(8,128)(2,1)S(1)} %get-tuple-element.38.hid_ref), custom_call_target="tpu_custom_call" | custom-call | tf_op jit(solution)/shard_map/pallas_call | solution.py:410
  (7 shorter events, 0.0 us)
Async XLA Ops:
  1.9 13.2 %collective-permute-start = (bf16[1040,128]{1,0:T(8,128)(2,1)S(1)}, bf16[1040,128]{1,0:T(8,128)(2,1)S(1)}, u32[]{:S(2)}, u32[]{:S(2)}) collective-permute-start(bf16[1040,128]{1,0:T(8,128)(2,1)S(1)} %key_prep.1.own), channel_id=1, source_target_pairs={{0,8},{4,12},{8,16},{12,20},{16,24},{20,28},{24,32},{28,36},{32,40... | collective-permute-start | bytes 798728 | tf_op jit(solution)/shard_map/ppermute | solution.py:453
  4.1 11.0 %collective-permute-start.2 = (bf16[1040,128]{1,0:T(8,128)(2,1)S(1)}, bf16[1040,128]{1,0:T(8,128)(2,1)S(1)}, u32[]{:S(2)}, u32[]{:S(2)}) collective-permute-start(bf16[1040,128]{1,0:T(8,128)(2,1)S(1)} %key_prep.1.own), channel_id=1, source_target_pairs={{0,120},{4,124},{8,0},{12,4},{16,8},{20,12},{24,16},{28,20},{32,24... | collective-permute-start | bytes 798728 | tf_op jit(solution)/shard_map/ppermute | solution.py:454
  9.1 11.7 %collective-permute-start.5 = (bf16[1040,128]{1,0:T(8,128)(2,1)S(1)}, bf16[1040,128]{1,0:T(8,128)(2,1)S(1)}, u32[]{:S(2)}, u32[]{:S(2)}) collective-permute-start(bf16[1040,128]{1,0:T(8,128)(2,1)S(1)} %key_prep.1.own), channel_id=1, source_target_pairs={{0,4},{4,0},{8,12},{12,8},{16,20},{20,16},{24,28},{28,24},{32,36},... | collective-permute-start | bytes 798728 | tf_op jit(solution)/shard_map/ppermute | solution.py:455
  15.7 12.5 %collective-permute-start.4 = (bf16[1040,128]{1,0:T(8,128)(2,1)S(1)}, bf16[1040,128]{1,0:T(8,128)(2,1)S(1)}, u32[]{:S(2)}, u32[]{:S(2)}) collective-permute-start(bf16[1040,128]{1,0:T(8,128)(2,1)S(1)} %shard_map.137), channel_id=1, source_target_pairs={{0,124},{4,8},{8,4},{12,16},{16,12},{20,24},{24,20},{28,32},{32,28... | collective-permute-start | bytes 798728 | tf_op jit(solution)/shard_map/ppermute | solution.py:492
  15.8 12.4 %collective-permute-start.1 = (bf16[1040,128]{1,0:T(8,128)(2,1)S(1)}, bf16[1040,128]{1,0:T(8,128)(2,1)S(1)}, u32[]{:S(2)}, u32[]{:S(2)}) collective-permute-start(bf16[1040,128]{1,0:T(8,128)(2,1)S(1)} %collective-permute-done.left_ref.b1), channel_id=1, source_target_pairs={{0,4},{4,0},{8,12},{12,8},{16,20},{20,16},{24,28},{28,24},{32,36},... | collective-permute-start | bytes 798728 | tf_op jit(solution)/shard_map/ppermute | solution.py:493
  20.8 7.5 %collective-permute-start.3 = (bf16[1040,128]{1,0:T(8,128)(2,1)S(1)}, bf16[1040,128]{1,0:T(8,128)(2,1)S(1)}, u32[]{:S(2)}, u32[]{:S(2)}) collective-permute-start(bf16[1040,128]{1,0:T(8,128)(2,1)S(1)} %collective-permute-done.2.right_ref.b3), channel_id=1, source_target_pairs={{0,4},{4,0},{8,12},{12,8},{16,20},{20,16},{24,28},{28,24},{32,36},... | collective-permute-start | bytes 798728 | tf_op jit(solution)/shard_map/ppermute | solution.py:494
  30.8 6.3 %collective-permute-start.7 = (bf16[128,512]{1,0:T(8,128)(2,1)S(1)}, bf16[128,512]{1,0:T(8,128)(2,1)S(1)}, u32[]{:S(2)}, u32[]{:S(2)}) collective-permute-start(bf16[128,512]{1,0:T(8,128)(2,1)S(1)} %get-tuple-element.34), channel_id=1, source_target_pairs={{0,2},{1,3},{2,0},{3,1},{4,6},{5,7},{6,4},{7,5},{8,10},{9,11},{10,... | collective-permute-start | bytes 393224 | tf_op jit(solution)/shard_map/ppermute | solution.py:544
  33.2 6.9 %collective-permute-start.8 = (bf16[128,512]{1,0:T(8,128)(2,1)S(1)}, bf16[128,512]{1,0:T(8,128)(2,1)S(1)}, u32[]{:S(2)}, u32[]{:S(2)}) collective-permute-start(bf16[128,512]{1,0:T(8,128)(2,1)S(1)} %get-tuple-element.35), channel_id=1, source_target_pairs={{0,3},{1,0},{2,1},{3,2},{4,7},{5,4},{6,5},{7,6},{8,11},{9,8},{10,9... | collective-permute-start | bytes 393224 | tf_op jit(solution)/shard_map/ppermute | solution.py:544
  36.0 6.2 %collective-permute-start.6 = (bf16[128,512]{1,0:T(8,128)(2,1)S(1)}, bf16[128,512]{1,0:T(8,128)(2,1)S(1)}, u32[]{:S(2)}, u32[]{:S(2)}) collective-permute-start(bf16[128,512]{1,0:T(8,128)(2,1)S(1)} %get-tuple-element.32), channel_id=1, source_target_pairs={{0,1},{1,2},{2,3},{3,0},{4,5},{5,6},{6,7},{7,4},{8,9},{9,10},{10,1... | collective-permute-start | bytes 393224 | tf_op jit(solution)/shard_map/ppermute | solution.py:544
  40.1 2.0 %copy-start.3 = (bf16[128,2048]{1,0:T(8,128)(2,1)S(1)}, bf16[128,2048]{1,0:T(8,128)(2,1)}, u32[]{:S(2)}) copy-start(bf16[128,2048]{1,0:T(8,128)(2,1)} %res_ref.1) | copy-start | bytes 1572868
  40.1 2.0 %copy-start.4 = (f32[2048]{0:T(1024)S(1)}, f32[2048]{0:T(1024)}, u32[]{:S(2)}) copy-start(f32[2048]{0:T(1024)} %param.22) | copy-start | bytes 24580
  42.1 40.7 %copy-start.2 = (bf16[1,512,2048]{2,1,0:T(8,128)(2,1)S(1)}, bf16[1,512,2048]{2,1,0:T(8,128)(2,1)}, u32[]{:S(2)}) copy-start(bf16[1,512,2048]{2,1,0:T(8,128)(2,1)} %down_ref.1) | copy-start | bytes 6291460
  44.2 38.7 %copy-start = (bf16[1,2048,512]{2,1,0:T(8,128)(2,1)S(1)}, bf16[1,2048,512]{2,1,0:T(8,128)(2,1)}, u32[]{:S(2)}) copy-start(bf16[1,2048,512]{2,1,0:T(8,128)(2,1)} %gate_ref.1) | copy-start | bytes 6291460
  44.2 38.7 %copy-start.1 = (bf16[1,2048,512]{2,1,0:T(8,128)(2,1)S(1)}, bf16[1,2048,512]{2,1,0:T(8,128)(2,1)}, u32[]{:S(2)}) copy-start(bf16[1,2048,512]{2,1,0:T(8,128)(2,1)} %up_ref.1) | copy-start | bytes 6291460
  88.3 34.2 %copy-start.5 = (f32[128,2]{0,1:T(2,128)S(1)}, f32[128,2]{0,1:T(2,128)}, u32[]{:S(2)}) copy-start(f32[128,2]{0,1:T(2,128)} %param.24) | copy-start | bytes 3076
